TPU v7x, 256 devices: a whole 4x4x8 slice. The times are simulated.
256 devices in a mesh: ep: 128 (over z, y, x), tp: 2 (over core).
Axes of the slice: x: 4, y: 4, z: 8, core: 2. Of those that a mesh axis runs over, the one named last changes fastest.
Arguments:
- tokens: bfloat16 [2048, 2048], P('ep'), may hold values from -6 to 6
- lengths: int32 [2048], P('ep'), may hold values from 1 to 1024, as said below
- attn_gain: float32 [2048], replicated, may hold values from 0.1 to 1.9
- w_query: bfloat16 [2048, 1024], P(None, 'tp'), may hold values from -0.125 to 0.125
- w_key: bfloat16 [2048, 128], P(None, 'tp'), may hold values from -0.125 to 0.125
- w_value: bfloat16 [2048, 128], P(None, 'tp'), may hold values from -0.125 to 0.125
- head_bias: float32 [16], P('tp'), may hold values from -7 to -2
- key_cache: bfloat16 [2048, 2, 64, 1024], P('ep', 'tp'), may hold values from -6 to 6
- value_cache: bfloat16 [2048, 2, 64, 1024], P('ep', 'tp'), may hold values from -6 to 6
- w_attn_out: bfloat16 [1024, 2048], P('tp'), may hold values from -0.1875 to 0.1875
- ffn_gain: float32 [2048], replicated, may hold values from 0.1 to 1.9
- w_router: bfloat16 [2048, 128], replicated, may hold values from -0.125 to 0.125
- routes: int32 [2048, 6], P('ep'), may hold values from 0 to 127, all different within a row; in each aligned block of 16 rows (0 to 15, 16 to 31, ...) at most 2 rows name the same one
- w_dense_gate: bfloat16 [2048, 512], P('ep', 'tp'), may hold values from -0.125 to 0.125
- w_dense_up: bfloat16 [2048, 512], P('ep', 'tp'), may hold values from -0.125 to 0.125
- w_dense_down: bfloat16 [512, 2048], P('tp', 'ep'), may hold values from -0.25 to 0.25
- dense_mix: float32 [2048], replicated, may hold values from -0.125 to 0.125
- w_expert_gate: bfloat16 [128, 2048, 512], P('ep', None, 'tp'), may hold values from -0.125 to 0.125
- w_expert_up: bfloat16 [128, 2048, 512], P('ep', None, 'tp'), may hold values from -0.125 to 0.125
- w_expert_down: bfloat16 [128, 512, 2048], P('ep', 'tp'), may hold values from -0.25 to 0.25
Outputs:
- layer_out: bfloat16 [2048, 2048], P('ep', 'tp')
- new_keys: bfloat16 [2048, 128], P('ep', 'tp')
- new_values: bfloat16 [2048, 128], P('ep', 'tp')
Inputs may be any that keep to these rules, and one draw needn't show every extreme that they name: `lengths`: every sequence holds between 1 and 1024 cached positions; in every draw some sequence holds exactly 1024. `routes`: each token names 6 different experts. Among the rows of one device no expert is named by more than 2 rows.
All inputs are finite; a program needn't handle non-finite values.
Results may differ from a plain program's by a relative error of at most 0.014.
Values may be sent and summed in bfloat16 or wider, within the bound.
No kernel may reach another device: no remote copies, remote signals or barrier semaphores. Data moves between devices by JAX's collectives and lax.ppermute only.
A program may use at most 64 MiB of HBM per device.

v0:
```python
import jax
import jax.numpy as jnp
from jax import lax
from jax.sharding import Mesh
from jax.sharding import PartitionSpec as P

EP = ("ep_0", "ep_1", "ep_2")


def cut_along(x, dim, size):
    shape = x.shape
    parts = x.reshape(*shape[:dim], size, shape[dim] // size, *shape[dim + 1 :])
    return jnp.moveaxis(parts, dim, 0)


def sum_at_owner(x, axis, dim):
    size = lax.axis_size(axis)
    parts = lax.all_to_all(cut_along(x, dim, size), axis, 0, 0, tiled=True)
    return jnp.sum(parts.astype(jnp.float32), axis=0)


def from_everyone(x, axis):
    copies = jnp.broadcast_to(x, (lax.axis_size(axis), *x.shape))
    return lax.all_to_all(copies, axis, split_axis=0, concat_axis=0, tiled=True)


def of_everyone(x, axis):
    return from_everyone(x, axis).astype(jnp.float32).sum(axis=0)


def laid_out(parts, dim):
    shape = list(parts.shape[1:])
    shape[dim] *= parts.shape[0]
    return jnp.moveaxis(parts, 0, dim).reshape(shape)


def collect(x, axis, dim):
    return laid_out(from_everyone(x, axis), dim)


def grouped_exchange(x, axis, split_dim, concat_dim, work, item_dim, out_dim):
    items = jax.tree.leaves(x)[0].shape[item_dim]
    count = 2 if items % 2 == 0 else 1
    finished = []
    for k in range(count):
        group = jax.tree.map(
            lambda a: lax.slice_in_dim(
                a, k * (items // count), (k + 1) * (items // count), axis=item_dim
            ),
            x,
        )
        finished.append(
            work(
                lax.all_to_all(
                    group, axis, split_axis=split_dim, concat_axis=concat_dim, tiled=True
                )
            )
        )
    return jax.tree.map(lambda *parts: jnp.concatenate(parts, axis=out_dim), *finished)


def sent_together(arrays, axis, dim, along):
    widths = [a.shape[along] for a in arrays]
    both = jnp.concatenate(arrays, axis=along)
    out = lax.all_gather(both, axis, axis=dim, tiled=True)
    return tuple(jnp.split(out, [sum(widths[:k]) for k in range(1, len(widths))], axis=along))


def gather_axes(x, axes, dim):
    for axis in reversed(axes):
        x = lax.all_gather(x, axis, axis=dim, tiled=True)
    return x


def rms_scale(values, gain):
    wide = values.astype(jnp.float32)
    return wide * lax.rsqrt(jnp.mean(wide * wide, axis=-1, keepdims=True) + 1e-06) * gain


def stick_read(queries, lengths, head_bias, key_cache, value_cache):
    seq_count, local_kv, head_dim, cache_len = key_cache.shape
    group_size = head_bias.shape[0] // local_kv
    grouped = queries.reshape(seq_count, local_kv, group_size, head_dim)
    head_shift = head_bias.reshape(1, local_kv, group_size, 1)
    span_len = min(512, cache_len)
    block_count = (jnp.max(lengths) + span_len - 1) // span_len
    span_index = lax.iota(jnp.int32, span_len)
    after_mask = (span_index[:, None] > span_index[None, :]).astype(jnp.float32)

    def visit(visit_index, carry):
        totals, log_later = carry
        first = (block_count - 1 - visit_index) * span_len
        key_block = lax.dynamic_slice_in_dim(key_cache, first, span_len, 3)
        value_block = lax.dynamic_slice_in_dim(value_cache, first, span_len, 3)
        scores = (
            jnp.einsum("skgd,skdc->skgc", grouped, key_block, preferred_element_type=jnp.float32)
            * head_dim ** (-0.5)
            + head_shift
        )
        positions = first + span_index
        visible = (positions[None, :] < lengths[:, None])[:, None, None, :]
        log_keep = jnp.where(visible, jax.nn.log_sigmoid(-scores), 0.0)
        log_after = jnp.einsum("skgj,jc->skgc", log_keep, after_mask) + log_later[..., None]
        weights = jnp.where(visible, jnp.exp(jax.nn.log_sigmoid(scores) + log_after), 0.0).astype(
            jnp.bfloat16
        )
        totals = totals + jnp.einsum(
            "skgc,skdc->skgd", weights, value_block, preferred_element_type=jnp.float32
        )
        return (totals, log_later + jnp.sum(log_keep, axis=3))

    start_totals = jnp.zeros((seq_count, local_kv, group_size, head_dim), jnp.float32)
    start_later = jnp.zeros((seq_count, local_kv, group_size), jnp.float32)
    totals, unused_later = lax.fori_loop(0, block_count, visit, (start_totals, start_later))
    return totals.reshape(seq_count, -1).astype(jnp.bfloat16)


def expert_math(inputs, w_expert_gate, w_expert_up, w_expert_down):
    gate_rows = jnp.einsum(
        "njcd,jdf->njcf", inputs, w_expert_gate, preferred_element_type=jnp.float32
    )
    up_rows = jnp.einsum("njcd,jdf->njcf", inputs, w_expert_up, preferred_element_type=jnp.float32)
    hidden = (jax.nn.silu(gate_rows) * up_rows).astype(jnp.bfloat16)
    partial_value = jnp.einsum(
        "njcf,jfd->njcd", hidden, w_expert_down, preferred_element_type=jnp.float32
    ).astype(jnp.bfloat16)
    return sum_at_owner(partial_value, "tp", 3).astype(jnp.bfloat16)


def shards(
    tokens,
    lengths,
    attn_gain,
    w_query,
    w_key,
    w_value,
    head_bias,
    key_cache,
    value_cache,
    w_attn_out,
    ffn_gain,
    w_router,
    routes,
    w_dense_gate,
    w_dense_up,
    w_dense_down,
    dense_mix,
    w_expert_gate,
    w_expert_up,
    w_expert_down,
):
    seq_count, model_width = tokens.shape
    normed = rms_scale(tokens, attn_gain).astype(jnp.bfloat16)
    new_keys = jnp.dot(normed, w_key, preferred_element_type=jnp.float32).astype(jnp.bfloat16)
    new_values = jnp.dot(normed, w_value, preferred_element_type=jnp.float32).astype(jnp.bfloat16)
    queries = jnp.dot(normed, w_query, preferred_element_type=jnp.float32).astype(jnp.bfloat16)
    heads_out = stick_read(queries, lengths, head_bias, key_cache, value_cache)
    attn_partial = jnp.dot(heads_out, w_attn_out, preferred_element_type=jnp.float32).astype(
        jnp.bfloat16
    )
    attn = of_everyone(attn_partial, "tp").astype(jnp.float32)
    residual = (tokens.astype(jnp.float32) + attn).astype(jnp.bfloat16)
    normed2 = rms_scale(residual, ffn_gain).astype(jnp.bfloat16)
    expert_total = w_router.shape[1]
    top_count = routes.shape[1]
    probs = jax.nn.sigmoid(jnp.dot(normed2, w_router, preferred_element_type=jnp.float32))
    hits = routes[:, :, None] == lax.iota(jnp.int32, expert_total)[None, None, :]
    picked = jnp.sum(jnp.where(hits, probs[:, None, :], 0.0), axis=-1)
    gates = picked / jnp.sum(picked, axis=-1, keepdims=True) * 2.5
    capacity = max(2, 2 * seq_count * top_count // expert_total)
    slot_total = expert_total * capacity
    flat_routes = routes.reshape(-1)
    route_count = flat_routes.shape[0]
    matching = flat_routes[:, None] == flat_routes[None, :]
    earlier = lax.iota(jnp.int32, route_count)[:, None] > lax.iota(jnp.int32, route_count)[None, :]
    slot_rank = jnp.sum(jnp.logical_and(matching, earlier).astype(jnp.int32), axis=1)
    target = flat_routes * capacity + slot_rank
    one_hot = (target[:, None] == lax.iota(jnp.int32, slot_total)[None, :]).astype(jnp.bfloat16)
    dispatch = jnp.sum(one_hot.reshape(seq_count, top_count, slot_total), axis=1)
    send_rows = jnp.einsum(
        "sr,sd->rd", dispatch, normed2, preferred_element_type=jnp.float32
    ).astype(jnp.bfloat16)
    send_rows = send_rows.reshape(expert_total, capacity, model_width)
    local_experts = w_expert_gate.shape[0]
    core_count = lax.axis_size("tp")
    half_cap = capacity // core_count
    own_slots = lax.dynamic_slice_in_dim(send_rows, lax.axis_index("tp") * half_cap, half_cap, 1)

    def run_halves(received):
        source_count = received.shape[0] // local_experts
        item_count = received.shape[1]
        both = collect(received, "tp", 0)
        inputs = both.reshape(core_count * source_count, local_experts, item_count, model_width)
        summed = expert_math(inputs, w_expert_gate, w_expert_up, w_expert_down)
        summed = summed.reshape(
            core_count, source_count * local_experts, item_count, summed.shape[3]
        )
        return lax.all_to_all(summed, EP, split_axis=1, concat_axis=1, tiled=True)

    returned = grouped_exchange(own_slots, EP, 0, 0, run_halves, 1, 2)
    half_width = returned.shape[3]
    split_target = (
        slot_rank // half_cap * (expert_total * half_cap)
        + flat_routes * half_cap
        + slot_rank % half_cap
    )
    route_rows = returned.reshape(-1, half_width)[split_target]
    route_rows = route_rows.reshape(seq_count, top_count, half_width)
    routed = jnp.sum(gates[:, :, None] * route_rows.astype(jnp.float32), axis=1)
    portions = sent_together((w_dense_gate, w_dense_up), EP, 0, 1)
    gate_sum = jnp.dot(normed2, portions[0], preferred_element_type=jnp.float32)
    up_sum = jnp.dot(normed2, portions[1], preferred_element_type=jnp.float32)
    dense_hidden = (jax.nn.silu(gate_sum) * up_sum).astype(jnp.bfloat16)
    dense_partial = jnp.dot(
        dense_hidden, gather_axes(w_dense_down, EP, 1), preferred_element_type=jnp.float32
    ).astype(jnp.bfloat16)
    dense = sum_at_owner(dense_partial, "tp", 1)
    mix_gate = jax.nn.sigmoid(jnp.sum(normed2.astype(jnp.float32) * dense_mix, axis=-1))
    offset = lax.axis_index("tp") * half_width
    residual_half = lax.dynamic_slice_in_dim(residual, offset, half_width, 1)
    layer_out = (residual_half.astype(jnp.float32) + mix_gate[:, None] * dense + routed).astype(
        jnp.bfloat16
    )
    return (layer_out, new_keys, new_values)


def solution(mesh):
    finer = Mesh(mesh.devices.reshape(8, 4, 4, mesh.shape["tp"]), ("ep_0", "ep_1", "ep_2", "tp"))
    placed = (
        P(EP, None),
        P(EP),
        P(),
        P(None, "tp"),
        P(None, "tp"),
        P(None, "tp"),
        P("tp"),
        P(EP, "tp", None, None),
        P(EP, "tp", None, None),
        P("tp", None),
        P(),
        P(),
        P(EP, None),
        P(EP, "tp"),
        P(EP, "tp"),
        P("tp", EP),
        P(),
        P(EP, None, "tp"),
        P(EP, None, "tp"),
        P(EP, "tp", None),
    )
    return jax.shard_map(
        shards,
        mesh=finer,
        in_specs=placed,
        out_specs=(P(EP, "tp"), P(EP, "tp"), P(EP, "tp")),
        check_vma=False,
    )
```

profile of v0, /device:TPU:2, one launch (start us, length us, event | category | flops | bytes accessed | tf_op | source)
XLA Modules:
  0.0 184.0 jit_solution(10105115625662482061)
XLA Ops:
  7.2 1.5 pad_maximum_fusion
  8.7 1.3 reduce_max.9
  10.7 1.0 fusion.68
  11.7 2.1 %convolution_convert_fusion.4 = bf16[16,512]{1,0:T(8,128)(2,1)S(1)} fusion(bf16[2048,512]{1,0:T(8,128)(2,1)} %param.25, bf16[16,2048]{1,0:T(8,128)(2,1)} %param.22, f32[2048]{0:T(1024)} %param.24, f32[16]{0:T(128)S(1)} %add_rsqrt_fusion.1), kind=kOutput, calls=%fused_computation.53 | convolution fusion | flops 33693696 | bytes 2187328 | tf_op jit(solution)/shard_map/dot_general | solution.py:156
  13.9 7.6 %while.15 = (s32[]{:T(128)}, f32[16,1,8,64]{3,2,0,1:T(8,128)S(1)}, f32[16,1,8]{0,2,1:T(8,128)S(1)}, s32[]{:T(128)}, s32[]{:T(128)}, /*index=5*/s32[16]{0:T(128)S...) while((s32[]{:T(128)}, f32[16,1,8,64]{3,2,0,1:T(8,128)S(1)}, ...), condition=%wide.region_4.5_spmd.clone, body=%wide.region_2.4_spmd.clone.sunk | while | flops 86458888 | bytes 3047731 | solution.py:114
  14.0 1.6 fusion.112
  15.7 1.9 %fusion.113 = f32[16,1,8,64]{3,2,0,1:T(8,128)S(1)} fusion(f32[16,1,8,64]{3,2,0,1:T(8,128)S(1)} %get-tuple-element.330, bf16[16,1,64,1024]{3,2,0,1:T(8,128)(2,1)} %get-tuple-element.352, s32[]{:T(128)S(6)} %select_n.127, f32[16,8,512]{2,1,0:T(8,128)S(1)} %get-tuple-element.313, f32[16,8]{1,0:T(8,128)S(1)} %copy.97, ...), kind=kOutput, calls=%fused_computation.13.clone.1 | convolution fusion | flops 77340672 | bytes 1695748 | tf_op jit(solution)/shard_map/while/body/skgc,skdc->skgd/dot_general | solution.py:107
  17.8 1.6 fusion.112
  19.5 1.9 %fusion.113 = f32[16,1,8,64]{3,2,0,1:T(8,128)S(1)} fusion(f32[16,1,8,64]{3,2,0,1:T(8,128)S(1)} %get-tuple-element.330, bf16[16,1,64,1024]{3,2,0,1:T(8,128)(2,1)} %get-tuple-element.352, s32[]{:T(128)S(6)} %select_n.127, f32[16,8,512]{2,1,0:T(8,128)S(1)} %get-tuple-element.313, f32[16,8]{1,0:T(8,128)S(1)} %copy.97, ...), kind=kOutput, calls=%fused_computation.13.clone.1 | convolution fusion | flops 77340672 | bytes 1695748 | tf_op jit(solution)/shard_map/while/body/skgc,skdc->skgd/dot_general | solution.py:107
  22.7 3.4 %all-to-all-start = ((bf16[2,16,2048]{2,1,0:T(8,128)(2,1)}), bf16[2,16,2048]{2,1,0:T(8,128)(2,1)S(1)}, u32[]{:S(2)}, u32[]{:S(2)}) async-start(bf16[2,16,2048]{2,1,0:T(8,128)(2,1)} %broadcast_in_dim.40), calls=%async_computation | async-start | bytes 262144 | tf_op jit(solution)/shard_map/all_to_all | solution.py:24
  27.7 1.5 convolution_convert_fusion.1
  29.2 1.7 reshape.252
  30.9 2.1 %constant_dynamic-slice_fusion = bf16[128,1,2048]{2,1,0:T(2,128)(2,1)} fusion(bf16[128,2,2048]{2,1,0:T(2,128)(2,1)S(1)} %reshape.252, s32[]{:T(128)S(6)} %select_n.73), kind=kLoop, calls=%fused_computation.119 | loop fusion | bytes 1048580 | tf_op jit(solution)/shard_map/dynamic_slice | solution.py:187
  33.5 4.8 %reduce.8 = bf16[128,2048]{1,0:T(8,128)(2,1)S(1)} reduce(bf16[128,1,2048]{2,1,0:T(2,128)(2,1)} %constant_dynamic-slice_fusion, bf16[]{:T(256)} %broadcast.211), dimensions={1}, to_apply=%constant_dynamic-slice_fusion.reduce_sub_computation | reduce | bytes 1048578 | tf_op jit(solution)/shard_map/dynamic_slice | solution.py:187
  38.3 1.2 reshape.275
  39.5 15.7 %all-to-all-start.2 = ((bf16[128,2,1024]{2,1,0:T(2,128)(2,1)}), bf16[128,2,1024]{2,1,0:T(2,128)(2,1)}, u32[]{:S(2)}, u32[]{:S(2)}) async-start(bf16[128,2,1024]{2,1,0:T(2,128)(2,1)} %reshape.275), calls=%async_computation.2 | async-start | bytes 1048576 | tf_op jit(solution)/shard_map/all_to_all | solution.py:54
  55.3 12.1 %all_gather.13 = bf16[256,64]{0,1:T(8,128)(2,1)S(1)} all-gather(bf16[256,16]{0,1:T(8,128)(2,1)S(1)} %copy-done.8), channel_id=1, replica_groups=mesh['ep_0'=8,'ep_1'=4,'ep_2'=4,'tp'=2] {'ep_2'}, dimensions={1}, use_global_device_ids=true | all-gather | bytes 40960 | tf_op jit(solution)/shard_map/all_gather | solution.py:71
  67.3 13.1 %all_gather.14 = bf16[256,256]{0,1:T(8,128)(2,1)} all-gather(bf16[256,64]{0,1:T(8,128)(2,1)S(1)} %all_gather.13), channel_id=1, replica_groups=mesh['ep_0'=8,'ep_1'=4,'ep_2'=4,'tp'=2] {'ep_1'}, dimensions={1}, use_global_device_ids=true | all-gather | bytes 163840 | tf_op jit(solution)/shard_map/all_gather | solution.py:71
  81.6 3.6 %reshape.276 = bf16[128,1,2048]{2,1,0:T(2,128)(2,1)S(1)} reshape(bf16[128,2,1024]{2,1,0:T(2,128)(2,1)} %all-to-all-done.2) | data formatting | bytes 1048576
  85.7 4.7 %all_to_all.33 = bf16[2,128,1,2048]{3,1,2,0:T(8,128)(2,1)S(1)} all-to-all(bf16[2,128,1,2048]{3,1,2,0:T(8,128)(2,1)S(1)} %broadcast_in_dim.43), channel_id=1, replica_groups=mesh['ep_0'=8,'ep_1'=4,'ep_2'=4,'tp'=2] {'tp'}, dimensions={0} | all-to-all | bytes 2097152 | tf_op jit(solution)/shard_map/all_to_all | solution.py:24
  90.8 3.8 %convolution_convert_fusion = bf16[256,2048]{1,0:T(8,128)(2,1)} fusion(bf16[1,256,2048]{2,1,0:T(8,128)(2,1)} %param.41, bf16[256,2048]{1,0:T(8,128)(2,1)S(1)} %bitcast.128, bf16[1,2048,256]{2,1,0:T(8,128)(2,1)} %param.40, f32[256,1,1,256]{3,0,2,1:T(8,128)S(1)} %convolution_bitcast_fusion.1), kind=kOutput, calls=%fused_computation.44 | convolution fusion | flops 537788416 | bytes 4456448 | tf_op jit(solution)/shard_map/njcf,jfd->njcd/dot_general | solution.py:124
  94.6 1.3 copy.92
  95.9 4.6 %all_to_all.34 = bf16[2,256,1,1,1024]{4,1,3,2,0:T(8,128)(2,1)S(1)} all-to-all(bf16[2,256,1,1,1024]{4,1,3,2,0:T(8,128)(2,1)S(1)} %bitcast.129), channel_id=1, replica_groups=mesh['ep_0'=8,'ep_1'=4,'ep_2'=4,'tp'=2] {'tp'}, dimensions={0} | all-to-all | bytes 2097152 | tf_op jit(solution)/shard_map/all_to_all | solution.py:18
  100.6 1.2 reduce_sum.128
  101.7 2.4 %copy.83 = bf16[2,128,1,1024]{3,0,2,1:T(2,128)(2,1)} copy(bf16[2,128,1,1024]{3,1,0,2:T(8,128)(2,1)} %bitcast.131) | data formatting | bytes 1048576 | tf_op jit(solution)/shard_map/reshape | solution.py:195
  104.1 12.8 %all-to-all-start.5 = ((bf16[2,128,1,1024]{3,0,2,1:T(2,128)(2,1)}), bf16[2,128,1,1024]{3,0,2,1:T(2,128)(2,1)S(1)}, u32[]{:S(2)}, u32[]{:S(2)}) async-start(bf16[2,128,1,1024]{3,0,2,1:T(2,128)(2,1)} %copy.83), calls=%async_computation.5 | async-start | bytes 1048576 | tf_op jit(solution)/shard_map/all_to_all | solution.py:198
  117.2 0.8 convolution_convert_fusion.6
  118.9 19.9 %all-to-all-done.5 = bf16[2,128,1,1024]{3,0,2,1:T(2,128)(2,1)S(1)} async-done(((bf16[2,128,1,1024]{3,0,2,1:T(2,128)(2,1)}), bf16[2,128,1,1024]{3,0,2,1:T(2,128)(2,1)S(1)}, u32[]{:S(2)}, u32[]{:S(2)}) %all-to-all-start.5) | async-done | bytes 524320 | tf_op jit(solution)/shard_map/all_to_all | solution.py:198
  140.1 1.5 fusion.53
  141.6 28.6 %all-gather.5.cloned.1.call-done = bf16[256,2048]{0,1:T(8,128)(2,1)} async-done(((bf16[256,256]{0,1:T(8,128)(2,1)}), bf16[256,2048]{0,1:T(8,128)(2,1)}) %all-gather.5.cloned.1.call-update) | async-done | bytes 1048592 | tf_op jit(solution)/shard_map/all_gather | solution.py:71
  170.2 2.4 %convolution_convert_fusion.2 = bf16[16,2048]{1,0:T(8,128)(2,1)S(1)} fusion(bf16[256,2048]{0,1:T(8,128)(2,1)} %all-gather.5.cloned.1.call-done, bf16[2048,512]{1,0:T(8,128)(2,1)} %all-gather.3.cloned.1.call-done, f32[16,256]{1,0:T(8,128)S(1)} %fusion.53, bf16[16,2048]{1,0:T(8,128)(2,1)S(1)} %get-tuple-element.246, f32[2048]{0:T(1024)S(1)} %copy-done.4, ...), kind=kOutput, calls=%fused_computation.46 | convolution fusion | flops 33742848 | bytes 2252864 | tf_op jit(solution)/shard_map/dot_general | solution.py:214
  172.6 3.8 %all_to_all.35 = bf16[2,16,1024]{2,1,0:T(8,128)(2,1)S(1)} all-to-all(bf16[2,16,1024]{2,1,0:T(8,128)(2,1)S(1)} %bitcast.135), channel_id=1, replica_groups=mesh['ep_0'=8,'ep_1'=4,'ep_2'=4,'tp'=2] {'tp'}, dimensions={0} | all-to-all | bytes 131072 | tf_op jit(solution)/shard_map/all_to_all | solution.py:18
  (96 shorter events, 9.1 us)
Async XLA Ops:
  7.2 14.5 %copy-start = (bf16[512,2048]{1,0:T(8,128)(2,1)S(1)}, bf16[512,2048]{1,0:T(8,128)(2,1)}, u32[]{:S(2)}) copy-start(bf16[512,2048]{1,0:T(8,128)(2,1)} %param.31) | copy-start | bytes 6291460
  7.2 6.7 %copy-start.6 = (s32[16]{0:T(128)S(1)}, s32[16]{0:T(128)}, u32[]{:S(2)}) copy-start(s32[16]{0:T(128)} %param.23) | copy-start | bytes 196
  7.2 6.7 %copy-start.19 = (f32[8]{0:T(128)S(1)}, f32[8]{0:T(128)}, u32[]{:S(2)}) copy-start(f32[8]{0:T(128)} %param.28) | copy-start | bytes 100
  7.2 132.9 %all-gather.3.cloned.1.call-start = ((), (), s32[]{:S(2)}) async-start(), calls=%async_computation.6 | async-start | bytes 2113536 | tf_op jit(solution)/shard_map/all_gather | solution.py:65
  11.7 2.2 %copy-start.12 = (f32[16]{0:T(128)}, f32[16]{0:T(128)S(1)}, u32[]{:S(2)}) copy-start(f32[16]{0:T(128)S(1)} %add_rsqrt_fusion.1) | copy-start | bytes 196
  21.5 4.6 %copy-start.5 = (s32[16,6]{0,1:T(8,128)S(1)}, s32[16,6]{0,1:T(8,128)}, u32[]{:S(2)}) copy-start(s32[16,6]{0,1:T(8,128)} %param.34) | copy-start | bytes 1156
  21.5 6.1 %copy-start.2 = (bf16[16,2048]{1,0:T(8,128)(2,1)S(1)}, bf16[16,2048]{1,0:T(8,128)(2,1)}, u32[]{:S(2)}) copy-start(bf16[16,2048]{1,0:T(8,128)(2,1)} %param.22) | copy-start | bytes 196612
  21.5 6.2 %copy-start.4 = (f32[2048]{0:T(1024)S(1)}, f32[2048]{0:T(1024)}, u32[]{:S(2)}) copy-start(f32[2048]{0:T(1024)} %param.32) | copy-start | bytes 24580
  22.7 4.8 %all-to-all-start = ((bf16[2,16,2048]{2,1,0:T(8,128)(2,1)}), bf16[2,16,2048]{2,1,0:T(8,128)(2,1)S(1)}, u32[]{:S(2)}, u32[]{:S(2)}) async-start(bf16[2,16,2048]{2,1,0:T(8,128)(2,1)} %broadcast_in_dim.40), calls=%async_computation | async-start | bytes 262144 | tf_op jit(solution)/shard_map/all_to_all | solution.py:24
  26.5 0.5 copy-start.14
  27.7 53.4 %copy-start.10 = (f32[16]{0:T(128)}, f32[16]{0:T(128)S(1)}, u32[]{:S(2)}) copy-start(f32[16]{0:T(128)S(1)} %add_rsqrt_fusion) | copy-start | bytes 196
  33.0 22.2 %copy-start.8 = (bf16[256,16]{0,1:T(8,128)(2,1)S(1)}, bf16[256,16]{0,1:T(8,128)(2,1)}, u32[]{:S(2)}) copy-start(bf16[256,16]{0,1:T(8,128)(2,1)} %param.37) | copy-start | bytes 24580
  33.0 48.1 %copy-start.3 = (bf16[2048,128]{1,0:T(8,128)(2,1)S(1)}, bf16[2048,128]{1,0:T(8,128)(2,1)}, u32[]{:S(2)}) copy-start(bf16[2048,128]{1,0:T(8,128)(2,1)} %param.33) | copy-start | bytes 1572868
  39.5 42.2 %all-to-all-start.2 = ((bf16[128,2,1024]{2,1,0:T(2,128)(2,1)}), bf16[128,2,1024]{2,1,0:T(2,128)(2,1)}, u32[]{:S(2)}, u32[]{:S(2)}) async-start(bf16[128,2,1024]{2,1,0:T(2,128)(2,1)} %reshape.275), calls=%async_computation.2 | async-start | bytes 1048576 | tf_op jit(solution)/shard_map/all_to_all | solution.py:54
  55.2 115.0 %all-gather.5.cloned.1.call-start = ((), (), s32[]{:S(2)}) async-start(), calls=%async_computation.7 | async-start | bytes 1179648 | tf_op jit(solution)/shard_map/all_gather | solution.py:71
  85.5 4.8 %copy-start.1 = (bf16[1,2048,256]{2,1,0:T(8,128)(2,1)S(1)}, bf16[1,2048,256]{2,1,0:T(8,128)(2,1)}, u32[]{:S(2)}) copy-start(bf16[1,2048,256]{2,1,0:T(8,128)(2,1)} %param.39) | copy-start | bytes 3145732
  100.5 16.4 %copy-start.15 = (s32[96]{0:T(128)S(1)}, s32[96]{0:T(128)}, u32[]{:S(2)}) copy-start(s32[96]{0:T(128)} %copy-done.14) | copy-start | bytes 1156
  100.5 16.4 %copy-start.16 = (s32[96,1]{0,1:T(1,128)S(1)}, s32[96,1]{0,1:T(1,128)}, u32[]{:S(2)}) copy-start(s32[96,1]{0,1:T(1,128)} %reshape.261) | copy-start | bytes 1156
  100.5 16.5 %copy-start.9 = (f32[2048]{0:T(1024)S(1)}, f32[2048]{0:T(1024)}, u32[]{:S(2)}) copy-start(f32[2048]{0:T(1024)} %param.38) | copy-start | bytes 24580
  100.5 16.5 %copy-start.11 = (f32[16]{0:T(128)S(1)}, f32[16]{0:T(128)}, u32[]{:S(2)}) copy-start(f32[16]{0:T(128)} %copy-done.10) | copy-start | bytes 196
  100.5 16.7 %copy-start.7 = (f32[2048]{0:T(1024)S(1)}, f32[2048]{0:T(1024)}, u32[]{:S(2)}) copy-start(f32[2048]{0:T(1024)} %param.24) | copy-start | bytes 24580
  100.5 16.7 %copy-start.13 = (f32[16]{0:T(128)S(1)}, f32[16]{0:T(128)}, u32[]{:S(2)}) copy-start(f32[16]{0:T(128)} %copy-done.12) | copy-start | bytes 196
  101.7 15.5 %copy-start.17 = (bf16[2048,64]{0,1:T(8,128)(2,1)S(1)}, bf16[2048,64]{0,1:T(8,128)(2,1)}, u32[]{:S(2)}) copy-start(bf16[2048,64]{0,1:T(8,128)(2,1)} %param.26) | copy-start | bytes 786436
  101.7 16.4 %copy-start.18 = (bf16[2048,64]{0,1:T(8,128)(2,1)S(1)}, bf16[2048,64]{0,1:T(8,128)(2,1)}, u32[]{:S(2)}) copy-start(bf16[2048,64]{0,1:T(8,128)(2,1)} %param.27) | copy-start | bytes 786436
  104.1 34.7 %all-to-all-start.5 = ((bf16[2,128,1,1024]{3,0,2,1:T(2,128)(2,1)}), bf16[2,128,1,1024]{3,0,2,1:T(2,128)(2,1)S(1)}, u32[]{:S(2)}, u32[]{:S(2)}) async-start(bf16[2,128,1,1024]{3,0,2,1:T(2,128)(2,1)} %copy.83), calls=%async_computation.5 | async-start | bytes 1048576 | tf_op jit(solution)/shard_map/all_to_all | solution.py:198
Sparse Core Ops, SparseCore 0:
  12.2 119.9 all-gather.2
  134.0 36.1 all-gather.4
where the time goes:
time: 186 us; the launch traced here: 184 us
  waiting for transfers between devices  48.9 us (26%)
  blocking collectives  38.3 us (21%)
  starting transfers between devices  32 us (17%)
  matrix products  21 us (11%)
  local copies, waits for them, and re-layouts  17 us (9%)
  between operations  15.1 us (8%)
  other arithmetic  11.7 us (6%)
    all_gather x1, waiting for transfers between devices, gather_axes(): x = lax.all_gather(x, axis, axis=dim, tiled=True)  28.6 us
    all_gather x2, blocking collectives, gather_axes(): x = lax.all_gather(x, axis, axis=dim, tiled=True)  25.2 us
    all_to_all x1, waiting for transfers between devices, run_halves(): return lax.all_to_all(summed, EP, split_axis=1, concat_axis=1, tiled=True)  19.9 us
    all_to_all x1, starting transfers between devices, grouped_exchange(): lax.all_to_all(group, axis, split_axis=split_dim, concat_axis=concat_dim,...  15.7 us
    all_to_all x1, starting transfers between devices, run_halves(): return lax.all_to_all(summed, EP, split_axis=1, concat_axis=1, tiled=True)  12.8 us
    all_to_all x2, blocking collectives, sum_at_owner(): parts = lax.all_to_all(cut_along(x, dim, size), axis, 0, 0, tiled=True)  8.37 us
    unnamed x44, local copies, waits for them, and re-layouts  5.78 us
    dynamic_slice x1, other arithmetic, shards(): lax.dynamic_slice_in_dim(send_rows, lax.axis_index('tp') * half_cap, half...  4.77 us
  transfers between devices with their start and end apart: 5, of which 3 were waited for; matrix products, arithmetic and copies ran while one was open for 24% of the time, Pallas kernels for 0%

commit v1 on v0

v1 whole, which is shorter than its diff:
```python
import jax
import jax.numpy as jnp
from jax import lax
from jax.experimental import pallas as pl
from jax.experimental.pallas import tpu as pltpu
from jax.sharding import Mesh
from jax.sharding import PartitionSpec as P

EP = ("ep_0", "ep_1", "ep_2")
LINE = "ep_0"
PLANE = ("ep_1", "ep_2")
SWAP = ((0, 1), (1, 0))
F32 = jnp.float32
BF16 = jnp.bfloat16

GATE_HI, GATE_LO, MIX_HI, MIX_LO, DENSE = 8, 16, 24, 25, 32


def rms_scale(values, gain):
    wide = values.astype(F32)
    return wide * lax.rsqrt(jnp.mean(wide * wide, axis=-1, keepdims=True) + 1e-06) * gain


def stick_read(queries, lengths, head_bias, key_cache, value_cache):
    seq_count, local_kv, head_dim, cache_len = key_cache.shape
    group_size = head_bias.shape[0] // local_kv
    grouped = queries.reshape(seq_count, local_kv, group_size, head_dim)
    head_shift = head_bias.reshape(1, local_kv, group_size, 1)
    span_len = min(512, cache_len)
    block_count = (jnp.max(lengths) + span_len - 1) // span_len
    span_index = lax.iota(jnp.int32, span_len)
    after_mask = (span_index[:, None] > span_index[None, :]).astype(F32)

    def visit(visit_index, carry):
        totals, log_later = carry
        first = (block_count - 1 - visit_index) * span_len
        key_block = lax.dynamic_slice_in_dim(key_cache, first, span_len, 3)
        value_block = lax.dynamic_slice_in_dim(value_cache, first, span_len, 3)
        scores = (
            jnp.einsum("skgd,skdc->skgc", grouped, key_block, preferred_element_type=F32)
            * head_dim ** (-0.5)
            + head_shift
        )
        positions = first + span_index
        visible = (positions[None, :] < lengths[:, None])[:, None, None, :]
        log_keep = jnp.where(visible, jax.nn.log_sigmoid(-scores), 0.0)
        log_after = jnp.einsum("skgj,jc->skgc", log_keep, after_mask) + log_later[..., None]
        weights = jnp.where(visible, jnp.exp(jax.nn.log_sigmoid(scores) + log_after), 0.0).astype(
            BF16
        )
        totals = totals + jnp.einsum(
            "skgc,skdc->skgd", weights, value_block, preferred_element_type=F32
        )
        return (totals, log_later + jnp.sum(log_keep, axis=3))

    start_totals = jnp.zeros((seq_count, local_kv, group_size, head_dim), F32)
    start_later = jnp.zeros((seq_count, local_kv, group_size), F32)
    totals, unused_later = lax.fori_loop(0, block_count, visit, (start_totals, start_later))
    return totals.reshape(seq_count, -1).astype(BF16)


def call(kernel, out_shape, smem_count, inputs, limit=48):
    in_specs = [pl.BlockSpec(memory_space=pltpu.SMEM)] * smem_count
    in_specs += [pl.BlockSpec(memory_space=pltpu.VMEM)] * (len(inputs) - smem_count)
    return pl.pallas_call(
        kernel,
        out_shape=out_shape,
        in_specs=in_specs,
        out_specs=jax.tree.map(lambda _: pl.BlockSpec(memory_space=pltpu.VMEM), out_shape),
        compiler_params=pltpu.CompilerParams(vmem_limit_bytes=limit * 1024 * 1024),
    )(*inputs)


def rows_kernel(
    core_ref,
    tokens_ref,
    own_ref,
    other_ref,
    gain_ref,
    router_ref,
    routes_ref,
    gate_ref,
    up_ref,
    down_ref,
    mix_ref,
    send_ref,
    residual_ref,
):
    first_core = core_ref[0] == 0
    lines, seq_count, _ = send_ref.shape
    half = residual_ref.shape[1]
    attn = own_ref[...].astype(F32) + other_ref[...].astype(F32)
    residual = (tokens_ref[...].astype(F32) + attn).astype(BF16)
    normed = rms_scale(residual, gain_ref[...]).astype(BF16)
    residual_ref[...] = jnp.where(first_core, residual[:, :half], residual[:, half:])
    probs = jax.nn.sigmoid(jnp.dot(normed, router_ref[...], preferred_element_type=F32))
    mix = jax.nn.sigmoid(jnp.sum(normed.astype(F32) * mix_ref[...], axis=-1, keepdims=True))
    routes = routes_ref[...]
    lane = lax.broadcasted_iota(jnp.int32, probs.shape, 1)
    picked = [
        jnp.sum(jnp.where(lane == routes[:, k : k + 1], probs, 0.0), axis=-1, keepdims=True)
        for k in range(routes.shape[1])
    ]
    total = sum(picked[1:], picked[0])
    meta_lane = lax.broadcasted_iota(jnp.int32, (seq_count, 128), 1)
    meta = jnp.zeros((seq_count, 128), F32)

    def put(meta, at, value):
        return jnp.where(meta_lane == at, value, meta)

    for k, one in enumerate(picked):
        gate = one / total * 2.5
        high = gate.astype(BF16).astype(F32)
        meta = put(meta, k, routes[:, k : k + 1].astype(F32))
        meta = put(meta, GATE_HI + k, high)
        meta = put(meta, GATE_LO + k, gate - high)
    mix_high = mix.astype(BF16).astype(F32)
    meta = put(put(meta, MIX_HI, mix_high), MIX_LO, mix - mix_high)
    eye = (
        lax.broadcasted_iota(jnp.int32, (seq_count, seq_count), 0)
        == lax.broadcasted_iota(jnp.int32, (seq_count, seq_count), 1)
    ).astype(BF16)
    down = lax.dot_general(eye, down_ref[...], (((1,), (1,)), ((), ())), preferred_element_type=F32)
    parts = (gate_ref[...].astype(F32), up_ref[...].astype(F32), down)
    part = parts[0].shape[1] // lines
    row = jnp.where(first_core, normed[:, :half], normed[:, half:])
    for line in range(lines):
        block = meta
        at = line * part
        for n, values in enumerate(parts):
            tile = values[:, at // 128 * 128 : at // 128 * 128 + 128]
            to = DENSE + n * part
            moved = pltpu.roll(tile, (to - at % 128) % 128, 1)
            inside = jnp.logical_and(meta_lane >= to, meta_lane < to + part)
            block = jnp.where(inside, moved, block)
        send_ref[line, :, :half] = row
        send_ref[line, :, half:] = block.astype(BF16)


def slots_kernel(line_ref, got_ref, send_ref, combine_ref):
    lines, seq_count, width = got_ref.shape
    places, _, half = send_ref.shape
    token_total = lines * seq_count
    capacity = seq_count
    slot_total = places * capacity
    got = got_ref[...].reshape(token_total, width)
    meta = got[:, half:].astype(F32).T
    slot = lax.broadcasted_iota(jnp.int32, (slot_total, token_total), 0)
    token = lax.broadcasted_iota(jnp.int32, (slot_total, token_total), 1)
    expert = (line_ref[0] * places + slot // capacity).astype(F32)
    hit = jnp.zeros((slot_total, token_total), F32)
    gate = jnp.zeros((slot_total, token_total), F32)
    for k in range(6):
        same = meta[k : k + 1] == expert
        hit = jnp.where(same, 1.0, hit)
        gate = jnp.where(same, meta[GATE_HI + k : GATE_HI + k + 1] + meta[GATE_LO + k : GATE_LO + k + 1], gate)
    row = lax.broadcasted_iota(jnp.int32, (token_total, token_total), 0)
    column = lax.broadcasted_iota(jnp.int32, (token_total, token_total), 1)
    earlier = jnp.logical_and(row // seq_count == column // seq_count, row < column)
    rank = jnp.dot(hit.astype(BF16), earlier.astype(BF16), preferred_element_type=F32)
    per_source = capacity // lines
    here = jnp.logical_and(
        token // seq_count == slot % capacity // per_source,
        rank == (slot % per_source).astype(F32),
    )
    chosen = jnp.where(here, hit, 0.0)
    rows = jnp.dot(chosen.astype(BF16), got[:, :half], preferred_element_type=F32)
    send_ref[:, :capacity, :] = rows.astype(BF16).reshape(places, capacity, half)
    for line in range(lines):
        block = got_ref[line, :, half:]
        send_ref[:, capacity:, line * 128 : line * 128 + 128] = jnp.broadcast_to(
            block[None], (places, seq_count, 128)
        )
    weights = jnp.where(here, gate * hit, 0.0).T
    high = weights.astype(BF16)
    combine_ref[:, :slot_total] = high
    combine_ref[:, slot_total:] = (weights - high.astype(F32)).astype(BF16)


def experts_kernel(
    core_ref, own_ref, other_ref, line_own_ref, line_other_ref, gate_ref, up_ref, down_ref, keep_ref, send_ref
):
    core = core_ref[0]
    places, rows, half = own_ref.shape
    capacity = rows // 2
    slot_total = places * capacity
    lines, seq_count, _ = line_own_ref.shape
    token_total = lines * seq_count
    mine = pl.ds(pl.multiple_of(core * half, half), half)
    theirs = pl.ds(pl.multiple_of((1 - core) * half, half), half)
    x_own = own_ref[:, :capacity, :].reshape(slot_total, half)
    x_other = other_ref[:, :capacity, :].reshape(slot_total, half)

    def project(weight_ref):
        return jnp.dot(x_own, weight_ref[mine, :], preferred_element_type=F32) + jnp.dot(
            x_other, weight_ref[theirs, :], preferred_element_type=F32
        )

    hidden = (jax.nn.silu(project(gate_ref)) * project(up_ref)).astype(BF16)
    keep_ref[:slot_total, :] = jnp.dot(hidden, down_ref[:, mine], preferred_element_type=F32).astype(BF16)
    send_ref[:slot_total, :] = jnp.dot(hidden, down_ref[:, theirs], preferred_element_type=F32).astype(BF16)

    half_lines = lines // 2
    block = half // half_lines

    def dense_weights(line):
        at = pl.multiple_of(line * 128, 128)
        return own_ref[:, capacity:, pl.ds(at, 128)].reshape(block, 128)

    line_own = line_own_ref[:, :, :half].reshape(token_total, half)
    line_other = line_other_ref[:, :, :half].reshape(token_total, half)
    sums = jnp.zeros((token_total, 128), F32)
    for k in range(half_lines):
        at = slice(k * block, (k + 1) * block)
        sums += jnp.dot(line_own[:, at], dense_weights(core * half_lines + k), preferred_element_type=F32)
        sums += jnp.dot(line_other[:, at], dense_weights((1 - core) * half_lines + k), preferred_element_type=F32)
    lane = lax.broadcasted_iota(jnp.int32, sums.shape, 1)
    gate = pltpu.roll(sums, 64, 1)
    up = pltpu.roll(sums, 32, 1)
    dense = jnp.where(lane >= 96, jax.nn.silu(gate) * up, 0.0).astype(BF16)
    for k in range(half_lines):
        at = slice(k * block, (k + 1) * block)
        for target, side in ((keep_ref, core), (send_ref, 1 - core)):
            target[slot_total:, at] = lax.dot_general(
                dense,
                dense_weights(side * half_lines + k),
                (((1,), (1,)), ((), ())),
                preferred_element_type=F32,
            ).astype(BF16)


def combine_kernel(back_ref, combine_ref, line_ref, keep_ref, got_ref, send_ref):
    lines, seq_count, half = send_ref.shape
    token_total = lines * seq_count
    slot_total = back_ref.shape[0] * back_ref.shape[1]
    back = back_ref[...].reshape(slot_total, half)
    routed = jnp.dot(combine_ref[:, :slot_total], back, preferred_element_type=F32)
    routed += jnp.dot(combine_ref[:, slot_total:], back, preferred_element_type=F32)
    meta = line_ref[...].reshape(token_total, line_ref.shape[2])[:, half:].astype(F32)
    mix = meta[:, MIX_HI : MIX_HI + 1] + meta[:, MIX_LO : MIX_LO + 1]
    dense = keep_ref[slot_total:, :].astype(F32) + got_ref[slot_total:, :].astype(F32)
    send_ref[...] = (routed + mix * dense).astype(BF16).reshape(lines, seq_count, half)


def shards(
    tokens,
    lengths,
    attn_gain,
    w_query,
    w_key,
    w_value,
    head_bias,
    key_cache,
    value_cache,
    w_attn_out,
    ffn_gain,
    w_router,
    routes,
    w_dense_gate,
    w_dense_up,
    w_dense_down,
    dense_mix,
    w_expert_gate,
    w_expert_up,
    w_expert_down,
):
    seq_count, width = tokens.shape
    half = width // 2
    lines = lax.axis_size(LINE)
    places = lax.axis_size(PLANE)
    slot_total = places * seq_count
    token_total = lines * seq_count
    core = lax.axis_index("tp").astype(jnp.int32).reshape(1)
    line = lax.axis_index(LINE).astype(jnp.int32).reshape(1)
    normed = rms_scale(tokens, attn_gain).astype(BF16)
    new_keys = jnp.dot(normed, w_key, preferred_element_type=F32).astype(BF16)
    new_values = jnp.dot(normed, w_value, preferred_element_type=F32).astype(BF16)
    queries = jnp.dot(normed, w_query, preferred_element_type=F32).astype(BF16)
    heads_out = stick_read(queries, lengths, head_bias, key_cache, value_cache)
    attn_own = jnp.dot(heads_out, w_attn_out, preferred_element_type=F32).astype(BF16)
    attn_other = lax.ppermute(attn_own, "tp", SWAP)
    line_send, residual = call(
        rows_kernel,
        (
            jax.ShapeDtypeStruct((lines, seq_count, half + 128), BF16),
            jax.ShapeDtypeStruct((seq_count, half), BF16),
        ),
        1,
        (
            core,
            tokens,
            attn_own,
            attn_other,
            ffn_gain.reshape(1, width),
            w_router,
            routes,
            w_dense_gate,
            w_dense_up,
            w_dense_down,
            dense_mix.reshape(1, width),
        ),
    )
    line_own = lax.all_to_all(line_send, LINE, 0, 0, tiled=True)
    line_other = lax.ppermute(line_own, "tp", SWAP)
    slot_send, combine = call(
        slots_kernel,
        (
            jax.ShapeDtypeStruct((places, 2 * seq_count, half), BF16),
            jax.ShapeDtypeStruct((token_total, 2 * slot_total), BF16),
        ),
        1,
        (line, line_own),
    )
    slot_own = lax.all_to_all(slot_send, PLANE, 0, 0, tiled=True)
    slot_other = lax.ppermute(slot_own, "tp", SWAP)
    keep, send = call(
        experts_kernel,
        (jax.ShapeDtypeStruct((slot_total + token_total, half), BF16),) * 2,
        1,
        (
            core,
            slot_own,
            slot_other,
            line_own,
            line_other,
            w_expert_gate[0],
            w_expert_up[0],
            w_expert_down[0],
        ),
    )
    got = lax.ppermute(send, "tp", SWAP)
    results = (keep[:slot_total].astype(F32) + got[:slot_total].astype(F32)).astype(BF16)
    back = lax.all_to_all(results.reshape(places, seq_count, half), PLANE, 0, 0, tiled=True)
    partial = call(
        combine_kernel,
        jax.ShapeDtypeStruct((lines, seq_count, half), BF16),
        0,
        (back, combine, line_own, keep, got),
    )
    parts = lax.all_to_all(partial, LINE, 0, 0, tiled=True)
    layer_out = (residual.astype(F32) + jnp.sum(parts.astype(F32), axis=0)).astype(BF16)
    return (layer_out, new_keys, new_values)


def solution(mesh):
    finer = Mesh(mesh.devices.reshape(8, 4, 4, mesh.shape["tp"]), ("ep_0", "ep_1", "ep_2", "tp"))
    placed = (
        P(EP, None),
        P(EP),
        P(),
        P(None, "tp"),
        P(None, "tp"),
        P(None, "tp"),
        P("tp"),
        P(EP, "tp", None, None),
        P(EP, "tp", None, None),
        P("tp", None),
        P(),
        P(),
        P(EP, None),
        P(EP, "tp"),
        P(EP, "tp"),
        P("tp", EP),
        P(),
        P(EP, None, "tp"),
        P(EP, None, "tp"),
        P(EP, "tp", None),
    )
    return jax.shard_map(
        shards,
        mesh=finer,
        in_specs=placed,
        out_specs=(P(EP, "tp"), P(EP, "tp"), P(EP, "tp")),
        check_vma=False,
    )
```

time: 186 us -> 103 us (0.55)
  waiting for transfers between devices: 48.9 us -> 26 us
  starting transfers between devices: 32 us -> 16.4 us
  local copies, waits for them, and re-layouts: 17 us -> 2.45 us
  between operations: 15.1 us -> 1.54 us
  matrix products: 21 us -> 9.56 us
  other arithmetic: 11.7 us -> 3.36 us
  Pallas kernels: 0 us -> 5.17 us
    all_gather x2 -> x0, waiting for transfers between devices: 28.6 us -> none  [the longest x1 28.6 us: gather_axes(): x = lax.all_gather(x, axis, axis=dim, tiled=True)]
    all_gather x2 -> x0, blocking collectives: 25.2 us -> none  [gather_axes(): x = lax.all_gather(x, axis, axis=dim, tiled=True)]
    all_to_all x3 -> x2, blocking collectives: 13.1 us -> 37.4 us  [the longest x1 22.6 us: shards(): slot_own = lax.all_to_all(slot_send, PLANE, 0, 0, tiled=True)]
    all_to_all x3 -> x2, starting transfers between devices: 31.9 us -> 15.7 us  [the longest x1 12.3 us: shards(): line_own = lax.all_to_all(line_send, LINE, 0, 0, tiled=True)]
    dot_general x10 -> x4, matrix products: 14 us -> 6.03 us  [the longest x1 2.07 us: shards(): queries = jnp.dot(normed, w_query, preferred_element_type=F32).astype(BF16)]
    reshape x5 -> x0, local copies, waits for them, and re-layouts: 6.09 us -> none  [the longest x1 2.43 us: run_halves(): summed.reshape(core_count, source_count * local_experts, item_count, summ...]
    ppermute x0 -> x4, waiting for transfers between devices: none -> 5.67 us  [the longest x1 2.57 us: shards(): line_other = lax.ppermute(line_own, 'tp', SWAP)]
    pallas_call x0 -> x4, Pallas kernels: none -> 5.17 us  [call(): pl.pallas_call(kernel, out_shape=out_shape, in_specs=in_specs, out_specs=...]
  transfers between devices with their start and end apart: 5 -> 6, of which waited for: 3 -> 5; matrix products, arithmetic and copies ran while one was open for 24% -> 4% of each run, Pallas kernels for 0% -> 0%
where the time goes in v1:
time: 103 us; the launch traced here: 102 us
  blocking collectives  37.4 us (36%)
  waiting for transfers between devices  26 us (25%)
  starting transfers between devices  16.4 us (16%)
  matrix products  9.56 us (9%)
  Pallas kernels  5.17 us (5%)
  other arithmetic  3.36 us (3%)
  local copies, waits for them, and re-layouts  2.45 us (2%)
  between operations  1.54 us (1%)
    all_to_all x1, blocking collectives, shards(): slot_own = lax.all_to_all(slot_send, PLANE, 0, 0, tiled=True)  22.6 us
    all_to_all x1, blocking collectives, shards(): lax.all_to_all(results.reshape(places, seq_count, half), PLANE, 0, 0, til...  14.8 us
    all_to_all x1, waiting for transfers between devices, shards(): line_own = lax.all_to_all(line_send, LINE, 0, 0, tiled=True)  12.9 us
    all_to_all x1, starting transfers between devices, shards(): line_own = lax.all_to_all(line_send, LINE, 0, 0, tiled=True)  12.3 us
    all_to_all x1, waiting for transfers between devices, shards(): parts = lax.all_to_all(partial, LINE, 0, 0, tiled=True)  7.4 us
    pallas_call x4, Pallas kernels, call(): pl.pallas_call(kernel, out_shape=out_shape, in_specs=in_specs, out_specs=...  5.17 us
    all_to_all x1, starting transfers between devices, shards(): parts = lax.all_to_all(partial, LINE, 0, 0, tiled=True)  3.41 us
    ppermute x1, waiting for transfers between devices, shards(): line_other = lax.ppermute(line_own, 'tp', SWAP)  2.57 us
  transfers between devices with their start and end apart: 6, of which 5 were waited for; matrix products, arithmetic and copies ran while one was open for 4% of the time, Pallas kernels for 0%

profile of v1, /device:TPU:2, one launch (start us, length us, event | category | flops | bytes accessed | tf_op | source)
XLA Modules:
  0.0 101.9 jit_solution(3493136900283921456)
XLA Ops:
  0.7 1.4 %reduce_max.9 = s32[]{:T(128)} reduce(s32[16]{0:T(128)} %param.23, s32[]{:T(128)} %constant.63.clone.1), dimensions={0}, to_apply=%region_0.0 | reduce | flops 15 | bytes 72 | tf_op jit(solution)/shard_map/reduce_max | solution.py:30
  2.8 1.0 fusion.44
  3.8 2.1 %convolution_convert_fusion.1 = bf16[16,512]{1,0:T(8,128)(2,1)S(1)} fusion(bf16[2048,512]{1,0:T(8,128)(2,1)} %param.25, bf16[16,2048]{1,0:T(8,128)(2,1)} %tokens_ref.1, f32[2048]{0:T(1024)} %param.24, f32[16]{0:T(128)S(1)} %add_rsqrt_fusion), kind=kOutput, calls=%fused_computation.44 | convolution fusion | flops 33693696 | bytes 2187328 | tf_op jit(solution)/shard_map/dot_general | solution.py:278
  5.8 0.1 reshape.133
  6.0 3.8 %while.15 = (s32[]{:T(128)}, f32[16,1,8,64]{3,2,0,1:T(8,128)S(1)}, f32[16,1,8]{0,2,1:T(8,128)S(1)}, s32[]{:T(128)}, s32[]{:T(128)}, /*index=5*/s32[16]{0:T(128)S...) while((s32[]{:T(128)}, f32[16,1,8,64]{3,2,0,1:T(8,128)S(1)}, ...), condition=%wide.region_4.5_spmd.clone, body=%wide.region_2.4_spmd.clone.sunk | while | flops 86458888 | bytes 3047723 | solution.py:58
  6.1 1.6 %fusion.63 = (f32[16,8]{1,0:T(8,128)S(1)}, f32[16,8,512]{2,1,0:T(8,128)S(1)}) fusion(pred[16,512]{1,0:T(8,128)(4,1)S(1)} %broadcast_compare_fusion.2, f32[8]{0:T(128)S(1)} %bitcast.73, bf16[16,1,8,64]{3,2,0,1:T(8,128)(2,1)S(1)} %get-tuple-element.318, bf16[16,1,64,1024]{3,2,0,1:T(8,128)(2,1)} %get-tuple-element.317, s32[]{:T(128)S(6)} %select_n.86), kind=kOutput, calls=%fused_computation.34.clone.1 | convolution fusion | flops 9109376 | bytes 1335844 | tf_op jit(solution)/shard_map/while/body/skgd,skdc->skgc/dot_general | solution.py:40
  7.8 1.9 %fusion.64 = f32[16,1,8,64]{3,2,0,1:T(8,128)S(1)} fusion(f32[16,1,8,64]{3,2,0,1:T(8,128)S(1)} %get-tuple-element.298, bf16[16,1,64,1024]{3,2,0,1:T(8,128)(2,1)} %get-tuple-element.320, s32[]{:T(128)S(6)} %select_n.86, f32[16,8,512]{2,1,0:T(8,128)S(1)} %get-tuple-element.281, f32[16,8]{1,0:T(8,128)S(1)} %copy.36, ...), kind=kOutput, calls=%fused_computation.12.clone.1 | convolution fusion | flops 77340672 | bytes 1695748 | tf_op jit(solution)/shard_map/while/body/skgc,skdc->skgd/dot_general | solution.py:51
  9.9 0.1 convert_element_type.56
  10.0 0.4 convolution_convert_fusion.own_ref
  10.5 0.1 copy.33.down_ref
  10.6 0.1 copy.32.routes_ref
  10.7 0.9 collective-permute-done.other_ref
  11.7 1.0 %copy-done.3 = bf16[2048,128]{1,0:T(8,128)(2,1)S(1)} copy-done((bf16[2048,128]{1,0:T(8,128)(2,1)S(1)}, bf16[2048,128]{1,0:T(8,128)(2,1)}, u32[]{:S(2)}) %copy-start.3) | copy-done | bytes 524312
  12.7 0.4 shard_map.211
  13.2 0.7 copy-done.4
  13.9 12.3 %all-to-all-start = ((bf16[8,16,1152]{2,1,0:T(8,128)(2,1)}), bf16[8,16,1152]{2,1,0:T(8,128)(2,1)S(1)}, u32[]{:S(2)}, u32[]{:S(2)}) async-start(bf16[8,16,1152]{2,1,0:T(8,128)(2,1)} %copy-done.4), calls=%async_computation | async-start | bytes 589824 | tf_op jit(solution)/shard_map/all_to_all | solution.py:303
  26.1 12.9 %all-to-all-done.got_ref.line_own_ref.line_ref = bf16[8,16,1152]{2,1,0:T(8,128)(2,1)S(1)} async-done(((bf16[8,16,1152]{2,1,0:T(8,128)(2,1)}), bf16[8,16,1152]{2,1,0:T(8,128)(2,1)S(1)}, u32[]{:S(2)}, u32[]{:S(2)}) %all-to-all-start) | async-done | bytes 294944 | tf_op jit(solution)/shard_map/all_to_all | solution.py:303
  39.0 0.6 shard_map.212
  39.6 22.6 %all_to_all.20.own_ref = bf16[16,32,1024]{2,1,0:T(8,128)(2,1)S(1)} all-to-all(bf16[16,32,1024]{2,1,0:T(8,128)(2,1)S(1)} %get-tuple-element.147), channel_id=1, replica_groups=mesh['ep_0'=8,'ep_1'=4,'ep_2'=4,'tp'=2] {'ep_1','ep_2'}, dimensions={0} | all-to-all | bytes 2097152 | tf_op jit(solution)/shard_map/all_to_all | solution.py:314
  62.2 0.5 collective-permute-start.2
  62.8 2.6 %collective-permute-done.2.line_other_ref = bf16[8,16,1152]{2,1,0:T(8,128)(2,1)S(1)} collective-permute-done((bf16[8,16,1152]{2,1,0:T(8,128)(2,1)S(1)}, bf16[8,16,1152]{2,1,0:T(8,128)(2,1)S(1)}, u32[]{:S(2)}, u32[]{:S(2)}) %collective-permute-start.2) | collective-permute-done | bytes 294944 | tf_op jit(solution)/shard_map/ppermute | solution.py:304
  65.3 3.1 %shard_map.213 = (bf16[384,1024]{1,0:T(8,128)(2,1)S(1)}, bf16[384,1024]{1,0:T(8,128)(2,1)S(1)}) custom-call(s32[1]{0:T(128)} %bitcast.core_ref, bf16[16,32,1024]{2,1,0:T(8,128)(2,1)S(1)} %all_to_all.20.own_ref, bf16[16,32,1024]{2,1,0:T(8,128)(2,1)S(1)} %collective-permute-done.1.other_ref, ...), custom_call_target="tpu_custom_call" | custom-call | tf_op jit(solution)/shard_map/pallas_call | solution.py:65
  68.5 0.2 collective-permute-start.3
  68.7 2.1 %collective-permute-done.3.got_ref = bf16[384,1024]{1,0:T(8,128)(2,1)S(1)} collective-permute-done((bf16[384,1024]{1,0:T(8,128)(2,1)S(1)}, bf16[384,1024]{1,0:T(8,128)(2,1)S(1)}, u32[]{:S(2)}, u32[]{:S(2)}) %collective-permute-start.3) | collective-permute-done | bytes 786464 | tf_op jit(solution)/shard_map/ppermute | solution.py:331
  70.8 0.2 add_convert_fusion
  71.0 14.8 %all_to_all.21.back_ref = bf16[16,16,1024]{2,1,0:T(8,128)(2,1)S(1)} all-to-all(bf16[16,16,1024]{2,1,0:T(8,128)(2,1)S(1)} %bitcast.66), channel_id=1, replica_groups=mesh['ep_0'=8,'ep_1'=4,'ep_2'=4,'tp'=2] {'ep_1','ep_2'}, dimensions={0} | all-to-all | bytes 1048576 | tf_op jit(solution)/shard_map/all_to_all | solution.py:333
  85.8 1.0 shard_map.214
  86.8 3.4 %all-to-all-start.3 = ((bf16[8,16,1024]{2,1,0:T(8,128)(2,1)}), bf16[8,16,1024]{2,1,0:T(8,128)(2,1)S(1)}, u32[]{:S(2)}, u32[]{:S(2)}) async-start(bf16[8,16,1024]{2,1,0:T(8,128)(2,1)} %shard_map.214), calls=%async_computation.3 | async-start | bytes 524288 | tf_op jit(solution)/shard_map/all_to_all | solution.py:340
  90.3 1.8 %convolution_convert_fusion.2 = bf16[16,64]{1,0:T(8,128)(2,1)} fusion(bf16[2048,64]{0,1:T(8,128)(2,1)} %param.27, bf16[16,2048]{1,0:T(8,128)(2,1)S(1)} %copy-done.2, f32[2048]{0:T(1024)S(1)} %copy-done.10, f32[16]{0:T(128)S(1)} %add_rsqrt_fusion), kind=kOutput, calls=%fused_computation.45 | convolution fusion | flops 4326400 | bytes 337984 | tf_op jit(solution)/shard_map/dot_general | solution.py:277
  92.1 1.8 %convolution_convert_fusion.3 = bf16[16,64]{1,0:T(8,128)(2,1)} fusion(bf16[2048,64]{0,1:T(8,128)(2,1)} %param.26, bf16[16,2048]{1,0:T(8,128)(2,1)S(1)} %copy-done.2, f32[2048]{0:T(1024)S(1)} %copy-done.10, f32[16]{0:T(128)S(1)} %add_rsqrt_fusion), kind=kOutput, calls=%fused_computation.46 | convolution fusion | flops 4326400 | bytes 337984 | tf_op jit(solution)/shard_map/dot_general | solution.py:276
  93.8 7.4 %all-to-all-done.3 = bf16[8,16,1024]{2,1,0:T(8,128)(2,1)S(1)} async-done(((bf16[8,16,1024]{2,1,0:T(8,128)(2,1)}), bf16[8,16,1024]{2,1,0:T(8,128)(2,1)S(1)}, u32[]{:S(2)}, u32[]{:S(2)}) %all-to-all-start.3) | async-done | bytes 262176 | tf_op jit(solution)/shard_map/all_to_all | solution.py:340
  101.3 0.6 add_convert_fusion.1
  (39 shorter events, 0.5 us)
Async XLA Ops:
  0.6 9.3 %copy-start = (bf16[512,2048]{1,0:T(8,128)(2,1)S(1)}, bf16[512,2048]{1,0:T(8,128)(2,1)}, u32[]{:S(2)}) copy-start(bf16[512,2048]{1,0:T(8,128)(2,1)} %param.31) | copy-start | bytes 6291460
  0.6 5.3 %copy-start.9 = (s32[16]{0:T(128)S(1)}, s32[16]{0:T(128)}, u32[]{:S(2)}) copy-start(s32[16]{0:T(128)} %param.23) | copy-start | bytes 196
  0.7 5.3 %copy-start.13 = (f32[8]{0:T(128)S(1)}, f32[8]{0:T(128)}, u32[]{:S(2)}) copy-start(f32[8]{0:T(128)} %param.28) | copy-start | bytes 100
  9.8 0.7 copy-start.11
  9.8 0.9 copy-start.12
  9.8 1.9 %copy-start.2 = (bf16[16,2048]{1,0:T(8,128)(2,1)S(1)}, bf16[16,2048]{1,0:T(8,128)(2,1)}, u32[]{:S(2)}) copy-start(bf16[16,2048]{1,0:T(8,128)(2,1)} %tokens_ref.1) | copy-start | bytes 196612
  9.8 1.9 %copy-start.5 = (f32[2048]{0:T(1024)S(1)}, f32[2048]{0:T(1024)}, u32[]{:S(2)}) copy-start(f32[2048]{0:T(1024)} %param.32) | copy-start | bytes 24580
  9.8 1.8 %copy-start.6 = (bf16[16,256]{1,0:T(8,128)(2,1)S(1)}, bf16[16,256]{1,0:T(8,128)(2,1)}, u32[]{:S(2)}) copy-start(bf16[16,256]{1,0:T(8,128)(2,1)} %gate_ref.1) | copy-start | bytes 24580
  9.8 1.8 %copy-start.7 = (bf16[16,256]{1,0:T(8,128)(2,1)S(1)}, bf16[16,256]{1,0:T(8,128)(2,1)}, u32[]{:S(2)}) copy-start(bf16[16,256]{1,0:T(8,128)(2,1)} %up_ref.1) | copy-start | bytes 24580
  9.8 1.8 %copy-start.8 = (f32[2048]{0:T(1024)S(1)}, f32[2048]{0:T(1024)}, u32[]{:S(2)}) copy-start(f32[2048]{0:T(1024)} %param.38) | copy-start | bytes 24580
  10.4 55.0 %copy-start.1 = (bf16[1,2048,256]{2,1,0:T(8,128)(2,1)S(1)}, bf16[1,2048,256]{2,1,0:T(8,128)(2,1)}, u32[]{:S(2)}) copy-start(bf16[1,2048,256]{2,1,0:T(8,128)(2,1)} %param.39) | copy-start | bytes 3145732
  10.4 1.3 %collective-permute-start = (bf16[16,2048]{1,0:T(8,128)(2,1)S(1)}, bf16[16,2048]{1,0:T(8,128)(2,1)S(1)}, u32[]{:S(2)}, u32[]{:S(2)}) collective-permute-start(bf16[16,2048]{1,0:T(8,128)(2,1)S(1)} %convolution_convert_fusion.own_ref), channel_id=1, source_target_pairs={{0,1},{1,0},{2,3},{3,2},{4,5},{5,4},{6,7},{7,6},{8,9},{9,8},{10,11... | collective-permute-start | bytes 196616 | tf_op jit(solution)/shard_map/ppermute | solution.py:281
  11.7 1.0 %copy-start.3 = (bf16[2048,128]{1,0:T(8,128)(2,1)S(1)}, bf16[2048,128]{1,0:T(8,128)(2,1)}, u32[]{:S(2)}) copy-start(bf16[2048,128]{1,0:T(8,128)(2,1)} %router_ref.1) | copy-start | bytes 1572868
  13.2 0.7 copy-start.4
  13.9 25.2 %all-to-all-start = ((bf16[8,16,1152]{2,1,0:T(8,128)(2,1)}), bf16[8,16,1152]{2,1,0:T(8,128)(2,1)S(1)}, u32[]{:S(2)}, u32[]{:S(2)}) async-start(bf16[8,16,1152]{2,1,0:T(8,128)(2,1)} %copy-done.4), calls=%async_computation | async-start | bytes 589824 | tf_op jit(solution)/shard_map/all_to_all | solution.py:303
  62.2 3.1 %collective-permute-start.1 = (bf16[16,32,1024]{2,1,0:T(8,128)(2,1)S(1)}, bf16[16,32,1024]{2,1,0:T(8,128)(2,1)S(1)}, u32[]{:S(2)}, u32[]{:S(2)}) collective-permute-start(bf16[16,32,1024]{2,1,0:T(8,128)(2,1)S(1)} %all_to_all.20.own_ref), channel_id=1, source_target_pairs={{0,1},{1,0},{2,3},{3,2},{4,5},{5,4},{6,7},{7,6},{8,9},{9,8},{10,11... | collective-permute-start | bytes 3145736 | tf_op jit(solution)/shard_map/ppermute | solution.py:315
  62.2 3.1 %collective-permute-start.2 = (bf16[8,16,1152]{2,1,0:T(8,128)(2,1)S(1)}, bf16[8,16,1152]{2,1,0:T(8,128)(2,1)S(1)}, u32[]{:S(2)}, u32[]{:S(2)}) collective-permute-start(bf16[8,16,1152]{2,1,0:T(8,128)(2,1)S(1)} %all-to-all-done.got_ref.line_own_ref.line_ref), channel_id=1, source_target_pairs={{0,1},{1,0},{2,3},{3,2},{4,5},{5,4},{6,7},{7,6},{8,9},{9,8},{10,11... | collective-permute-start | bytes 884744 | tf_op jit(solution)/shard_map/ppermute | solution.py:304
  68.5 2.4 %collective-permute-start.3 = (bf16[384,1024]{1,0:T(8,128)(2,1)S(1)}, bf16[384,1024]{1,0:T(8,128)(2,1)S(1)}, u32[]{:S(2)}, u32[]{:S(2)}) collective-permute-start(bf16[384,1024]{1,0:T(8,128)(2,1)S(1)} %get-tuple-element.149), channel_id=1, source_target_pairs={{0,1},{1,0},{2,3},{3,2},{4,5},{5,4},{6,7},{7,6},{8,9},{9,8},{10,11... | collective-permute-start | bytes 2359304 | tf_op jit(solution)/shard_map/ppermute | solution.py:331
  71.0 19.2 %copy-start.10 = (f32[2048]{0:T(1024)S(1)}, f32[2048]{0:T(1024)}, u32[]{:S(2)}) copy-start(f32[2048]{0:T(1024)} %param.24) | copy-start | bytes 24580
  86.8 14.4 %all-to-all-start.3 = ((bf16[8,16,1024]{2,1,0:T(8,128)(2,1)}), bf16[8,16,1024]{2,1,0:T(8,128)(2,1)S(1)}, u32[]{:S(2)}, u32[]{:S(2)}) async-start(bf16[8,16,1024]{2,1,0:T(8,128)(2,1)} %shard_map.214), calls=%async_computation.3 | async-start | bytes 524288 | tf_op jit(solution)/shard_map/all_to_all | solution.py:340

commit v2 on v1

--- a/solution.py
+++ b/solution.py
@@ -21,52 +21,158 @@
     return wide * lax.rsqrt(jnp.mean(wide * wide, axis=-1, keepdims=True) + 1e-06) * gain
 
 
-def stick_read(queries, lengths, head_bias, key_cache, value_cache):
-    seq_count, local_kv, head_dim, cache_len = key_cache.shape
-    group_size = head_bias.shape[0] // local_kv
-    grouped = queries.reshape(seq_count, local_kv, group_size, head_dim)
-    head_shift = head_bias.reshape(1, local_kv, group_size, 1)
-    span_len = min(512, cache_len)
-    block_count = (jnp.max(lengths) + span_len - 1) // span_len
-    span_index = lax.iota(jnp.int32, span_len)
-    after_mask = (span_index[:, None] > span_index[None, :]).astype(F32)
-
-    def visit(visit_index, carry):
-        totals, log_later = carry
-        first = (block_count - 1 - visit_index) * span_len
-        key_block = lax.dynamic_slice_in_dim(key_cache, first, span_len, 3)
-        value_block = lax.dynamic_slice_in_dim(value_cache, first, span_len, 3)
-        scores = (
-            jnp.einsum("skgd,skdc->skgc", grouped, key_block, preferred_element_type=F32)
-            * head_dim ** (-0.5)
-            + head_shift
+def attend_kernel(
+    bias_hbm,
+    lengths_hbm,
+    tokens_hbm,
+    gain_hbm,
+    query_hbm,
+    key_hbm,
+    value_hbm,
+    out_hbm,
+    partial_ref,
+    bias_ref,
+    lengths_ref,
+    tokens_ref,
+    gain_ref,
+    query_buf,
+    key_buf,
+    value_buf,
+    out_buf,
+    sems,
+):
+    seq_count, width = tokens_ref.shape
+    head_total = query_buf.shape[1]
+    row_total, cache_len = key_buf.shape
+    head_dim = row_total // seq_count
+    heads = head_total // head_dim
+    copies = []
+
+    def fetch(source, target, pieces):
+        size = source.shape[0] // pieces
+        made = []
+        for n in range(pieces):
+            at = pl.ds(n * size, size)
+            made.append(pltpu.make_async_copy(source.at[at, :], target.at[at, :], sems.at[len(copies)]))
+            copies.append(made[-1])
+        return made
+
+    small_copies = [
+        fetch(source, target, 1)[0]
+        for source, target in (
+            (tokens_hbm, tokens_ref),
+            (gain_hbm, gain_ref),
+            (bias_hbm, bias_ref),
+            (lengths_hbm, lengths_ref),
         )
-        positions = first + span_index
-        visible = (positions[None, :] < lengths[:, None])[:, None, None, :]
-        log_keep = jnp.where(visible, jax.nn.log_sigmoid(-scores), 0.0)
-        log_after = jnp.einsum("skgj,jc->skgc", log_keep, after_mask) + log_later[..., None]
-        weights = jnp.where(visible, jnp.exp(jax.nn.log_sigmoid(scores) + log_after), 0.0).astype(
-            BF16
+    ]
+    query_copies = fetch(query_hbm, query_buf, 2)
+    key_copies = fetch(key_hbm, key_buf, 2)
+    value_copies = fetch(value_hbm, value_buf, 2)
+    out_copies = fetch(out_hbm, out_buf, 1)
+    for copy in copies:
+        copy.start()
+
+    for copy in small_copies:
+        copy.wait()
+    normed = rms_scale(tokens_ref[...], gain_ref[...]).astype(BF16)
+    row = lax.broadcasted_iota(jnp.int32, (heads * seq_count, 1), 0)
+    bias = jnp.zeros((heads * seq_count, 1), F32)
+    for h in range(heads):
+        bias = jnp.where(row // seq_count == h, bias_ref[:, h : h + 1], bias)
+    lengths = jnp.zeros((seq_count, 1), jnp.int32)
+    for n in range(seq_count):
+        lengths = jnp.where(row[:seq_count] == n, lengths_ref[:, n : n + 1], lengths)
+    lengths = jnp.concatenate([lengths] * heads, axis=0)
+    lane = lax.broadcasted_iota(jnp.int32, (seq_count, 128), 1)
+    low = lane < head_dim
+    own = (
+        lax.broadcasted_iota(jnp.int32, (seq_count, row_total), 1) // head_dim
+        == lax.broadcasted_iota(jnp.int32, (seq_count, row_total), 0)
+    )
+    span = 256
+    after_mask = (
+        lax.broadcasted_iota(jnp.int32, (span, span), 0) > lax.broadcasted_iota(jnp.int32, (span, span), 1)
+    ).astype(BF16)
+
+    queries = jnp.zeros((seq_count, head_total), F32)
+    piece = width // len(query_copies)
+    for n, copy in enumerate(query_copies):
+        copy.wait()
+        at = slice(n * piece, (n + 1) * piece)
+        queries += jnp.dot(normed[:, at], query_buf[at, :], preferred_element_type=F32)
+    queries = queries.astype(BF16).astype(F32)
+    spread = []
+    for h in range(heads):
+        tile = queries[:, h // 2 * 128 : h // 2 * 128 + 128]
+        turned = pltpu.roll(tile, head_dim, 1)
+        both = jnp.where(low, tile, turned) if h % 2 == 0 else jnp.where(low, turned, tile)
+        wide = jnp.concatenate([both] * (row_total // 128), axis=1)
+        spread.append(jnp.where(own, wide, 0.0).astype(BF16))
+    spread = jnp.concatenate(spread, axis=0)
+
+    scores = None
+    piece = row_total // len(key_copies)
+    for n, copy in enumerate(key_copies):
+        copy.wait()
+        at = slice(n * piece, (n + 1) * piece)
+        part = jnp.dot(spread[:, at], key_buf[at, :], preferred_element_type=F32)
+        scores = part if scores is None else scores + part
+    later = jnp.zeros((heads * seq_count, 1), F32)
+    sticks = []
+    for block in reversed(range(cache_len // span)):
+        score = scores[:, block * span : (block + 1) * span] * head_dim ** (-0.5) + bias
+        position = lax.broadcasted_iota(jnp.int32, score.shape, 1) + block * span
+        visible = position < lengths
+        soft = jnp.log1p(jnp.exp(-jnp.abs(score)))
+        log_keep = jnp.where(visible, -(jnp.maximum(score, 0.0) + soft), 0.0)
+        high = log_keep.astype(BF16)
+        rest = (log_keep - high.astype(F32)).astype(BF16)
+        log_after = jnp.dot(high, after_mask, preferred_element_type=F32)
+        log_after += jnp.dot(rest, after_mask, preferred_element_type=F32)
+        weight = jnp.exp(jnp.minimum(score, 0.0) - soft + (log_after + later))
+        sticks.append(jnp.where(visible, weight, 0.0).astype(BF16))
+        later += jnp.sum(log_keep, axis=-1, keepdims=True)
+    sticks = jnp.concatenate(sticks[::-1], axis=1)
+
+    read = []
+    piece = row_total // len(value_copies)
+    for n, copy in enumerate(value_copies):
+        copy.wait()
+        read.append(
+            lax.dot_general(
+                sticks,
+                value_buf[n * piece : (n + 1) * piece, :],
+                (((1,), (1,)), ((), ())),
+                preferred_element_type=F32,
+            )
         )
-        totals = totals + jnp.einsum(
-            "skgc,skdc->skgd", weights, value_block, preferred_element_type=F32
-        )
-        return (totals, log_later + jnp.sum(log_keep, axis=3))
-
-    start_totals = jnp.zeros((seq_count, local_kv, group_size, head_dim), F32)
-    start_later = jnp.zeros((seq_count, local_kv, group_size), F32)
-    totals, unused_later = lax.fori_loop(0, block_count, visit, (start_totals, start_later))
-    return totals.reshape(seq_count, -1).astype(BF16)
-
-
-def call(kernel, out_shape, smem_count, inputs, limit=48):
+    read = jnp.concatenate(read, axis=1)
+    folded = []
+    for h in range(heads):
+        mine = jnp.where(own, read[h * seq_count : (h + 1) * seq_count], 0.0)
+        tile = mine[:, :128]
+        for n in range(1, row_total // 128):
+            tile += mine[:, n * 128 : (n + 1) * 128]
+        folded.append(tile + pltpu.roll(tile, head_dim, 1))
+    heads_out = jnp.concatenate(
+        [jnp.where(low, folded[h], folded[h + 1]) for h in range(0, heads, 2)], axis=1
+    ).astype(BF16)
+    for copy in out_copies:
+        copy.wait()
+    partial_ref[...] = jnp.dot(heads_out, out_buf[...], preferred_element_type=F32).astype(BF16)
+
+
+def call(kernel, out_shape, smem_count, inputs, limit, hbm_count=0, scratch=()):
     in_specs = [pl.BlockSpec(memory_space=pltpu.SMEM)] * smem_count
-    in_specs += [pl.BlockSpec(memory_space=pltpu.VMEM)] * (len(inputs) - smem_count)
+    in_specs += [pl.BlockSpec(memory_space=pltpu.VMEM)] * (len(inputs) - smem_count - hbm_count)
+    in_specs += [pl.BlockSpec(memory_space=pltpu.HBM)] * hbm_count
     return pl.pallas_call(
         kernel,
         out_shape=out_shape,
         in_specs=in_specs,
         out_specs=jax.tree.map(lambda _: pl.BlockSpec(memory_space=pltpu.VMEM), out_shape),
+        scratch_shapes=scratch,
         compiler_params=pltpu.CompilerParams(vmem_limit_bytes=limit * 1024 * 1024),
     )(*inputs)
 
@@ -116,12 +222,7 @@
         meta = put(meta, GATE_LO + k, gate - high)
     mix_high = mix.astype(BF16).astype(F32)
     meta = put(put(meta, MIX_HI, mix_high), MIX_LO, mix - mix_high)
-    eye = (
-        lax.broadcasted_iota(jnp.int32, (seq_count, seq_count), 0)
-        == lax.broadcasted_iota(jnp.int32, (seq_count, seq_count), 1)
-    ).astype(BF16)
-    down = lax.dot_general(eye, down_ref[...], (((1,), (1,)), ((), ())), preferred_element_type=F32)
-    parts = (gate_ref[...].astype(F32), up_ref[...].astype(F32), down)
+    parts = [ref[...].astype(F32) for ref in (gate_ref, up_ref, down_ref)]
     part = parts[0].shape[1] // lines
     row = jnp.where(first_core, normed[:, :half], normed[:, half:])
     for line in range(lines):
@@ -177,56 +278,76 @@
     combine_ref[:, slot_total:] = (weights - high.astype(F32)).astype(BF16)
 
 
-def experts_kernel(
-    core_ref, own_ref, other_ref, line_own_ref, line_other_ref, gate_ref, up_ref, down_ref, keep_ref, send_ref
+def dense_weights(slots_ref, side, at):
+    places, rows, _ = slots_ref.shape
+    capacity = rows // 2
+    lane = pl.multiple_of((side * 4 + at) * 128, 128)
+    return slots_ref[:, capacity:, pl.ds(lane, 128)].reshape(places * capacity, 128)
+
+
+def half_products(side, slots_ref, line_ref, gate_ref, up_ref, dense_ref):
+    places, rows, half = slots_ref.shape
+    mine = pl.ds(pl.multiple_of(side * half, half), half)
+    values = slots_ref[:, : rows // 2, :].reshape(places * rows // 2, half)
+    gate = jnp.dot(values, gate_ref[mine, :], preferred_element_type=F32)
+    up = jnp.dot(values, up_ref[mine, :], preferred_element_type=F32)
+    line = line_ref[:, :, :half].reshape(-1, half)
+    block = half // 4
+    dense = sum(
+        jnp.dot(
+            line[:, k * block : (k + 1) * block], dense_weights(dense_ref, side, k), preferred_element_type=F32
+        )
+        for k in range(4)
+    )
+    return gate, up, dense
+
+
+def own_kernel(core_ref, slots_ref, line_ref, gate_ref, up_ref, gate_out, up_out, dense_out):
+    gate, up, dense = half_products(core_ref[0], slots_ref, line_ref, gate_ref, up_ref, slots_ref)
+    gate_out[...] = gate
+    up_out[...] = up
+    dense_out[...] = dense
+
+
+def down_products(side, hidden, dense, down_ref, dense_ref, target_ref):
+    slot_total, half = hidden.shape[0], target_ref.shape[1]
+    mine = pl.ds(pl.multiple_of(side * half, half), half)
+    target_ref[:slot_total, :] = jnp.dot(hidden, down_ref[:, mine], preferred_element_type=F32).astype(BF16)
+    block = half // 4
+    for k in range(4):
+        target_ref[slot_total:, k * block : (k + 1) * block] = lax.dot_general(
+            dense, dense_weights(dense_ref, side, k), (((1,), (1,)), ((), ())), preferred_element_type=F32
+        ).astype(BF16)
+
+
+def other_kernel(
+    core_ref,
+    gate_sum,
+    up_sum,
+    dense_sum,
+    own_ref,
+    other_ref,
+    line_ref,
+    gate_ref,
+    up_ref,
+    down_ref,
+    send_ref,
+    hidden_ref,
+    dense_ref,
 ):
-    core = core_ref[0]
-    places, rows, half = own_ref.shape
-    capacity = rows // 2
-    slot_total = places * capacity
-    lines, seq_count, _ = line_own_ref.shape
-    token_total = lines * seq_count
-    mine = pl.ds(pl.multiple_of(core * half, half), half)
-    theirs = pl.ds(pl.multiple_of((1 - core) * half, half), half)
-    x_own = own_ref[:, :capacity, :].reshape(slot_total, half)
-    x_other = other_ref[:, :capacity, :].reshape(slot_total, half)
-
-    def project(weight_ref):
-        return jnp.dot(x_own, weight_ref[mine, :], preferred_element_type=F32) + jnp.dot(
-            x_other, weight_ref[theirs, :], preferred_element_type=F32
-        )
-
-    hidden = (jax.nn.silu(project(gate_ref)) * project(up_ref)).astype(BF16)
-    keep_ref[:slot_total, :] = jnp.dot(hidden, down_ref[:, mine], preferred_element_type=F32).astype(BF16)
-    send_ref[:slot_total, :] = jnp.dot(hidden, down_ref[:, theirs], preferred_element_type=F32).astype(BF16)
-
-    half_lines = lines // 2
-    block = half // half_lines
-
-    def dense_weights(line):
-        at = pl.multiple_of(line * 128, 128)
-        return own_ref[:, capacity:, pl.ds(at, 128)].reshape(block, 128)
-
-    line_own = line_own_ref[:, :, :half].reshape(token_total, half)
-    line_other = line_other_ref[:, :, :half].reshape(token_total, half)
-    sums = jnp.zeros((token_total, 128), F32)
-    for k in range(half_lines):
-        at = slice(k * block, (k + 1) * block)
-        sums += jnp.dot(line_own[:, at], dense_weights(core * half_lines + k), preferred_element_type=F32)
-        sums += jnp.dot(line_other[:, at], dense_weights((1 - core) * half_lines + k), preferred_element_type=F32)
-    lane = lax.broadcasted_iota(jnp.int32, sums.shape, 1)
-    gate = pltpu.roll(sums, 64, 1)
-    up = pltpu.roll(sums, 32, 1)
-    dense = jnp.where(lane >= 96, jax.nn.silu(gate) * up, 0.0).astype(BF16)
-    for k in range(half_lines):
-        at = slice(k * block, (k + 1) * block)
-        for target, side in ((keep_ref, core), (send_ref, 1 - core)):
-            target[slot_total:, at] = lax.dot_general(
-                dense,
-                dense_weights(side * half_lines + k),
-                (((1,), (1,)), ((), ())),
-                preferred_element_type=F32,
-            ).astype(BF16)
+    side = 1 - core_ref[0]
+    gate, up, dense = half_products(side, other_ref, line_ref, gate_ref, up_ref, own_ref)
+    hidden = (jax.nn.silu(gate_sum[...] + gate) * (up_sum[...] + up)).astype(BF16)
+    dense += dense_sum[...]
+    lane = lax.broadcasted_iota(jnp.int32, dense.shape, 1)
+    dense = jnp.where(lane >= 96, jax.nn.silu(pltpu.roll(dense, 64, 1)) * pltpu.roll(dense, 32, 1), 0.0).astype(BF16)
+    hidden_ref[...] = hidden
+    dense_ref[...] = dense
+    down_products(side, hidden, dense, down_ref, own_ref, send_ref)
+
+
+def keep_kernel(core_ref, hidden_ref, dense_ref, own_ref, down_ref, keep_ref):
+    down_products(core_ref[0], hidden_ref[...], dense_ref[...], down_ref, own_ref, keep_ref)
 
 
 def combine_kernel(back_ref, combine_ref, line_ref, keep_ref, got_ref, send_ref):
@@ -272,12 +393,36 @@
     token_total = lines * seq_count
     core = lax.axis_index("tp").astype(jnp.int32).reshape(1)
     line = lax.axis_index(LINE).astype(jnp.int32).reshape(1)
-    normed = rms_scale(tokens, attn_gain).astype(BF16)
-    new_keys = jnp.dot(normed, w_key, preferred_element_type=F32).astype(BF16)
-    new_values = jnp.dot(normed, w_value, preferred_element_type=F32).astype(BF16)
-    queries = jnp.dot(normed, w_query, preferred_element_type=F32).astype(BF16)
-    heads_out = stick_read(queries, lengths, head_bias, key_cache, value_cache)
-    attn_own = jnp.dot(heads_out, w_attn_out, preferred_element_type=F32).astype(BF16)
+    cache_rows = seq_count * key_cache.shape[2]
+    cache_len = key_cache.shape[3]
+    attn_own = call(
+        attend_kernel,
+        jax.ShapeDtypeStruct((seq_count, width), BF16),
+        0,
+        (
+            head_bias.reshape(1, -1),
+            lengths.reshape(1, seq_count),
+            tokens,
+            attn_gain.reshape(1, width),
+            w_query,
+            key_cache.reshape(cache_rows, cache_len),
+            value_cache.reshape(cache_rows, cache_len),
+            w_attn_out,
+        ),
+        52,
+        hbm_count=8,
+        scratch=(
+            pltpu.VMEM((1, head_bias.shape[0]), F32),
+            pltpu.VMEM((1, seq_count), jnp.int32),
+            pltpu.VMEM(tokens.shape, BF16),
+            pltpu.VMEM((1, width), F32),
+            pltpu.VMEM(w_query.shape, BF16),
+            pltpu.VMEM((cache_rows, cache_len), BF16),
+            pltpu.VMEM((cache_rows, cache_len), BF16),
+            pltpu.VMEM(w_attn_out.shape, BF16),
+            pltpu.SemaphoreType.DMA((11,)),
+        ),
+    )
     attn_other = lax.ppermute(attn_own, "tp", SWAP)
     line_send, residual = call(
         rows_kernel,
@@ -296,9 +441,10 @@
             routes,
             w_dense_gate,
             w_dense_up,
-            w_dense_down,
+            w_dense_down.T,
             dense_mix.reshape(1, width),
         ),
+        8,
     )
     line_own = lax.all_to_all(line_send, LINE, 0, 0, tiled=True)
     line_other = lax.ppermute(line_own, "tp", SWAP)
@@ -310,25 +456,29 @@
         ),
         1,
         (line, line_own),
+        8,
     )
     slot_own = lax.all_to_all(slot_send, PLANE, 0, 0, tiled=True)
     slot_other = lax.ppermute(slot_own, "tp", SWAP)
-    keep, send = call(
-        experts_kernel,
-        (jax.ShapeDtypeStruct((slot_total + token_total, half), BF16),) * 2,
+    weights = (w_expert_gate[0], w_expert_up[0])
+    hidden_shape = (slot_total, w_expert_gate.shape[2])
+    sums = call(
+        own_kernel,
+        (jax.ShapeDtypeStruct(hidden_shape, F32),) * 2 + (jax.ShapeDtypeStruct((token_total, 128), F32),),
         1,
-        (
-            core,
-            slot_own,
-            slot_other,
-            line_own,
-            line_other,
-            w_expert_gate[0],
-            w_expert_up[0],
-            w_expert_down[0],
-        ),
+        (core, slot_own, line_own, *weights),
+        8,
+    )
+    both_shape = jax.ShapeDtypeStruct((slot_total + token_total, half), BF16)
+    send, hidden, dense = call(
+        other_kernel,
+        (both_shape, jax.ShapeDtypeStruct(hidden_shape, BF16), jax.ShapeDtypeStruct((token_total, 128), BF16)),
+        1,
+        (core, *sums, slot_own, slot_other, line_other, *weights, w_expert_down[0]),
+        12,
     )
     got = lax.ppermute(send, "tp", SWAP)
+    keep = call(keep_kernel, both_shape, 1, (core, hidden, dense, slot_own, w_expert_down[0]), 8)
     results = (keep[:slot_total].astype(F32) + got[:slot_total].astype(F32)).astype(BF16)
     back = lax.all_to_all(results.reshape(places, seq_count, half), PLANE, 0, 0, tiled=True)
     partial = call(
@@ -336,9 +486,13 @@
         jax.ShapeDtypeStruct((lines, seq_count, half), BF16),
         0,
         (back, combine, line_own, keep, got),
+        8,
     )
     parts = lax.all_to_all(partial, LINE, 0, 0, tiled=True)
     layer_out = (residual.astype(F32) + jnp.sum(parts.astype(F32), axis=0)).astype(BF16)
+    normed = rms_scale(tokens, attn_gain).astype(BF16)
+    new_keys = jnp.dot(normed, w_key, preferred_element_type=F32).astype(BF16)
+    new_values = jnp.dot(normed, w_value, preferred_element_type=F32).astype(BF16)
     return (layer_out, new_keys, new_values)
 
 

time: 103 us -> 95.6 us (0.928)
  blocking collectives: 37.4 us -> 22.6 us
  waiting for transfers between devices: 26 us -> 37.1 us
  matrix products: 9.56 us -> 2.62 us
  Pallas kernels: 5.17 us -> 9.3 us
  other arithmetic: 3.36 us -> 1.8 us
  starting transfers between devices: 16.4 us -> 17.7 us
    all_to_all x1 -> x0, blocking collectives: 14.8 us -> none  [shards(): lax.all_to_all(results.reshape(places, seq_count, half), PLANE, 0, 0, til...]
    all_to_all x0 -> x1, waiting for transfers between devices: none -> 10.7 us  [shards(): lax.all_to_all(results.reshape(places, seq_count, half), PLANE, 0, 0, til...]
    dot_general x4 -> x0, matrix products: 5.99 us -> none  [the longest x1 2.07 us: shards(): queries = jnp.dot(normed, w_query, preferred_element_type=F32).astype(BF16)]
    all_to_all x0 -> x1, starting transfers between devices: none -> 4.95 us  [shards(): lax.all_to_all(results.reshape(places, seq_count, half), PLANE, 0, 0, til...]
    pallas_call x4 -> x7, Pallas kernels: 5.17 us -> 9.3 us  [call(): pl.pallas_call(kernel, out_shape=out_shape, in_specs=in_specs, out_specs=...]
    all_to_all x1, starting transfers between devices: 12.3 us -> 8.47 us  [shards(): line_own = lax.all_to_all(line_send, LINE, 0, 0, tiled=True)]
    reduce_max x1 -> x0, other arithmetic: 1.44 us -> none  [stick_read(): block_count = (jnp.max(lengths) + span_len - 1) // span_len]
    all_to_all x1, waiting for transfers between devices: 7.4 us -> 8.58 us  [shards(): parts = lax.all_to_all(partial, LINE, 0, 0, tiled=True)]
  transfers between devices with their start and end apart: 6 -> 7, of which waited for: 5 -> 6; matrix products, arithmetic and copies ran while one was open for 4% -> 3% of each run, Pallas kernels for 0% -> 1%
where the time goes in v2:
time: 95.6 us; the launch traced here: 95 us
  waiting for transfers between devices  37.1 us (39%)
  blocking collectives  22.6 us (24%)
  starting transfers between devices  17.7 us (19%)
  Pallas kernels  9.3 us (10%)
  local copies, waits for them, and re-layouts  3.03 us (3%)
  matrix products  2.62 us (3%)
  other arithmetic  1.8 us (2%)
    all_to_all x1, blocking collectives, shards(): slot_own = lax.all_to_all(slot_send, PLANE, 0, 0, tiled=True)  22.6 us
    all_to_all x1, waiting for transfers between devices, shards(): line_own = lax.all_to_all(line_send, LINE, 0, 0, tiled=True)  12.9 us
    all_to_all x1, waiting for transfers between devices, shards(): lax.all_to_all(results.reshape(places, seq_count, half), PLANE, 0, 0, til...  10.7 us
    pallas_call x7, Pallas kernels, call(): pl.pallas_call(kernel, out_shape=out_shape, in_specs=in_specs, out_specs=...  9.3 us
    all_to_all x1, waiting for transfers between devices, shards(): parts = lax.all_to_all(partial, LINE, 0, 0, tiled=True)  8.58 us
    all_to_all x1, starting transfers between devices, shards(): line_own = lax.all_to_all(line_send, LINE, 0, 0, tiled=True)  8.47 us
    all_to_all x1, starting transfers between devices, shards(): lax.all_to_all(results.reshape(places, seq_count, half), PLANE, 0, 0, til...  4.95 us
    all_to_all x1, starting transfers between devices, shards(): parts = lax.all_to_all(partial, LINE, 0, 0, tiled=True)  3.41 us
  transfers between devices with their start and end apart: 7, of which 6 were waited for; matrix products, arithmetic and copies ran while one was open for 3% of the time, Pallas kernels for 1%

profile of v2, /device:TPU:2, one launch (start us, length us, event | category | flops | bytes accessed | tf_op | source)
XLA Modules:
  0.0 95.0 jit_solution(13891084843464875696)
XLA Ops:
  0.6 0.0 copy-start
  0.7 0.9 copy-done.4
  1.5 0.7 copy-done.12
  2.2 0.7 copy-done.14
  2.9 0.7 copy-done.15
  3.6 4.9 %shard_map.211.own_ref = bf16[16,2048]{1,0:T(8,128)(2,1)S(1)} custom-call(f32[1,8]{1,0:T(1,128)S(1)} %bitcast.26, s32[1,16]{1,0:T(1,128)S(1)} %bitcast.27, bf16[16,2048]{1,0:T(8,128)(2,1)S(1)} %copy-done.4, f32[1,2048]{1,0:T(1,128)S(1)} %bitcast.25, bf16[2048,512]{1,0:T(8,128)(2,1)} %query_hbm.1, bf16[1024,1024]{1,0:T(8,128)(2,1)} %bitcast.29, ...), custom_call_target="tpu_custom_call" | custom-call | tf_op jit(solution)/shard_map/pallas_call | solution.py:170
  8.5 0.0 copy-start.2
  8.5 0.1 collective-permute-start
  8.6 0.1 copy.23.routes_ref
  8.7 1.1 %collective-permute-done.other_ref = bf16[16,2048]{1,0:T(8,128)(2,1)S(1)} collective-permute-done((bf16[16,2048]{1,0:T(8,128)(2,1)S(1)}, bf16[16,2048]{1,0:T(8,128)(2,1)S(1)}, u32[]{:S(2)}, u32[]{:S(2)}) %collective-permute-start) | collective-permute-done | bytes 65568 | tf_op jit(solution)/shard_map/ppermute | solution.py:426
  9.9 1.1 %shard_map.212 = (bf16[8,16,1152]{2,1,0:T(8,128)(2,1)}, bf16[16,1024]{1,0:T(8,128)(2,1)S(1)}) custom-call(s32[1]{0:T(128)} %bitcast.core_ref, bf16[16,2048]{1,0:T(8,128)(2,1)S(1)} %copy-done.5, bf16[16,2048]{1,0:T(8,128)(2,1)S(1)} %shard_map.211.own_ref, bf16[16,2048]{1,0:T(8,128)(2,1)S(1)} %collective-permute-done.other_ref, f32[1,2048]{1,0:T(1,128)S(1)} %bitcast.22, ...), custom_call_target="tpu_custom_call" | custom-call | tf_op jit(solution)/shard_map/pallas_call | solution.py:170
  11.1 8.5 %all-to-all-start = ((bf16[8,16,1152]{2,1,0:T(8,128)(2,1)}), bf16[8,16,1152]{2,1,0:T(8,128)(2,1)S(1)}, u32[]{:S(2)}, u32[]{:S(2)}) async-start(bf16[8,16,1152]{2,1,0:T(8,128)(2,1)} %get-tuple-element.14), calls=%async_computation | async-start | bytes 589824 | tf_op jit(solution)/shard_map/all_to_all | solution.py:449
  19.5 12.9 %all-to-all-done.got_ref.line_ref = bf16[8,16,1152]{2,1,0:T(8,128)(2,1)S(1)} async-done(((bf16[8,16,1152]{2,1,0:T(8,128)(2,1)}), bf16[8,16,1152]{2,1,0:T(8,128)(2,1)S(1)}, u32[]{:S(2)}, u32[]{:S(2)}) %all-to-all-start) | async-done | bytes 294944 | tf_op jit(solution)/shard_map/all_to_all | solution.py:449
  32.4 0.6 shard_map.213
  33.0 22.6 %all_to_all.20.slots_ref.own_ref = bf16[16,32,1024]{2,1,0:T(8,128)(2,1)S(1)} all-to-all(bf16[16,32,1024]{2,1,0:T(8,128)(2,1)S(1)} %get-tuple-element.15), channel_id=1, replica_groups=mesh['ep_0'=8,'ep_1'=4,'ep_2'=4,'tp'=2] {'ep_1','ep_2'}, dimensions={0} | all-to-all | bytes 2097152 | tf_op jit(solution)/shard_map/all_to_all | solution.py:461
  55.6 0.5 collective-permute-start.2
  56.1 0.5 shard_map.214
  56.7 2.1 %collective-permute-done.2.line_ref = bf16[8,16,1152]{2,1,0:T(8,128)(2,1)S(1)} collective-permute-done((bf16[8,16,1152]{2,1,0:T(8,128)(2,1)S(1)}, bf16[8,16,1152]{2,1,0:T(8,128)(2,1)S(1)}, u32[]{:S(2)}, u32[]{:S(2)}) %collective-permute-start.2) | collective-permute-done | bytes 294944 | tf_op jit(solution)/shard_map/ppermute | solution.py:450
  58.7 0.8 shard_map.215
  59.5 0.2 collective-permute-start.3
  59.7 0.4 shard_map.216.keep_ref
  60.1 1.8 %collective-permute-done.3.got_ref = bf16[384,1024]{1,0:T(8,128)(2,1)S(1)} collective-permute-done((bf16[384,1024]{1,0:T(8,128)(2,1)S(1)}, bf16[384,1024]{1,0:T(8,128)(2,1)S(1)}, u32[]{:S(2)}, u32[]{:S(2)}) %collective-permute-start.3) | collective-permute-done | bytes 786464 | tf_op jit(solution)/shard_map/ppermute | solution.py:480
  61.9 1.0 %add_convert_fusion = bf16[256,1024]{1,0:T(8,128)(2,1)} fusion(bf16[384,1024]{1,0:T(8,128)(2,1)S(1)} %collective-permute-done.3.got_ref, bf16[384,1024]{1,0:T(8,128)(2,1)S(1)} %shard_map.216.keep_ref), kind=kLoop, calls=%fused_computation.2 | loop fusion | flops 1048576 | bytes 1572864 | tf_op jit(solution)/shard_map/convert_element_type | solution.py:482
  62.9 5.0 %all-to-all-start.2 = ((bf16[16,16,1024]{2,1,0:T(8,128)(2,1)}), bf16[16,16,1024]{2,1,0:T(8,128)(2,1)S(1)}, u32[]{:S(2)}, u32[]{:S(2)}) async-start(bf16[16,16,1024]{2,1,0:T(8,128)(2,1)} %bitcast.28), calls=%async_computation.2 | async-start | bytes 1048576 | tf_op jit(solution)/shard_map/all_to_all | solution.py:483
  67.8 0.1 fusion
  68.0 10.7 %all-to-all-done.2.back_ref = bf16[16,16,1024]{2,1,0:T(8,128)(2,1)S(1)} async-done(((bf16[16,16,1024]{2,1,0:T(8,128)(2,1)}), bf16[16,16,1024]{2,1,0:T(8,128)(2,1)S(1)}, u32[]{:S(2)}, u32[]{:S(2)}) %all-to-all-start.2) | async-done | bytes 524320 | tf_op jit(solution)/shard_map/all_to_all | solution.py:483
  78.7 1.0 %shard_map.217 = bf16[8,16,1024]{2,1,0:T(8,128)(2,1)} custom-call(bf16[16,16,1024]{2,1,0:T(8,128)(2,1)S(1)} %all-to-all-done.2.back_ref, bf16[128,512]{1,0:T(8,128)(2,1)S(1)} %get-tuple-element.22.combine_ref, bf16[8,16,1152]{2,1,0:T(8,128)(2,1)S(1)} %all-to-all-done.got_ref.line_ref, bf16[384,1024]{1,0:T(8,128)(2,1)S(1)} %shard_map.216.keep_ref, ...), custom_call_target="tpu_custom_call" | custom-call | tf_op jit(solution)/shard_map/pallas_call | solution.py:170
  79.7 3.4 %all-to-all-start.3 = ((bf16[8,16,1024]{2,1,0:T(8,128)(2,1)}), bf16[8,16,1024]{2,1,0:T(8,128)(2,1)S(1)}, u32[]{:S(2)}, u32[]{:S(2)}) async-start(bf16[8,16,1024]{2,1,0:T(8,128)(2,1)} %shard_map.217), calls=%async_computation.3 | async-start | bytes 524288 | tf_op jit(solution)/shard_map/all_to_all | solution.py:491
  83.1 0.8 convolution_convert_fusion
  84.0 1.8 %convolution_convert_fusion.1 = bf16[16,64]{1,0:T(8,128)(2,1)} fusion(bf16[2048,64]{0,1:T(8,128)(2,1)} %param.24, bf16[16,2048]{1,0:T(8,128)(2,1)S(1)} %copy-done.5, f32[2048]{0:T(1024)S(1)} %copy-done.13, f32[16]{0:T(128)S(1)} %add_rsqrt_fusion), kind=kOutput, calls=%fused_computation.1 | convolution fusion | flops 4326400 | bytes 337984 | tf_op jit(solution)/shard_map/dot_general | solution.py:494
  85.7 8.6 %all-to-all-done.3 = bf16[8,16,1024]{2,1,0:T(8,128)(2,1)S(1)} async-done(((bf16[8,16,1024]{2,1,0:T(8,128)(2,1)}), bf16[8,16,1024]{2,1,0:T(8,128)(2,1)S(1)}, u32[]{:S(2)}, u32[]{:S(2)}) %all-to-all-start.3) | async-done | bytes 262176 | tf_op jit(solution)/shard_map/all_to_all | solution.py:491
  94.4 0.6 add_convert_fusion.1
  (32 shorter events, 0.1 us)
Async XLA Ops:
  0.6 82.5 %copy-start = (bf16[2048,64]{0,1:T(8,128)(2,1)S(1)}, bf16[2048,64]{0,1:T(8,128)(2,1)}, u32[]{:S(2)}) copy-start(bf16[2048,64]{0,1:T(8,128)(2,1)} %param.25) | copy-start | bytes 786436
  0.7 0.9 copy-start.4
  1.5 0.7 copy-start.12
  2.2 0.7 copy-start.14
  2.9 0.7 copy-start.15
  3.5 5.1 %copy-start.16 = (s32[16,6]{0,1:T(8,128)S(1)}, s32[16,6]{0,1:T(8,128)}, u32[]{:S(2)}) copy-start(s32[16,6]{0,1:T(8,128)} %param.32) | copy-start | bytes 1156
  3.5 6.3 %copy-start.5 = (bf16[16,2048]{1,0:T(8,128)(2,1)S(1)}, bf16[16,2048]{1,0:T(8,128)(2,1)}, u32[]{:S(2)}) copy-start(bf16[16,2048]{1,0:T(8,128)(2,1)} %tokens_ref.1) | copy-start | bytes 196612
  3.5 6.3 %copy-start.6 = (bf16[2048,128]{1,0:T(8,128)(2,1)S(1)}, bf16[2048,128]{1,0:T(8,128)(2,1)}, u32[]{:S(2)}) copy-start(bf16[2048,128]{1,0:T(8,128)(2,1)} %router_ref.1) | copy-start | bytes 1572868
  3.5 6.3 %copy-start.7 = (f32[2048]{0:T(1024)S(1)}, f32[2048]{0:T(1024)}, u32[]{:S(2)}) copy-start(f32[2048]{0:T(1024)} %param.30) | copy-start | bytes 24580
  3.6 6.3 %copy-start.8 = (bf16[16,256]{1,0:T(8,128)(2,1)S(1)}, bf16[16,256]{1,0:T(8,128)(2,1)}, u32[]{:S(2)}) copy-start(bf16[16,256]{1,0:T(8,128)(2,1)} %gate_ref.1) | copy-start | bytes 24580
  3.6 6.3 %copy-start.9 = (bf16[16,256]{1,0:T(8,128)(2,1)S(1)}, bf16[16,256]{1,0:T(8,128)(2,1)}, u32[]{:S(2)}) copy-start(bf16[16,256]{1,0:T(8,128)(2,1)} %up_ref.1) | copy-start | bytes 24580
  3.6 6.3 %copy-start.10 = (bf16[256,16]{0,1:T(8,128)(2,1)S(1)}, bf16[256,16]{0,1:T(8,128)(2,1)}, u32[]{:S(2)}) copy-start(bf16[256,16]{0,1:T(8,128)(2,1)} %param.35) | copy-start | bytes 24580
  3.6 6.3 %copy-start.11 = (f32[2048]{0:T(1024)S(1)}, f32[2048]{0:T(1024)}, u32[]{:S(2)}) copy-start(f32[2048]{0:T(1024)} %param.36) | copy-start | bytes 24580
  8.5 47.7 %copy-start.2 = (bf16[1,2048,256]{2,1,0:T(8,128)(2,1)S(1)}, bf16[1,2048,256]{2,1,0:T(8,128)(2,1)}, u32[]{:S(2)}) copy-start(bf16[1,2048,256]{2,1,0:T(8,128)(2,1)} %param.37) | copy-start | bytes 3145732
  8.5 47.6 %copy-start.3 = (bf16[1,2048,256]{2,1,0:T(8,128)(2,1)S(1)}, bf16[1,2048,256]{2,1,0:T(8,128)(2,1)}, u32[]{:S(2)}) copy-start(bf16[1,2048,256]{2,1,0:T(8,128)(2,1)} %param.38) | copy-start | bytes 3145732
  8.5 1.3 %collective-permute-start = (bf16[16,2048]{1,0:T(8,128)(2,1)S(1)}, bf16[16,2048]{1,0:T(8,128)(2,1)S(1)}, u32[]{:S(2)}, u32[]{:S(2)}) collective-permute-start(bf16[16,2048]{1,0:T(8,128)(2,1)S(1)} %shard_map.211.own_ref), channel_id=1, source_target_pairs={{0,1},{1,0},{2,3},{3,2},{4,5},{5,4},{6,7},{7,6},{8,9},{9,8},{10,11... | collective-permute-start | bytes 196616 | tf_op jit(solution)/shard_map/ppermute | solution.py:426
  11.1 21.4 %all-to-all-start = ((bf16[8,16,1152]{2,1,0:T(8,128)(2,1)}), bf16[8,16,1152]{2,1,0:T(8,128)(2,1)S(1)}, u32[]{:S(2)}, u32[]{:S(2)}) async-start(bf16[8,16,1152]{2,1,0:T(8,128)(2,1)} %get-tuple-element.14), calls=%async_computation | async-start | bytes 589824 | tf_op jit(solution)/shard_map/all_to_all | solution.py:449
  55.6 3.1 %copy-start.1 = (bf16[1,256,2048]{2,1,0:T(8,128)(2,1)S(1)}, bf16[1,256,2048]{2,1,0:T(8,128)(2,1)}, u32[]{:S(2)}) copy-start(bf16[1,256,2048]{2,1,0:T(8,128)(2,1)} %param.39) | copy-start | bytes 3145732
  55.6 3.1 %collective-permute-start.1 = (bf16[16,32,1024]{2,1,0:T(8,128)(2,1)S(1)}, bf16[16,32,1024]{2,1,0:T(8,128)(2,1)S(1)}, u32[]{:S(2)}, u32[]{:S(2)}) collective-permute-start(bf16[16,32,1024]{2,1,0:T(8,128)(2,1)S(1)} %all_to_all.20.slots_ref.own_ref), channel_id=1, source_target_pairs={{0,1},{1,0},{2,3},{3,2},{4,5},{5,4},{6,7},{7,6},{8,9},{9,8},{10,11... | collective-permute-start | bytes 3145736 | tf_op jit(solution)/shard_map/ppermute | solution.py:462
  55.6 3.1 %collective-permute-start.2 = (bf16[8,16,1152]{2,1,0:T(8,128)(2,1)S(1)}, bf16[8,16,1152]{2,1,0:T(8,128)(2,1)S(1)}, u32[]{:S(2)}, u32[]{:S(2)}) collective-permute-start(bf16[8,16,1152]{2,1,0:T(8,128)(2,1)S(1)} %all-to-all-done.got_ref.line_ref), channel_id=1, source_target_pairs={{0,1},{1,0},{2,3},{3,2},{4,5},{5,4},{6,7},{7,6},{8,9},{9,8},{10,11... | collective-permute-start | bytes 884744 | tf_op jit(solution)/shard_map/ppermute | solution.py:450
  59.5 2.4 %collective-permute-start.3 = (bf16[384,1024]{1,0:T(8,128)(2,1)S(1)}, bf16[384,1024]{1,0:T(8,128)(2,1)S(1)}, u32[]{:S(2)}, u32[]{:S(2)}) collective-permute-start(bf16[384,1024]{1,0:T(8,128)(2,1)S(1)} %get-tuple-element.21), channel_id=1, source_target_pairs={{0,1},{1,0},{2,3},{3,2},{4,5},{5,4},{6,7},{7,6},{8,9},{9,8},{10,11... | collective-permute-start | bytes 2359304 | tf_op jit(solution)/shard_map/ppermute | solution.py:480
  62.9 20.2 %copy-start.13 = (f32[2048]{0:T(1024)S(1)}, f32[2048]{0:T(1024)}, u32[]{:S(2)}) copy-start(f32[2048]{0:T(1024)} %param.22) | copy-start | bytes 24580
  62.9 15.8 %all-to-all-start.2 = ((bf16[16,16,1024]{2,1,0:T(8,128)(2,1)}), bf16[16,16,1024]{2,1,0:T(8,128)(2,1)S(1)}, u32[]{:S(2)}, u32[]{:S(2)}) async-start(bf16[16,16,1024]{2,1,0:T(8,128)(2,1)} %bitcast.28), calls=%async_computation.2 | async-start | bytes 1048576 | tf_op jit(solution)/shard_map/all_to_all | solution.py:483
  79.7 14.6 %all-to-all-start.3 = ((bf16[8,16,1024]{2,1,0:T(8,128)(2,1)}), bf16[8,16,1024]{2,1,0:T(8,128)(2,1)S(1)}, u32[]{:S(2)}, u32[]{:S(2)}) async-start(bf16[8,16,1024]{2,1,0:T(8,128)(2,1)} %shard_map.217), calls=%async_computation.3 | async-start | bytes 524288 | tf_op jit(solution)/shard_map/all_to_all | solution.py:491

commit v3 on v2

--- a/solution.py
+++ b/solution.py
@@ -167,6 +167,7 @@
     in_specs = [pl.BlockSpec(memory_space=pltpu.SMEM)] * smem_count
     in_specs += [pl.BlockSpec(memory_space=pltpu.VMEM)] * (len(inputs) - smem_count - hbm_count)
     in_specs += [pl.BlockSpec(memory_space=pltpu.HBM)] * hbm_count
+    held = [pltpu.with_memory_space_constraint(x, pltpu.HBM) for x in inputs[len(inputs) - hbm_count :]]
     return pl.pallas_call(
         kernel,
         out_shape=out_shape,
@@ -174,11 +175,12 @@
         out_specs=jax.tree.map(lambda _: pl.BlockSpec(memory_space=pltpu.VMEM), out_shape),
         scratch_shapes=scratch,
         compiler_params=pltpu.CompilerParams(vmem_limit_bytes=limit * 1024 * 1024),
-    )(*inputs)
+    )(*inputs[: len(inputs) - hbm_count], *held)
 
 
 def rows_kernel(
     core_ref,
+    line_ref,
     tokens_ref,
     own_ref,
     other_ref,
@@ -240,7 +242,8 @@
 
 def slots_kernel(line_ref, got_ref, send_ref, combine_ref):
     lines, seq_count, width = got_ref.shape
-    places, _, half = send_ref.shape
+    places = send_ref.shape[0]
+    half = width - 128
     token_total = lines * seq_count
     capacity = seq_count
     slot_total = places * capacity
@@ -266,39 +269,50 @@
     )
     chosen = jnp.where(here, hit, 0.0)
     rows = jnp.dot(chosen.astype(BF16), got[:, :half], preferred_element_type=F32)
-    send_ref[:, :capacity, :] = rows.astype(BF16).reshape(places, capacity, half)
-    for line in range(lines):
-        block = got_ref[line, :, half:]
-        send_ref[:, capacity:, line * 128 : line * 128 + 128] = jnp.broadcast_to(
-            block[None], (places, seq_count, 128)
-        )
+    send_ref[:, :, :half] = rows.astype(BF16).reshape(places, capacity, half)
+    group = (lax.broadcasted_iota(jnp.int32, (seq_count, 128), 1)) // 32
+    for n in range(3):
+        for first in range(0, lines, 4):
+            tile = jnp.zeros((seq_count, 128), F32)
+            for k in range(4):
+                block = got[(first + k) * seq_count : (first + k + 1) * seq_count, half:].astype(F32)
+                moved = pltpu.roll(block, (k * 32 - DENSE - n * 32) % 128, 1)
+                tile = jnp.where(group == k, moved, tile)
+            at = half + (n * lines + first) * 32
+            send_ref[:, :, at : at + 128] = jnp.broadcast_to(tile.astype(BF16)[None], (places, seq_count, 128))
     weights = jnp.where(here, gate * hit, 0.0).T
     high = weights.astype(BF16)
     combine_ref[:, :slot_total] = high
     combine_ref[:, slot_total:] = (weights - high.astype(F32)).astype(BF16)
 
 
-def dense_weights(slots_ref, side, at):
-    places, rows, _ = slots_ref.shape
-    capacity = rows // 2
-    lane = pl.multiple_of((side * 4 + at) * 128, 128)
-    return slots_ref[:, capacity:, pl.ds(lane, 128)].reshape(places * capacity, 128)
+def dense_weights(slots_ref, half, part, line):
+    lanes = 32 * 8
+    at = pl.multiple_of(half + part * lanes + line // 4 * 128, 128)
+    return slots_ref[:, :, pl.ds(at, 128)].reshape(-1, 128)
+
+
+def lane_group(shape):
+    return lax.broadcasted_iota(jnp.int32, shape, 1) // 32
 
 
 def half_products(side, slots_ref, line_ref, gate_ref, up_ref, dense_ref):
-    places, rows, half = slots_ref.shape
+    half = line_ref.shape[2] - 128
     mine = pl.ds(pl.multiple_of(side * half, half), half)
-    values = slots_ref[:, : rows // 2, :].reshape(places * rows // 2, half)
+    values = slots_ref[:, :, :half].reshape(-1, half)
     gate = jnp.dot(values, gate_ref[mine, :], preferred_element_type=F32)
     up = jnp.dot(values, up_ref[mine, :], preferred_element_type=F32)
-    line = line_ref[:, :, :half].reshape(-1, half)
+    rows = line_ref[:, :, :half].reshape(-1, half)
     block = half // 4
-    dense = sum(
-        jnp.dot(
-            line[:, k * block : (k + 1) * block], dense_weights(dense_ref, side, k), preferred_element_type=F32
-        )
-        for k in range(4)
-    )
+    group = lane_group((rows.shape[0], 128))
+    dense = []
+    for part in range(2):
+        weights = dense_weights(dense_ref, half, part, side * 4)
+        total = jnp.zeros(group.shape, F32)
+        for k in range(4):
+            product = jnp.dot(rows[:, k * block : (k + 1) * block], weights, preferred_element_type=F32)
+            total += jnp.where(group == k, product, 0.0)
+        dense.append(total)
     return gate, up, dense
 
 
@@ -306,7 +320,8 @@
     gate, up, dense = half_products(core_ref[0], slots_ref, line_ref, gate_ref, up_ref, slots_ref)
     gate_out[...] = gate
     up_out[...] = up
-    dense_out[...] = dense
+    for n, values in enumerate(dense):
+        dense_out[n] = values
 
 
 def down_products(side, hidden, dense, down_ref, dense_ref, target_ref):
@@ -314,9 +329,14 @@
     mine = pl.ds(pl.multiple_of(side * half, half), half)
     target_ref[:slot_total, :] = jnp.dot(hidden, down_ref[:, mine], preferred_element_type=F32).astype(BF16)
     block = half // 4
+    weights = dense_weights(dense_ref, half, 2, side * 4)
+    group = lane_group(dense.shape)
     for k in range(4):
         target_ref[slot_total:, k * block : (k + 1) * block] = lax.dot_general(
-            dense, dense_weights(dense_ref, side, k), (((1,), (1,)), ((), ())), preferred_element_type=F32
+            jnp.where(group == k, dense, 0.0).astype(BF16),
+            weights,
+            (((1,), (1,)), ((), ())),
+            preferred_element_type=F32,
         ).astype(BF16)
 
 
@@ -338,16 +358,37 @@
     side = 1 - core_ref[0]
     gate, up, dense = half_products(side, other_ref, line_ref, gate_ref, up_ref, own_ref)
     hidden = (jax.nn.silu(gate_sum[...] + gate) * (up_sum[...] + up)).astype(BF16)
-    dense += dense_sum[...]
-    lane = lax.broadcasted_iota(jnp.int32, dense.shape, 1)
-    dense = jnp.where(lane >= 96, jax.nn.silu(pltpu.roll(dense, 64, 1)) * pltpu.roll(dense, 32, 1), 0.0).astype(BF16)
+    sums = []
+    for n, values in enumerate(dense):
+        total = values + dense_sum[n]
+        total += pltpu.roll(total, 64, 1)
+        sums.append(total + pltpu.roll(total, 32, 1))
+    dense = (jax.nn.silu(sums[0]) * sums[1]).astype(BF16)
     hidden_ref[...] = hidden
     dense_ref[...] = dense
-    down_products(side, hidden, dense, down_ref, own_ref, send_ref)
-
-
-def keep_kernel(core_ref, hidden_ref, dense_ref, own_ref, down_ref, keep_ref):
-    down_products(core_ref[0], hidden_ref[...], dense_ref[...], down_ref, own_ref, keep_ref)
+    down_products(side, hidden, dense.astype(F32), down_ref, own_ref, send_ref)
+
+
+def keep_kernel(
+    core_ref,
+    hidden_ref,
+    dense_ref,
+    own_ref,
+    down_ref,
+    tokens_ref,
+    gain_ref,
+    key_ref,
+    value_ref,
+    keep_ref,
+    keys_ref,
+    values_ref,
+):
+    down_products(core_ref[0], hidden_ref[...], dense_ref[...].astype(F32), down_ref, own_ref, keep_ref)
+    normed = rms_scale(tokens_ref[...], gain_ref[...]).astype(BF16)
+    for weight_ref, target_ref in ((key_ref, keys_ref), (value_ref, values_ref)):
+        target_ref[...] = lax.dot_general(
+            normed, weight_ref[...], (((1,), (1,)), ((), ())), preferred_element_type=F32
+        ).astype(BF16)
 
 
 def combine_kernel(back_ref, combine_ref, line_ref, keep_ref, got_ref, send_ref):
@@ -409,7 +450,7 @@
             value_cache.reshape(cache_rows, cache_len),
             w_attn_out,
         ),
-        52,
+        24,
         hbm_count=8,
         scratch=(
             pltpu.VMEM((1, head_bias.shape[0]), F32),
@@ -430,9 +471,10 @@
             jax.ShapeDtypeStruct((lines, seq_count, half + 128), BF16),
             jax.ShapeDtypeStruct((seq_count, half), BF16),
         ),
-        1,
+        2,
         (
             core,
+            line,
             tokens,
             attn_own,
             attn_other,
@@ -451,7 +493,7 @@
     slot_send, combine = call(
         slots_kernel,
         (
-            jax.ShapeDtypeStruct((places, 2 * seq_count, half), BF16),
+            jax.ShapeDtypeStruct((places, seq_count, half + 96 * lines), BF16),
             jax.ShapeDtypeStruct((token_total, 2 * slot_total), BF16),
         ),
         1,
@@ -464,7 +506,7 @@
     hidden_shape = (slot_total, w_expert_gate.shape[2])
     sums = call(
         own_kernel,
-        (jax.ShapeDtypeStruct(hidden_shape, F32),) * 2 + (jax.ShapeDtypeStruct((token_total, 128), F32),),
+        (jax.ShapeDtypeStruct(hidden_shape, F32),) * 2 + (jax.ShapeDtypeStruct((2, token_total, 128), F32),),
         1,
         (core, slot_own, line_own, *weights),
         8,
@@ -478,7 +520,24 @@
         12,
     )
     got = lax.ppermute(send, "tp", SWAP)
-    keep = call(keep_kernel, both_shape, 1, (core, hidden, dense, slot_own, w_expert_down[0]), 8)
+    new_shape = jax.ShapeDtypeStruct((seq_count, w_key.shape[1]), BF16)
+    keep, new_keys, new_values = call(
+        keep_kernel,
+        (both_shape, new_shape, new_shape),
+        1,
+        (
+            core,
+            hidden,
+            dense,
+            slot_own,
+            w_expert_down[0],
+            tokens,
+            attn_gain.reshape(1, width),
+            w_key.T,
+            w_value.T,
+        ),
+        8,
+    )
     results = (keep[:slot_total].astype(F32) + got[:slot_total].astype(F32)).astype(BF16)
     back = lax.all_to_all(results.reshape(places, seq_count, half), PLANE, 0, 0, tiled=True)
     partial = call(
@@ -490,9 +549,6 @@
     )
     parts = lax.all_to_all(partial, LINE, 0, 0, tiled=True)
     layer_out = (residual.astype(F32) + jnp.sum(parts.astype(F32), axis=0)).astype(BF16)
-    normed = rms_scale(tokens, attn_gain).astype(BF16)
-    new_keys = jnp.dot(normed, w_key, preferred_element_type=F32).astype(BF16)
-    new_values = jnp.dot(normed, w_value, preferred_element_type=F32).astype(BF16)
     return (layer_out, new_keys, new_values)
 
 

time: 95.6 us -> 86.3 us (0.903)
  blocking collectives: 22.6 us -> 70.5 us
  waiting for transfers between devices: 37.1 us -> 3.99 us
  starting transfers between devices: 17.7 us -> 0.82 us
  local copies, waits for them, and re-layouts: 3.03 us -> 0.15 us
  matrix products: 2.62 us -> 0 us
    all_to_all x0 -> x3, blocking collectives: none -> 49.4 us  [the longest x1 21.2 us: shards(): line_own = lax.all_to_all(line_send, LINE, 0, 0, tiled=True)]
    all_to_all x3 -> x0, waiting for transfers between devices: 32.2 us -> none  [the longest x1 12.9 us: shards(): line_own = lax.all_to_all(line_send, LINE, 0, 0, tiled=True)]
    all_to_all x3 -> x0, starting transfers between devices: 16.8 us -> none  [the longest x1 8.47 us: shards(): line_own = lax.all_to_all(line_send, LINE, 0, 0, tiled=True)]
    unnamed x35 -> x29, local copies, waits for them, and re-layouts: 3.03 us -> 0.15 us
    dot_general x2 -> x0, matrix products: 2.62 us -> none  [the longest x1 1.78 us: shards(): new_keys = jnp.dot(normed, w_key, preferred_element_type=F32).astype(BF16)]
    all_to_all x1, blocking collectives: 22.6 us -> 21.1 us  [shards(): slot_own = lax.all_to_all(slot_send, PLANE, 0, 0, tiled=True)]
  transfers between devices with their start and end apart: 7 -> 4, of which waited for: 6 -> 3; matrix products, arithmetic and copies ran while one was open for 3% -> 0% of each run, Pallas kernels for 1% -> 2%
where the time goes in v3:
time: 86.3 us; the launch traced here: 86 us
  blocking collectives  70.5 us (82%)
  Pallas kernels  8.85 us (10%)
  waiting for transfers between devices  3.99 us (5%)
    all_to_all x1, blocking collectives, shards(): line_own = lax.all_to_all(line_send, LINE, 0, 0, tiled=True)  21.2 us
    all_to_all x1, blocking collectives, shards(): slot_own = lax.all_to_all(slot_send, PLANE, 0, 0, tiled=True)  21.1 us
    all_to_all x1, blocking collectives, shards(): lax.all_to_all(results.reshape(places, seq_count, half), PLANE, 0, 0, til...  14.7 us
    all_to_all x1, blocking collectives, shards(): parts = lax.all_to_all(partial, LINE, 0, 0, tiled=True)  13.6 us
    pallas_call x7, Pallas kernels, call(): pl.pallas_call(kernel, out_shape=out_shape, in_specs=in_specs, out_specs=...  8.85 us
    ppermute x1, waiting for transfers between devices, shards(): line_other = lax.ppermute(line_own, 'tp', SWAP)  1.8 us
  transfers between devices with their start and end apart: 4, of which 3 were waited for; matrix products, arithmetic and copies ran while one was open for 0% of the time, Pallas kernels for 2%

profile of v3, /device:TPU:2, one launch (start us, length us, event | category | flops | bytes accessed | tf_op | source)
XLA Modules:
  0.0 86.0 jit_solution(17358431205978047823)
XLA Ops:
  0.6 0.0 copy-start.13
  0.6 0.0 copy-start.3
  0.7 0.0 copy-start.4
  0.7 5.0 %shard_map.211.own_ref = bf16[16,2048]{1,0:T(8,128)(2,1)S(1)} custom-call(f32[1,8]{1,0:T(1,128)} %bitcast.32, s32[1,16]{1,0:T(1,128)} %bitcast.33, bf16[16,2048]{1,0:T(8,128)(2,1)} %tokens_ref.3, f32[1,2048]{1,0:T(1,128)} %bitcast.24, bf16[2048,512]{1,0:T(8,128)(2,1)} %query_hbm.1, bf16[1024,1024]{1,0:T(8,128)(2,1)} %bitcast.30, ...), custom_call_target="tpu_custom_call" | custom-call | tf_op jit(solution)/shard_map/pallas_call | solution.py:171
  5.7 0.0 copy-start
  5.8 0.0 copy-start.1
  5.8 0.1 collective-permute-start
  5.9 0.1 copy.23.routes_ref
  6.0 1.1 %collective-permute-done.other_ref = bf16[16,2048]{1,0:T(8,128)(2,1)S(1)} collective-permute-done((bf16[16,2048]{1,0:T(8,128)(2,1)S(1)}, bf16[16,2048]{1,0:T(8,128)(2,1)S(1)}, u32[]{:S(2)}, u32[]{:S(2)}) %collective-permute-start) | collective-permute-done | bytes 65568 | tf_op jit(solution)/shard_map/ppermute | solution.py:467
  7.1 0.0 copy-done.4
  7.2 0.4 shard_map.212
  7.6 21.2 %all_to_all.20.got_ref.line_ref = bf16[8,16,1152]{2,1,0:T(8,128)(2,1)S(1)} all-to-all(bf16[8,16,1152]{2,1,0:T(8,128)(2,1)S(1)} %get-tuple-element.17), channel_id=1, replica_groups=mesh['ep_0'=8,'ep_1'=4,'ep_2'=4,'tp'=2] {'ep_0'}, dimensions={0} | all-to-all | bytes 589824 | tf_op jit(solution)/shard_map/all_to_all | solution.py:491
  28.8 0.5 shard_map.213
  29.3 21.1 %all_to_all.21.slots_ref.own_ref = bf16[16,16,1792]{2,1,0:T(8,128)(2,1)S(1)} all-to-all(bf16[16,16,1792]{2,1,0:T(8,128)(2,1)S(1)} %get-tuple-element.18), channel_id=1, replica_groups=mesh['ep_0'=8,'ep_1'=4,'ep_2'=4,'tp'=2] {'ep_1','ep_2'}, dimensions={0} | all-to-all | bytes 1835008 | tf_op jit(solution)/shard_map/all_to_all | solution.py:503
  50.4 0.0 collective-permute-start.1
  50.4 0.5 collective-permute-start.2
  50.9 0.6 shard_map.214
  51.5 1.8 %collective-permute-done.2.line_ref = bf16[8,16,1152]{2,1,0:T(8,128)(2,1)S(1)} collective-permute-done((bf16[8,16,1152]{2,1,0:T(8,128)(2,1)S(1)}, bf16[8,16,1152]{2,1,0:T(8,128)(2,1)S(1)}, u32[]{:S(2)}, u32[]{:S(2)}) %collective-permute-start.2) | collective-permute-done | bytes 294944 | tf_op jit(solution)/shard_map/ppermute | solution.py:492
  53.3 0.0 collective-permute-done.1.other_ref
  53.3 0.0 copy-done.2
  53.3 0.0 copy-start.6
  53.3 0.0 copy-start.7
  53.3 0.9 %shard_map.215 = (bf16[384,1024]{1,0:T(8,128)(2,1)S(1)}, bf16[256,256]{1,0:T(8,128)(2,1)S(1)}, bf16[128,128]{1,0:T(8,128)(2,1)S(1)}) custom-call(s32[1]{0:T(128)} %bitcast.core_ref, f32[256,256]{1,0:T(8,128)S(1)} %get-tuple-element.19.gate_sum, f32[256,256]{1,0:T(8,128)S(1)} %get-tuple-element.20.up_sum, f32[2,128,128]{2,1,0:T(8,128)S(1)} %get-tuple-element.21.dense_sum, ...), custom_call_target="tpu_custom_call" | custom-call | tf_op jit(solution)/shard_map/pallas_call | solution.py:171
  54.2 0.2 collective-permute-start.3
  54.4 0.0 copy-done.6
  54.4 1.1 %shard_map.216 = (bf16[384,1024]{1,0:T(8,128)(2,1)S(1)}, bf16[16,64]{1,0:T(8,128)(2,1)}, bf16[16,64]{1,0:T(8,128)(2,1)}) custom-call(s32[1]{0:T(128)} %bitcast.core_ref, bf16[256,256]{1,0:T(8,128)(2,1)S(1)} %get-tuple-element.22.hidden_ref, bf16[128,128]{1,0:T(8,128)(2,1)S(1)} %get-tuple-element.23.dense_ref, ...), custom_call_target="tpu_custom_call" | custom-call | tf_op jit(solution)/shard_map/pallas_call | solution.py:171
  55.5 1.0 %collective-permute-done.3.got_ref = bf16[384,1024]{1,0:T(8,128)(2,1)S(1)} collective-permute-done((bf16[384,1024]{1,0:T(8,128)(2,1)S(1)}, bf16[384,1024]{1,0:T(8,128)(2,1)S(1)}, u32[]{:S(2)}, u32[]{:S(2)}) %collective-permute-start.3) | collective-permute-done | bytes 786464 | tf_op jit(solution)/shard_map/ppermute | solution.py:522
  56.6 0.2 add_convert_fusion
  56.8 14.7 %all_to_all.22.back_ref = bf16[16,16,1024]{2,1,0:T(8,128)(2,1)S(1)} all-to-all(bf16[16,16,1024]{2,1,0:T(8,128)(2,1)S(1)} %bitcast.29), channel_id=1, replica_groups=mesh['ep_0'=8,'ep_1'=4,'ep_2'=4,'tp'=2] {'ep_1','ep_2'}, dimensions={0} | all-to-all | bytes 1048576 | tf_op jit(solution)/shard_map/all_to_all | solution.py:542
  71.5 0.3 shard_map.217
  71.8 13.6 %all_to_all.23 = bf16[8,16,1024]{2,1,0:T(8,128)(2,1)S(1)} all-to-all(bf16[8,16,1024]{2,1,0:T(8,128)(2,1)S(1)} %shard_map.217), channel_id=1, replica_groups=mesh['ep_0'=8,'ep_1'=4,'ep_2'=4,'tp'=2] {'ep_0'}, dimensions={0} | all-to-all | bytes 524288 | tf_op jit(solution)/shard_map/all_to_all | solution.py:550
  85.4 0.6 add_convert_fusion.1
  (19 shorter events, 0.1 us)
Async XLA Ops:
  0.6 5.2 %copy-start.13 = (s32[16,6]{0,1:T(8,128)S(1)}, s32[16,6]{0,1:T(8,128)}, u32[]{:S(2)}) copy-start(s32[16,6]{0,1:T(8,128)} %param.32) | copy-start | bytes 1156
  0.6 6.5 %copy-start.3 = (bf16[16,2048]{1,0:T(8,128)(2,1)S(1)}, bf16[16,2048]{1,0:T(8,128)(2,1)}, u32[]{:S(2)}) copy-start(bf16[16,2048]{1,0:T(8,128)(2,1)} %tokens_ref.3) | copy-start | bytes 196612
  0.7 6.5 %copy-start.4 = (bf16[2048,128]{1,0:T(8,128)(2,1)S(1)}, bf16[2048,128]{1,0:T(8,128)(2,1)}, u32[]{:S(2)}) copy-start(bf16[2048,128]{1,0:T(8,128)(2,1)} %router_ref.1) | copy-start | bytes 1572868
  0.7 6.4 %copy-start.8 = (f32[2048]{0:T(1024)S(1)}, f32[2048]{0:T(1024)}, u32[]{:S(2)}) copy-start(f32[2048]{0:T(1024)} %param.30) | copy-start | bytes 24580
  0.7 6.4 %copy-start.9 = (bf16[16,256]{1,0:T(8,128)(2,1)S(1)}, bf16[16,256]{1,0:T(8,128)(2,1)}, u32[]{:S(2)}) copy-start(bf16[16,256]{1,0:T(8,128)(2,1)} %gate_ref.1) | copy-start | bytes 24580
  0.7 6.4 %copy-start.10 = (bf16[16,256]{1,0:T(8,128)(2,1)S(1)}, bf16[16,256]{1,0:T(8,128)(2,1)}, u32[]{:S(2)}) copy-start(bf16[16,256]{1,0:T(8,128)(2,1)} %up_ref.1) | copy-start | bytes 24580
  0.7 6.4 %copy-start.11 = (bf16[256,16]{0,1:T(8,128)(2,1)S(1)}, bf16[256,16]{0,1:T(8,128)(2,1)}, u32[]{:S(2)}) copy-start(bf16[256,16]{0,1:T(8,128)(2,1)} %param.35) | copy-start | bytes 24580
  0.7 6.4 %copy-start.12 = (f32[2048]{0:T(1024)S(1)}, f32[2048]{0:T(1024)}, u32[]{:S(2)}) copy-start(f32[2048]{0:T(1024)} %param.36) | copy-start | bytes 24580
  5.7 45.2 %copy-start = (bf16[1,2048,256]{2,1,0:T(8,128)(2,1)S(1)}, bf16[1,2048,256]{2,1,0:T(8,128)(2,1)}, u32[]{:S(2)}) copy-start(bf16[1,2048,256]{2,1,0:T(8,128)(2,1)} %param.37) | copy-start | bytes 3145732
  5.8 45.1 %copy-start.1 = (bf16[1,2048,256]{2,1,0:T(8,128)(2,1)S(1)}, bf16[1,2048,256]{2,1,0:T(8,128)(2,1)}, u32[]{:S(2)}) copy-start(bf16[1,2048,256]{2,1,0:T(8,128)(2,1)} %param.38) | copy-start | bytes 3145732
  5.8 1.3 %collective-permute-start = (bf16[16,2048]{1,0:T(8,128)(2,1)S(1)}, bf16[16,2048]{1,0:T(8,128)(2,1)S(1)}, u32[]{:S(2)}, u32[]{:S(2)}) collective-permute-start(bf16[16,2048]{1,0:T(8,128)(2,1)S(1)} %shard_map.211.own_ref), channel_id=1, source_target_pairs={{0,1},{1,0},{2,3},{3,2},{4,5},{5,4},{6,7},{7,6},{8,9},{9,8},{10,11... | collective-permute-start | bytes 196616 | tf_op jit(solution)/shard_map/ppermute | solution.py:467
  50.4 2.9 %copy-start.2 = (bf16[1,256,2048]{2,1,0:T(8,128)(2,1)S(1)}, bf16[1,256,2048]{2,1,0:T(8,128)(2,1)}, u32[]{:S(2)}) copy-start(bf16[1,256,2048]{2,1,0:T(8,128)(2,1)} %param.39) | copy-start | bytes 3145732
  50.4 2.9 %collective-permute-start.1 = (bf16[16,16,1792]{2,1,0:T(8,128)(2,1)S(1)}, bf16[16,16,1792]{2,1,0:T(8,128)(2,1)S(1)}, u32[]{:S(2)}, u32[]{:S(2)}) collective-permute-start(bf16[16,16,1792]{2,1,0:T(8,128)(2,1)S(1)} %all_to_all.21.slots_ref.own_ref), channel_id=1, source_target_pairs={{0,1},{1,0},{2,3},{3,2},{4,5},{5,4},{6,7},{7,6},{8,9},{9,8},{10,11... | collective-permute-start | bytes 2752520 | tf_op jit(solution)/shard_map/ppermute | solution.py:504
  50.4 2.9 %collective-permute-start.2 = (bf16[8,16,1152]{2,1,0:T(8,128)(2,1)S(1)}, bf16[8,16,1152]{2,1,0:T(8,128)(2,1)S(1)}, u32[]{:S(2)}, u32[]{:S(2)}) collective-permute-start(bf16[8,16,1152]{2,1,0:T(8,128)(2,1)S(1)} %all_to_all.20.got_ref.line_ref), channel_id=1, source_target_pairs={{0,1},{1,0},{2,3},{3,2},{4,5},{5,4},{6,7},{7,6},{8,9},{9,8},{10,11... | collective-permute-start | bytes 884744 | tf_op jit(solution)/shard_map/ppermute | solution.py:492
  53.3 1.2 %copy-start.5 = (bf16[2048,64]{0,1:T(8,128)(2,1)S(1)}, bf16[2048,64]{0,1:T(8,128)(2,1)}, u32[]{:S(2)}) copy-start(bf16[2048,64]{0,1:T(8,128)(2,1)} %param.24) | copy-start | bytes 786436
  53.3 1.2 %copy-start.6 = (bf16[2048,64]{0,1:T(8,128)(2,1)S(1)}, bf16[2048,64]{0,1:T(8,128)(2,1)}, u32[]{:S(2)}) copy-start(bf16[2048,64]{0,1:T(8,128)(2,1)} %param.25) | copy-start | bytes 786436
  53.3 1.1 %copy-start.7 = (f32[2048]{0:T(1024)S(1)}, f32[2048]{0:T(1024)}, u32[]{:S(2)}) copy-start(f32[2048]{0:T(1024)} %param.22) | copy-start | bytes 24580
  54.2 2.4 %collective-permute-start.3 = (bf16[384,1024]{1,0:T(8,128)(2,1)S(1)}, bf16[384,1024]{1,0:T(8,128)(2,1)S(1)}, u32[]{:S(2)}, u32[]{:S(2)}) collective-permute-start(bf16[384,1024]{1,0:T(8,128)(2,1)S(1)} %get-tuple-element.25), channel_id=1, source_target_pairs={{0,1},{1,0},{2,3},{3,2},{4,5},{5,4},{6,7},{7,6},{8,9},{9,8},{10,11... | collective-permute-start | bytes 2359304 | tf_op jit(solution)/shard_map/ppermute | solution.py:522

commit v4 on v3

--- a/solution.py
+++ b/solution.py
@@ -324,15 +324,15 @@
         dense_out[n] = values
 
 
-def down_products(side, hidden, dense, down_ref, dense_ref, target_ref):
-    slot_total, half = hidden.shape[0], target_ref.shape[1]
+def down_products(side, hidden, dense, down_ref, dense_ref, target_ref, line_target):
+    half = target_ref.shape[1]
     mine = pl.ds(pl.multiple_of(side * half, half), half)
-    target_ref[:slot_total, :] = jnp.dot(hidden, down_ref[:, mine], preferred_element_type=F32).astype(BF16)
+    target_ref[...] = jnp.dot(hidden, down_ref[:, mine], preferred_element_type=F32).astype(BF16)
     block = half // 4
     weights = dense_weights(dense_ref, half, 2, side * 4)
     group = lane_group(dense.shape)
     for k in range(4):
-        target_ref[slot_total:, k * block : (k + 1) * block] = lax.dot_general(
+        line_target[:, k * block : (k + 1) * block] = lax.dot_general(
             jnp.where(group == k, dense, 0.0).astype(BF16),
             weights,
             (((1,), (1,)), ((), ())),
@@ -352,6 +352,7 @@
     up_ref,
     down_ref,
     send_ref,
+    line_send_ref,
     hidden_ref,
     dense_ref,
 ):
@@ -366,7 +367,7 @@
     dense = (jax.nn.silu(sums[0]) * sums[1]).astype(BF16)
     hidden_ref[...] = hidden
     dense_ref[...] = dense
-    down_products(side, hidden, dense.astype(F32), down_ref, own_ref, send_ref)
+    down_products(side, hidden, dense.astype(F32), down_ref, own_ref, send_ref, line_send_ref)
 
 
 def keep_kernel(
@@ -380,10 +381,11 @@
     key_ref,
     value_ref,
     keep_ref,
+    line_keep_ref,
     keys_ref,
     values_ref,
 ):
-    down_products(core_ref[0], hidden_ref[...], dense_ref[...].astype(F32), down_ref, own_ref, keep_ref)
+    down_products(core_ref[0], hidden_ref[...], dense_ref[...].astype(F32), down_ref, own_ref, keep_ref, line_keep_ref)
     normed = rms_scale(tokens_ref[...], gain_ref[...]).astype(BF16)
     for weight_ref, target_ref in ((key_ref, keys_ref), (value_ref, values_ref)):
         target_ref[...] = lax.dot_general(
@@ -391,7 +393,7 @@
         ).astype(BF16)
 
 
-def combine_kernel(back_ref, combine_ref, line_ref, keep_ref, got_ref, send_ref):
+def combine_kernel(back_ref, combine_ref, line_ref, line_keep_ref, line_got_ref, send_ref):
     lines, seq_count, half = send_ref.shape
     token_total = lines * seq_count
     slot_total = back_ref.shape[0] * back_ref.shape[1]
@@ -400,8 +402,15 @@
     routed += jnp.dot(combine_ref[:, slot_total:], back, preferred_element_type=F32)
     meta = line_ref[...].reshape(token_total, line_ref.shape[2])[:, half:].astype(F32)
     mix = meta[:, MIX_HI : MIX_HI + 1] + meta[:, MIX_LO : MIX_LO + 1]
-    dense = keep_ref[slot_total:, :].astype(F32) + got_ref[slot_total:, :].astype(F32)
+    dense = line_keep_ref[...].astype(F32) + line_got_ref[...].astype(F32)
     send_ref[...] = (routed + mix * dense).astype(BF16).reshape(lines, seq_count, half)
+
+
+def finish_kernel(residual_ref, parts_ref, out_ref):
+    total = parts_ref[0].astype(F32)
+    for n in range(1, parts_ref.shape[0]):
+        total += parts_ref[n].astype(F32)
+    out_ref[...] = (residual_ref[...].astype(F32) + total).astype(BF16)
 
 
 def shards(
@@ -511,19 +520,23 @@
         (core, slot_own, line_own, *weights),
         8,
     )
-    both_shape = jax.ShapeDtypeStruct((slot_total + token_total, half), BF16)
-    send, hidden, dense = call(
+    both_shape = (
+        jax.ShapeDtypeStruct((slot_total, half), BF16),
+        jax.ShapeDtypeStruct((token_total, half), BF16),
+    )
+    send, dense_send, hidden, dense = call(
         other_kernel,
-        (both_shape, jax.ShapeDtypeStruct(hidden_shape, BF16), jax.ShapeDtypeStruct((token_total, 128), BF16)),
+        (*both_shape, jax.ShapeDtypeStruct(hidden_shape, BF16), jax.ShapeDtypeStruct((token_total, 128), BF16)),
         1,
         (core, *sums, slot_own, slot_other, line_other, *weights, w_expert_down[0]),
         12,
     )
     got = lax.ppermute(send, "tp", SWAP)
+    dense_got = lax.ppermute(dense_send, "tp", SWAP)
     new_shape = jax.ShapeDtypeStruct((seq_count, w_key.shape[1]), BF16)
-    keep, new_keys, new_values = call(
+    keep, dense_keep, new_keys, new_values = call(
         keep_kernel,
-        (both_shape, new_shape, new_shape),
+        (*both_shape, new_shape, new_shape),
         1,
         (
             core,
@@ -538,17 +551,18 @@
         ),
         8,
     )
-    results = (keep[:slot_total].astype(F32) + got[:slot_total].astype(F32)).astype(BF16)
+    results = (keep.astype(F32) + got.astype(F32)).astype(BF16)
+    results, dense_got = lax.optimization_barrier((results, dense_got))
     back = lax.all_to_all(results.reshape(places, seq_count, half), PLANE, 0, 0, tiled=True)
     partial = call(
         combine_kernel,
         jax.ShapeDtypeStruct((lines, seq_count, half), BF16),
         0,
-        (back, combine, line_own, keep, got),
+        (back, combine, line_own, dense_keep, dense_got),
         8,
     )
     parts = lax.all_to_all(partial, LINE, 0, 0, tiled=True)
-    layer_out = (residual.astype(F32) + jnp.sum(parts.astype(F32), axis=0)).astype(BF16)
+    layer_out = call(finish_kernel, jax.ShapeDtypeStruct((seq_count, half), BF16), 0, (residual, parts), 8)
     return (layer_out, new_keys, new_values)
 
 

time: 86.3 us -> 86 us (level)
    pallas_call x7 -> x8, Pallas kernels: 8.85 us -> 9.5 us  [call(): pl.pallas_call(kernel, out_shape=out_shape, in_specs=in_specs, out_specs=...]
  transfers between devices with their start and end apart: 4 -> 5, of which waited for: 3 -> 4; matrix products, arithmetic and copies ran while one was open for 0% -> 0% of each run, Pallas kernels for 2% -> 2%
where the time goes in v4:
time: 86 us; the launch traced here: 85.8 us
  blocking collectives  70.5 us (82%)
  Pallas kernels  9.5 us (11%)
  waiting for transfers between devices  3.41 us (4%)
  starting transfers between devices  1.2 us (1%)
  between operations  0.86 us (1%)
    all_to_all x1, blocking collectives, shards(): line_own = lax.all_to_all(line_send, LINE, 0, 0, tiled=True)  21.2 us
    all_to_all x1, blocking collectives, shards(): slot_own = lax.all_to_all(slot_send, PLANE, 0, 0, tiled=True)  21.1 us
    all_to_all x1, blocking collectives, shards(): lax.all_to_all(results.reshape(places, seq_count, half), PLANE, 0, 0, til...  14.7 us
    all_to_all x1, blocking collectives, shards(): parts = lax.all_to_all(partial, LINE, 0, 0, tiled=True)  13.6 us
    pallas_call x8, Pallas kernels, call(): pl.pallas_call(kernel, out_shape=out_shape, in_specs=in_specs, out_specs=...  9.5 us
    ppermute x1, waiting for transfers between devices, shards(): line_other = lax.ppermute(line_own, 'tp', SWAP)  1.8 us
  transfers between devices with their start and end apart: 5, of which 4 were waited for; matrix products, arithmetic and copies ran while one was open for 0% of the time, Pallas kernels for 2%

profile of v4, /device:TPU:2, one launch (start us, length us, event | category | flops | bytes accessed | tf_op | source)
XLA Modules:
  0.0 85.8 jit_solution(13857221015527025533)
XLA Ops:
  0.6 0.0 copy-start.13
  0.6 0.0 copy-start.3
  0.7 5.0 %shard_map.211.own_ref = bf16[16,2048]{1,0:T(8,128)(2,1)S(1)} custom-call(f32[1,8]{1,0:T(1,128)} %bitcast.32, s32[1,16]{1,0:T(1,128)} %bitcast.33, bf16[16,2048]{1,0:T(8,128)(2,1)} %tokens_ref.3, f32[1,2048]{1,0:T(1,128)} %bitcast.24, bf16[2048,512]{1,0:T(8,128)(2,1)} %query_hbm.1, bf16[1024,1024]{1,0:T(8,128)(2,1)} %bitcast.30, ...), custom_call_target="tpu_custom_call" | custom-call | tf_op jit(solution)/shard_map/pallas_call | solution.py:171
  5.7 0.0 copy-start
  5.8 0.0 copy-start.1
  5.8 0.1 collective-permute-start
  5.9 0.1 copy.23.routes_ref
  6.0 1.1 %collective-permute-done.other_ref = bf16[16,2048]{1,0:T(8,128)(2,1)S(1)} collective-permute-done((bf16[16,2048]{1,0:T(8,128)(2,1)S(1)}, bf16[16,2048]{1,0:T(8,128)(2,1)S(1)}, u32[]{:S(2)}, u32[]{:S(2)}) %collective-permute-start) | collective-permute-done | bytes 65568 | tf_op jit(solution)/shard_map/ppermute | solution.py:476
  7.1 0.0 copy-done.4
  7.2 0.4 shard_map.212
  7.6 21.2 %all_to_all.20.got_ref.line_ref = bf16[8,16,1152]{2,1,0:T(8,128)(2,1)S(1)} all-to-all(bf16[8,16,1152]{2,1,0:T(8,128)(2,1)S(1)} %get-tuple-element.21), channel_id=1, replica_groups=mesh['ep_0'=8,'ep_1'=4,'ep_2'=4,'tp'=2] {'ep_0'}, dimensions={0} | all-to-all | bytes 589824 | tf_op jit(solution)/shard_map/all_to_all | solution.py:500
  28.8 0.5 shard_map.213
  29.3 21.1 %all_to_all.21.slots_ref.own_ref = bf16[16,16,1792]{2,1,0:T(8,128)(2,1)S(1)} all-to-all(bf16[16,16,1792]{2,1,0:T(8,128)(2,1)S(1)} %get-tuple-element.22), channel_id=1, replica_groups=mesh['ep_0'=8,'ep_1'=4,'ep_2'=4,'tp'=2] {'ep_1','ep_2'}, dimensions={0} | all-to-all | bytes 1835008 | tf_op jit(solution)/shard_map/all_to_all | solution.py:512
  50.4 0.0 collective-permute-start.1
  50.4 0.5 collective-permute-start.2
  50.9 0.6 shard_map.214
  51.5 1.8 %collective-permute-done.2.line_ref = bf16[8,16,1152]{2,1,0:T(8,128)(2,1)S(1)} collective-permute-done((bf16[8,16,1152]{2,1,0:T(8,128)(2,1)S(1)}, bf16[8,16,1152]{2,1,0:T(8,128)(2,1)S(1)}, u32[]{:S(2)}, u32[]{:S(2)}) %collective-permute-start.2) | collective-permute-done | bytes 294944 | tf_op jit(solution)/shard_map/ppermute | solution.py:501
  53.3 0.0 collective-permute-done.1.other_ref
  53.3 0.0 copy-done.2
  53.3 0.0 copy-start.6
  53.3 0.0 copy-start.7
  53.3 0.9 %shard_map.215 = (bf16[256,1024]{1,0:T(8,128)(2,1)S(1)}, bf16[128,1024]{1,0:T(8,128)(2,1)S(1)}, bf16[256,256]{1,0:T(8,128)(2,1)S(1)}, bf16[128,128]{1,0:T(8,128)(2,1)S(1)}) custom-call(s32[1]{0:T(128)} %bitcast.core_ref, f32[256,256]{1,0:T(8,128)S(1)} %get-tuple-element.23.gate_sum, f32[256,256]{1,0:T(8,128)S(1)} %get-tuple-element.24.up_sum, ...), custom_call_target="tpu_custom_call" | custom-call | tf_op jit(solution)/shard_map/pallas_call | solution.py:171
  54.2 0.2 collective-permute-start.3
  54.4 0.4 collective-permute-start.4
  54.8 1.1 %shard_map.216 = (bf16[256,1024]{1,0:T(8,128)(2,1)S(1)}, bf16[128,1024]{1,0:T(8,128)(2,1)S(1)}, bf16[16,64]{1,0:T(8,128)(2,1)}, bf16[16,64]{1,0:T(8,128)(2,1)}) custom-call(s32[1]{0:T(128)} %bitcast.core_ref, bf16[256,256]{1,0:T(8,128)(2,1)S(1)} %get-tuple-element.26.hidden_ref, bf16[128,128]{1,0:T(8,128)(2,1)S(1)} %get-tuple-element.27.dense_ref, ...), custom_call_target="tpu_custom_call" | custom-call | tf_op jit(solution)/shard_map/pallas_call | solution.py:171
  55.9 0.3 collective-permute-done.3
  56.2 0.2 add_convert_fusion
  56.4 0.2 collective-permute-done.4.line_got_ref
  56.6 14.7 %all_to_all.22.back_ref = bf16[16,16,1024]{2,1,0:T(8,128)(2,1)S(1)} all-to-all(bf16[16,16,1024]{2,1,0:T(8,128)(2,1)S(1)} %bitcast.29), channel_id=1, replica_groups=mesh['ep_0'=8,'ep_1'=4,'ep_2'=4,'tp'=2] {'ep_1','ep_2'}, dimensions={0} | all-to-all | bytes 1048576 | tf_op jit(solution)/shard_map/all_to_all | solution.py:556
  71.3 0.3 shard_map.217
  71.6 13.6 %all_to_all.23.parts_ref = bf16[8,16,1024]{2,1,0:T(8,128)(2,1)S(1)} all-to-all(bf16[8,16,1024]{2,1,0:T(8,128)(2,1)S(1)} %shard_map.217), channel_id=1, replica_groups=mesh['ep_0'=8,'ep_1'=4,'ep_2'=4,'tp'=2] {'ep_0'}, dimensions={0} | all-to-all | bytes 524288 | tf_op jit(solution)/shard_map/all_to_all | solution.py:564
  85.1 0.7 shard_map.218
  (20 shorter events, 0.0 us)
Async XLA Ops:
  0.6 5.2 %copy-start.13 = (s32[16,6]{0,1:T(8,128)S(1)}, s32[16,6]{0,1:T(8,128)}, u32[]{:S(2)}) copy-start(s32[16,6]{0,1:T(8,128)} %param.32) | copy-start | bytes 1156
  0.6 6.5 %copy-start.3 = (bf16[16,2048]{1,0:T(8,128)(2,1)S(1)}, bf16[16,2048]{1,0:T(8,128)(2,1)}, u32[]{:S(2)}) copy-start(bf16[16,2048]{1,0:T(8,128)(2,1)} %tokens_ref.3) | copy-start | bytes 196612
  0.7 6.5 %copy-start.4 = (bf16[2048,128]{1,0:T(8,128)(2,1)S(1)}, bf16[2048,128]{1,0:T(8,128)(2,1)}, u32[]{:S(2)}) copy-start(bf16[2048,128]{1,0:T(8,128)(2,1)} %router_ref.1) | copy-start | bytes 1572868
  0.7 6.4 %copy-start.8 = (f32[2048]{0:T(1024)S(1)}, f32[2048]{0:T(1024)}, u32[]{:S(2)}) copy-start(f32[2048]{0:T(1024)} %param.30) | copy-start | bytes 24580
  0.7 6.4 %copy-start.9 = (bf16[16,256]{1,0:T(8,128)(2,1)S(1)}, bf16[16,256]{1,0:T(8,128)(2,1)}, u32[]{:S(2)}) copy-start(bf16[16,256]{1,0:T(8,128)(2,1)} %gate_ref.1) | copy-start | bytes 24580
  0.7 6.4 %copy-start.10 = (bf16[16,256]{1,0:T(8,128)(2,1)S(1)}, bf16[16,256]{1,0:T(8,128)(2,1)}, u32[]{:S(2)}) copy-start(bf16[16,256]{1,0:T(8,128)(2,1)} %up_ref.1) | copy-start | bytes 24580
  0.7 6.4 %copy-start.11 = (bf16[256,16]{0,1:T(8,128)(2,1)S(1)}, bf16[256,16]{0,1:T(8,128)(2,1)}, u32[]{:S(2)}) copy-start(bf16[256,16]{0,1:T(8,128)(2,1)} %param.35) | copy-start | bytes 24580
  0.7 6.4 %copy-start.12 = (f32[2048]{0:T(1024)S(1)}, f32[2048]{0:T(1024)}, u32[]{:S(2)}) copy-start(f32[2048]{0:T(1024)} %param.36) | copy-start | bytes 24580
  5.7 45.2 %copy-start = (bf16[1,2048,256]{2,1,0:T(8,128)(2,1)S(1)}, bf16[1,2048,256]{2,1,0:T(8,128)(2,1)}, u32[]{:S(2)}) copy-start(bf16[1,2048,256]{2,1,0:T(8,128)(2,1)} %param.37) | copy-start | bytes 3145732
  5.8 45.1 %copy-start.1 = (bf16[1,2048,256]{2,1,0:T(8,128)(2,1)S(1)}, bf16[1,2048,256]{2,1,0:T(8,128)(2,1)}, u32[]{:S(2)}) copy-start(bf16[1,2048,256]{2,1,0:T(8,128)(2,1)} %param.38) | copy-start | bytes 3145732
  5.8 1.3 %collective-permute-start = (bf16[16,2048]{1,0:T(8,128)(2,1)S(1)}, bf16[16,2048]{1,0:T(8,128)(2,1)S(1)}, u32[]{:S(2)}, u32[]{:S(2)}) collective-permute-start(bf16[16,2048]{1,0:T(8,128)(2,1)S(1)} %shard_map.211.own_ref), channel_id=1, source_target_pairs={{0,1},{1,0},{2,3},{3,2},{4,5},{5,4},{6,7},{7,6},{8,9},{9,8},{10,11... | collective-permute-start | bytes 196616 | tf_op jit(solution)/shard_map/ppermute | solution.py:476
  50.4 2.9 %copy-start.2 = (bf16[1,256,2048]{2,1,0:T(8,128)(2,1)S(1)}, bf16[1,256,2048]{2,1,0:T(8,128)(2,1)}, u32[]{:S(2)}) copy-start(bf16[1,256,2048]{2,1,0:T(8,128)(2,1)} %param.39) | copy-start | bytes 3145732
  50.4 2.9 %collective-permute-start.1 = (bf16[16,16,1792]{2,1,0:T(8,128)(2,1)S(1)}, bf16[16,16,1792]{2,1,0:T(8,128)(2,1)S(1)}, u32[]{:S(2)}, u32[]{:S(2)}) collective-permute-start(bf16[16,16,1792]{2,1,0:T(8,128)(2,1)S(1)} %all_to_all.21.slots_ref.own_ref), channel_id=1, source_target_pairs={{0,1},{1,0},{2,3},{3,2},{4,5},{5,4},{6,7},{7,6},{8,9},{9,8},{10,11... | collective-permute-start | bytes 2752520 | tf_op jit(solution)/shard_map/ppermute | solution.py:513
  50.4 2.9 %collective-permute-start.2 = (bf16[8,16,1152]{2,1,0:T(8,128)(2,1)S(1)}, bf16[8,16,1152]{2,1,0:T(8,128)(2,1)S(1)}, u32[]{:S(2)}, u32[]{:S(2)}) collective-permute-start(bf16[8,16,1152]{2,1,0:T(8,128)(2,1)S(1)} %all_to_all.20.got_ref.line_ref), channel_id=1, source_target_pairs={{0,1},{1,0},{2,3},{3,2},{4,5},{5,4},{6,7},{7,6},{8,9},{9,8},{10,11... | collective-permute-start | bytes 884744 | tf_op jit(solution)/shard_map/ppermute | solution.py:501
  53.3 1.5 %copy-start.5 = (bf16[2048,64]{0,1:T(8,128)(2,1)S(1)}, bf16[2048,64]{0,1:T(8,128)(2,1)}, u32[]{:S(2)}) copy-start(bf16[2048,64]{0,1:T(8,128)(2,1)} %param.24) | copy-start | bytes 786436
  53.3 1.5 %copy-start.6 = (bf16[2048,64]{0,1:T(8,128)(2,1)S(1)}, bf16[2048,64]{0,1:T(8,128)(2,1)}, u32[]{:S(2)}) copy-start(bf16[2048,64]{0,1:T(8,128)(2,1)} %param.25) | copy-start | bytes 786436
  53.3 1.5 %copy-start.7 = (f32[2048]{0:T(1024)S(1)}, f32[2048]{0:T(1024)}, u32[]{:S(2)}) copy-start(f32[2048]{0:T(1024)} %param.22) | copy-start | bytes 24580
  54.2 2.0 %collective-permute-start.3 = (bf16[256,1024]{1,0:T(8,128)(2,1)S(1)}, bf16[256,1024]{1,0:T(8,128)(2,1)S(1)}, u32[]{:S(2)}, u32[]{:S(2)}) collective-permute-start(bf16[256,1024]{1,0:T(8,128)(2,1)S(1)} %get-tuple-element.29), channel_id=1, source_target_pairs={{0,1},{1,0},{2,3},{3,2},{4,5},{5,4},{6,7},{7,6},{8,9},{9,8},{10,11... | collective-permute-start | bytes 1572872 | tf_op jit(solution)/shard_map/ppermute | solution.py:534
  54.4 2.2 %collective-permute-start.4 = (bf16[128,1024]{1,0:T(8,128)(2,1)S(1)}, bf16[128,1024]{1,0:T(8,128)(2,1)S(1)}, u32[]{:S(2)}, u32[]{:S(2)}) collective-permute-start(bf16[128,1024]{1,0:T(8,128)(2,1)S(1)} %get-tuple-element.30), channel_id=1, source_target_pairs={{0,1},{1,0},{2,3},{3,2},{4,5},{5,4},{6,7},{7,6},{8,9},{9,8},{10,11... | collective-permute-start | bytes 786440 | tf_op jit(solution)/shard_map/ppermute | solution.py:535

commit v5 on v4

--- a/solution.py
+++ b/solution.py
@@ -296,96 +296,57 @@
     return lax.broadcasted_iota(jnp.int32, shape, 1) // 32
 
 
-def half_products(side, slots_ref, line_ref, gate_ref, up_ref, dense_ref):
-    half = line_ref.shape[2] - 128
+def half_products(side, slots_ref, width, gate_ref, up_ref):
+    half = width // 2
     mine = pl.ds(pl.multiple_of(side * half, half), half)
     values = slots_ref[:, :, :half].reshape(-1, half)
-    gate = jnp.dot(values, gate_ref[mine, :], preferred_element_type=F32)
-    up = jnp.dot(values, up_ref[mine, :], preferred_element_type=F32)
-    rows = line_ref[:, :, :half].reshape(-1, half)
+    return tuple(jnp.dot(values, ref[mine, :], preferred_element_type=F32) for ref in (gate_ref, up_ref))
+
+
+def dense_share(core, slots_ref, line_own_ref, line_other_ref):
+    half = line_own_ref.shape[2] - 128
     block = half // 4
-    group = lane_group((rows.shape[0], 128))
-    dense = []
+    group = lane_group((line_own_ref.shape[0] * line_own_ref.shape[1], 128))
+    sums = []
     for part in range(2):
-        weights = dense_weights(dense_ref, half, part, side * 4)
         total = jnp.zeros(group.shape, F32)
-        for k in range(4):
-            product = jnp.dot(rows[:, k * block : (k + 1) * block], weights, preferred_element_type=F32)
-            total += jnp.where(group == k, product, 0.0)
-        dense.append(total)
-    return gate, up, dense
-
-
-def own_kernel(core_ref, slots_ref, line_ref, gate_ref, up_ref, gate_out, up_out, dense_out):
-    gate, up, dense = half_products(core_ref[0], slots_ref, line_ref, gate_ref, up_ref, slots_ref)
-    gate_out[...] = gate
-    up_out[...] = up
-    for n, values in enumerate(dense):
-        dense_out[n] = values
-
-
-def down_products(side, hidden, dense, down_ref, dense_ref, target_ref, line_target):
-    half = target_ref.shape[1]
-    mine = pl.ds(pl.multiple_of(side * half, half), half)
-    target_ref[...] = jnp.dot(hidden, down_ref[:, mine], preferred_element_type=F32).astype(BF16)
-    block = half // 4
-    weights = dense_weights(dense_ref, half, 2, side * 4)
-    group = lane_group(dense.shape)
-    for k in range(4):
-        line_target[:, k * block : (k + 1) * block] = lax.dot_general(
-            jnp.where(group == k, dense, 0.0).astype(BF16),
+        for side, line_ref in ((core, line_own_ref), (1 - core, line_other_ref)):
+            rows = line_ref[:, :, :half].reshape(-1, half)
+            weights = dense_weights(slots_ref, half, part, side * 4)
+            for k in range(4):
+                product = jnp.dot(rows[:, k * block : (k + 1) * block], weights, preferred_element_type=F32)
+                total += jnp.where(group == k, product, 0.0)
+        total += pltpu.roll(total, 64, 1)
+        sums.append(total + pltpu.roll(total, 32, 1))
+    hidden = (jax.nn.silu(sums[0]) * sums[1]).astype(BF16).astype(F32)
+    weights = dense_weights(slots_ref, half, 2, core * 4)
+    return [
+        lax.dot_general(
+            jnp.where(group == k, hidden, 0.0).astype(BF16),
             weights,
             (((1,), (1,)), ((), ())),
             preferred_element_type=F32,
-        ).astype(BF16)
-
-
-def other_kernel(
+        )
+        for k in range(4)
+    ]
+
+
+def own_kernel(
     core_ref,
-    gate_sum,
-    up_sum,
-    dense_sum,
-    own_ref,
-    other_ref,
-    line_ref,
+    slots_ref,
     gate_ref,
     up_ref,
-    down_ref,
-    send_ref,
-    line_send_ref,
-    hidden_ref,
-    dense_ref,
-):
-    side = 1 - core_ref[0]
-    gate, up, dense = half_products(side, other_ref, line_ref, gate_ref, up_ref, own_ref)
-    hidden = (jax.nn.silu(gate_sum[...] + gate) * (up_sum[...] + up)).astype(BF16)
-    sums = []
-    for n, values in enumerate(dense):
-        total = values + dense_sum[n]
-        total += pltpu.roll(total, 64, 1)
-        sums.append(total + pltpu.roll(total, 32, 1))
-    dense = (jax.nn.silu(sums[0]) * sums[1]).astype(BF16)
-    hidden_ref[...] = hidden
-    dense_ref[...] = dense
-    down_products(side, hidden, dense.astype(F32), down_ref, own_ref, send_ref, line_send_ref)
-
-
-def keep_kernel(
-    core_ref,
-    hidden_ref,
-    dense_ref,
-    own_ref,
-    down_ref,
     tokens_ref,
     gain_ref,
     key_ref,
     value_ref,
-    keep_ref,
-    line_keep_ref,
+    gate_out,
+    up_out,
     keys_ref,
     values_ref,
 ):
-    down_products(core_ref[0], hidden_ref[...], dense_ref[...].astype(F32), down_ref, own_ref, keep_ref, line_keep_ref)
+    core = core_ref[0]
+    gate_out[...], up_out[...] = half_products(core, slots_ref, gate_ref.shape[0], gate_ref, up_ref)
     normed = rms_scale(tokens_ref[...], gain_ref[...]).astype(BF16)
     for weight_ref, target_ref in ((key_ref, keys_ref), (value_ref, values_ref)):
         target_ref[...] = lax.dot_general(
@@ -393,7 +354,35 @@
         ).astype(BF16)
 
 
-def combine_kernel(back_ref, combine_ref, line_ref, line_keep_ref, line_got_ref, send_ref):
+def down_product(side, hidden, down_ref):
+    half = down_ref.shape[1] // 2
+    mine = pl.ds(pl.multiple_of(side * half, half), half)
+    return jnp.dot(hidden, down_ref[:, mine], preferred_element_type=F32).astype(BF16)
+
+
+def other_kernel(
+    core_ref, gate_sum, up_sum, other_ref, line_other_ref, gate_ref, up_ref, down_ref, send_ref, hidden_ref
+):
+    del line_other_ref
+    side = 1 - core_ref[0]
+    gate, up = half_products(side, other_ref, gate_ref.shape[0], gate_ref, up_ref)
+    hidden = (jax.nn.silu(gate_sum[...] + gate) * (up_sum[...] + up)).astype(BF16)
+    hidden_ref[...] = hidden
+    send_ref[...] = down_product(side, hidden, down_ref)
+
+
+def keep_kernel(
+    core_ref, hidden_ref, down_ref, own_ref, other_ref, line_own_ref, line_other_ref, keep_ref, dense_out
+):
+    core = core_ref[0]
+    keep_ref[...] = down_product(core, hidden_ref[...], down_ref)
+    block = dense_out.shape[1] // 4
+    shares = [dense_share(core, ref, line_own_ref, line_other_ref) for ref in (own_ref, other_ref)]
+    for k, (own, other) in enumerate(zip(*shares, strict=True)):
+        dense_out[:, k * block : (k + 1) * block] = own + other
+
+
+def combine_kernel(back_ref, combine_ref, line_ref, dense_ref, send_ref):
     lines, seq_count, half = send_ref.shape
     token_total = lines * seq_count
     slot_total = back_ref.shape[0] * back_ref.shape[1]
@@ -402,8 +391,7 @@
     routed += jnp.dot(combine_ref[:, slot_total:], back, preferred_element_type=F32)
     meta = line_ref[...].reshape(token_total, line_ref.shape[2])[:, half:].astype(F32)
     mix = meta[:, MIX_HI : MIX_HI + 1] + meta[:, MIX_LO : MIX_LO + 1]
-    dense = line_keep_ref[...].astype(F32) + line_got_ref[...].astype(F32)
-    send_ref[...] = (routed + mix * dense).astype(BF16).reshape(lines, seq_count, half)
+    send_ref[...] = (routed + mix * dense_ref[...]).astype(BF16).reshape(lines, seq_count, half)
 
 
 def finish_kernel(residual_ref, parts_ref, out_ref):
@@ -513,52 +501,39 @@
     slot_other = lax.ppermute(slot_own, "tp", SWAP)
     weights = (w_expert_gate[0], w_expert_up[0])
     hidden_shape = (slot_total, w_expert_gate.shape[2])
-    sums = call(
+    hidden_shape = (slot_total, w_expert_gate.shape[2])
+    new_shape = jax.ShapeDtypeStruct((seq_count, w_key.shape[1]), BF16)
+    dense_shape = jax.ShapeDtypeStruct((token_total, half), F32)
+    gate_sum, up_sum, new_keys, new_values = call(
         own_kernel,
-        (jax.ShapeDtypeStruct(hidden_shape, F32),) * 2 + (jax.ShapeDtypeStruct((2, token_total, 128), F32),),
+        (*(jax.ShapeDtypeStruct(hidden_shape, F32),) * 2, new_shape, new_shape),
         1,
-        (core, slot_own, line_own, *weights),
+        (core, slot_own, *weights, tokens, attn_gain.reshape(1, width), w_key.T, w_value.T),
         8,
     )
-    both_shape = (
-        jax.ShapeDtypeStruct((slot_total, half), BF16),
-        jax.ShapeDtypeStruct((token_total, half), BF16),
-    )
-    send, dense_send, hidden, dense = call(
+    result_shape = jax.ShapeDtypeStruct((slot_total, half), BF16)
+    send, hidden = call(
         other_kernel,
-        (*both_shape, jax.ShapeDtypeStruct(hidden_shape, BF16), jax.ShapeDtypeStruct((token_total, 128), BF16)),
+        (result_shape, jax.ShapeDtypeStruct(hidden_shape, BF16)),
         1,
-        (core, *sums, slot_own, slot_other, line_other, *weights, w_expert_down[0]),
+        (core, gate_sum, up_sum, slot_other, line_other, *weights, w_expert_down[0]),
         12,
     )
     got = lax.ppermute(send, "tp", SWAP)
-    dense_got = lax.ppermute(dense_send, "tp", SWAP)
-    new_shape = jax.ShapeDtypeStruct((seq_count, w_key.shape[1]), BF16)
-    keep, dense_keep, new_keys, new_values = call(
+    keep, dense = call(
         keep_kernel,
-        (*both_shape, new_shape, new_shape),
+        (result_shape, dense_shape),
         1,
-        (
-            core,
-            hidden,
-            dense,
-            slot_own,
-            w_expert_down[0],
-            tokens,
-            attn_gain.reshape(1, width),
-            w_key.T,
-            w_value.T,
-        ),
-        8,
+        (core, hidden, w_expert_down[0], slot_own, slot_other, line_own, line_other),
+        12,
     )
     results = (keep.astype(F32) + got.astype(F32)).astype(BF16)
-    results, dense_got = lax.optimization_barrier((results, dense_got))
     back = lax.all_to_all(results.reshape(places, seq_count, half), PLANE, 0, 0, tiled=True)
     partial = call(
         combine_kernel,
         jax.ShapeDtypeStruct((lines, seq_count, half), BF16),
         0,
-        (back, combine, line_own, dense_keep, dense_got),
+        (back, combine, line_own, dense),
         8,
     )
     parts = lax.all_to_all(partial, LINE, 0, 0, tiled=True)

time: 86 us -> 85.6 us (level)
  transfers between devices with their start and end apart: 5 -> 4, of which waited for: 4 -> 3; matrix products, arithmetic and copies ran while one was open for 0% -> 0% of each run, Pallas kernels for 2% -> 3%
where the time goes in v5:
time: 85.6 us; the launch traced here: 85.4 us
  blocking collectives  70.5 us (82%)
  Pallas kernels  10.1 us (12%)
  waiting for transfers between devices  2.8 us (3%)
  between operations  0.87 us (1%)
    all_to_all x1, blocking collectives, shards(): line_own = lax.all_to_all(line_send, LINE, 0, 0, tiled=True)  21.2 us
    all_to_all x1, blocking collectives, shards(): slot_own = lax.all_to_all(slot_send, PLANE, 0, 0, tiled=True)  21.1 us
    all_to_all x1, blocking collectives, shards(): lax.all_to_all(results.reshape(places, seq_count, half), PLANE, 0, 0, til...  14.7 us
    all_to_all x1, blocking collectives, shards(): parts = lax.all_to_all(partial, LINE, 0, 0, tiled=True)  13.6 us
    pallas_call x8, Pallas kernels, call(): pl.pallas_call(kernel, out_shape=out_shape, in_specs=in_specs, out_specs=...  10.1 us
  transfers between devices with their start and end apart: 4, of which 3 were waited for; matrix products, arithmetic and copies ran while one was open for 0% of the time, Pallas kernels for 3%

profile of v5, /device:TPU:2, one launch (start us, length us, event | category | flops | bytes accessed | tf_op | source)
XLA Modules:
  0.0 85.4 jit_solution(10708000767474109721)
XLA Ops:
  0.7 5.0 %shard_map.211.own_ref = bf16[16,2048]{1,0:T(8,128)(2,1)S(1)} custom-call(f32[1,8]{1,0:T(1,128)} %bitcast.32, s32[1,16]{1,0:T(1,128)} %bitcast.33, bf16[16,2048]{1,0:T(8,128)(2,1)} %tokens_ref.3, f32[1,2048]{1,0:T(1,128)} %bitcast.24, bf16[2048,512]{1,0:T(8,128)(2,1)} %query_hbm.1, bf16[1024,1024]{1,0:T(8,128)(2,1)} %bitcast.30, ...), custom_call_target="tpu_custom_call" | custom-call | tf_op jit(solution)/shard_map/pallas_call | solution.py:171
  5.7 0.0 copy-start
  5.8 0.0 copy-start.1
  5.8 0.0 copy-start.5
  5.8 0.0 copy-start.6
  5.8 0.0 copy-start.7
  5.8 0.1 collective-permute-start
  5.9 0.0 copy-done.13
  5.9 0.1 copy.23.routes_ref
  6.0 1.1 %collective-permute-done.other_ref = bf16[16,2048]{1,0:T(8,128)(2,1)S(1)} collective-permute-done((bf16[16,2048]{1,0:T(8,128)(2,1)S(1)}, bf16[16,2048]{1,0:T(8,128)(2,1)S(1)}, u32[]{:S(2)}, u32[]{:S(2)}) %collective-permute-start) | collective-permute-done | bytes 65568 | tf_op jit(solution)/shard_map/ppermute | solution.py:464
  7.2 0.0 copy-done.9
  7.2 0.0 copy-done.10
  7.2 0.0 copy-done.11
  7.2 0.0 copy-done.12
  7.2 0.4 shard_map.212
  7.6 21.2 %all_to_all.20.got_ref.line_own_ref.line_ref = bf16[8,16,1152]{2,1,0:T(8,128)(2,1)S(1)} all-to-all(bf16[8,16,1152]{2,1,0:T(8,128)(2,1)S(1)} %get-tuple-element.16), channel_id=1, replica_groups=mesh['ep_0'=8,'ep_1'=4,'ep_2'=4,'tp'=2] {'ep_0'}, dimensions={0} | all-to-all | bytes 589824 | tf_op jit(solution)/shard_map/all_to_all | solution.py:488
  28.8 0.5 shard_map.213
  29.3 21.1 %all_to_all.21.slots_ref.own_ref = bf16[16,16,1792]{2,1,0:T(8,128)(2,1)S(1)} all-to-all(bf16[16,16,1792]{2,1,0:T(8,128)(2,1)S(1)} %get-tuple-element.17), channel_id=1, replica_groups=mesh['ep_0'=8,'ep_1'=4,'ep_2'=4,'tp'=2] {'ep_1','ep_2'}, dimensions={0} | all-to-all | bytes 1835008 | tf_op jit(solution)/shard_map/all_to_all | solution.py:500
  50.4 0.0 collective-permute-start.1
  50.4 0.5 collective-permute-start.2
  50.9 1.2 %shard_map.214 = (f32[256,256]{1,0:T(8,128)S(1)}, f32[256,256]{1,0:T(8,128)S(1)}, bf16[16,64]{1,0:T(8,128)(2,1)}, bf16[16,64]{1,0:T(8,128)(2,1)}) custom-call(s32[1]{0:T(128)} %bitcast.core_ref, bf16[16,16,1792]{2,1,0:T(8,128)(2,1)S(1)} %all_to_all.21.slots_ref.own_ref, bf16[2048,256]{1,0:T(8,128)(2,1)S(1)} %bitcast.16, bf16[2048,256]{1,0:T(8,128)(2,1)S(1)} %bitcast.18, ...), custom_call_target="tpu_custom_call" | custom-call | tf_op jit(solution)/shard_map/pallas_call | solution.py:171
  52.1 1.2 %collective-permute-done.2.line_other_ref = bf16[8,16,1152]{2,1,0:T(8,128)(2,1)S(1)} collective-permute-done((bf16[8,16,1152]{2,1,0:T(8,128)(2,1)S(1)}, bf16[8,16,1152]{2,1,0:T(8,128)(2,1)S(1)}, u32[]{:S(2)}, u32[]{:S(2)}) %collective-permute-start.2) | collective-permute-done | bytes 294944 | tf_op jit(solution)/shard_map/ppermute | solution.py:489
  53.3 0.0 collective-permute-done.1.other_ref
  53.3 0.7 shard_map.215
  54.0 0.2 collective-permute-start.3
  54.2 1.3 %shard_map.216 = (bf16[256,1024]{1,0:T(8,128)(2,1)S(1)}, f32[128,1024]{1,0:T(8,128)S(1)}) custom-call(s32[1]{0:T(128)} %bitcast.core_ref, bf16[256,256]{1,0:T(8,128)(2,1)S(1)} %get-tuple-element.20.hidden_ref, bf16[256,2048]{1,0:T(8,128)(2,1)S(1)} %bitcast.21, bf16[16,16,1792]{2,1,0:T(8,128)(2,1)S(1)} %all_to_all.21.slots_ref.own_ref, ...), custom_call_target="tpu_custom_call" | custom-call | tf_op jit(solution)/shard_map/pallas_call | solution.py:171
  55.5 0.5 collective-permute-done.3
  56.0 0.2 add_convert_fusion
  56.2 14.7 %all_to_all.22.back_ref = bf16[16,16,1024]{2,1,0:T(8,128)(2,1)S(1)} all-to-all(bf16[16,16,1024]{2,1,0:T(8,128)(2,1)S(1)} %bitcast.29), channel_id=1, replica_groups=mesh['ep_0'=8,'ep_1'=4,'ep_2'=4,'tp'=2] {'ep_1','ep_2'}, dimensions={0} | all-to-all | bytes 1048576 | tf_op jit(solution)/shard_map/all_to_all | solution.py:531
  70.9 0.3 shard_map.217
  71.2 13.6 %all_to_all.23.parts_ref = bf16[8,16,1024]{2,1,0:T(8,128)(2,1)S(1)} all-to-all(bf16[8,16,1024]{2,1,0:T(8,128)(2,1)S(1)} %shard_map.217), channel_id=1, replica_groups=mesh['ep_0'=8,'ep_1'=4,'ep_2'=4,'tp'=2] {'ep_0'}, dimensions={0} | all-to-all | bytes 524288 | tf_op jit(solution)/shard_map/all_to_all | solution.py:539
  84.7 0.7 shard_map.218
  (18 shorter events, 0.0 us)
Async XLA Ops:
  0.6 5.3 %copy-start.13 = (s32[16,6]{0,1:T(8,128)S(1)}, s32[16,6]{0,1:T(8,128)}, u32[]{:S(2)}) copy-start(s32[16,6]{0,1:T(8,128)} %param.32) | copy-start | bytes 1156
  0.6 6.5 %copy-start.3 = (bf16[16,2048]{1,0:T(8,128)(2,1)S(1)}, bf16[16,2048]{1,0:T(8,128)(2,1)}, u32[]{:S(2)}) copy-start(bf16[16,2048]{1,0:T(8,128)(2,1)} %tokens_ref.3) | copy-start | bytes 196612
  0.7 6.5 %copy-start.4 = (bf16[2048,128]{1,0:T(8,128)(2,1)S(1)}, bf16[2048,128]{1,0:T(8,128)(2,1)}, u32[]{:S(2)}) copy-start(bf16[2048,128]{1,0:T(8,128)(2,1)} %router_ref.1) | copy-start | bytes 1572868
  0.7 6.5 %copy-start.8 = (f32[2048]{0:T(1024)S(1)}, f32[2048]{0:T(1024)}, u32[]{:S(2)}) copy-start(f32[2048]{0:T(1024)} %param.30) | copy-start | bytes 24580
  0.7 6.5 %copy-start.9 = (bf16[16,256]{1,0:T(8,128)(2,1)S(1)}, bf16[16,256]{1,0:T(8,128)(2,1)}, u32[]{:S(2)}) copy-start(bf16[16,256]{1,0:T(8,128)(2,1)} %gate_ref.1) | copy-start | bytes 24580
  0.7 6.5 %copy-start.10 = (bf16[16,256]{1,0:T(8,128)(2,1)S(1)}, bf16[16,256]{1,0:T(8,128)(2,1)}, u32[]{:S(2)}) copy-start(bf16[16,256]{1,0:T(8,128)(2,1)} %up_ref.1) | copy-start | bytes 24580
  0.7 6.5 %copy-start.11 = (bf16[256,16]{0,1:T(8,128)(2,1)S(1)}, bf16[256,16]{0,1:T(8,128)(2,1)}, u32[]{:S(2)}) copy-start(bf16[256,16]{0,1:T(8,128)(2,1)} %param.35) | copy-start | bytes 24580
  0.7 6.5 %copy-start.12 = (f32[2048]{0:T(1024)S(1)}, f32[2048]{0:T(1024)}, u32[]{:S(2)}) copy-start(f32[2048]{0:T(1024)} %param.36) | copy-start | bytes 24580
  5.7 45.2 %copy-start = (bf16[1,2048,256]{2,1,0:T(8,128)(2,1)S(1)}, bf16[1,2048,256]{2,1,0:T(8,128)(2,1)}, u32[]{:S(2)}) copy-start(bf16[1,2048,256]{2,1,0:T(8,128)(2,1)} %param.37) | copy-start | bytes 3145732
  5.8 45.2 %copy-start.1 = (bf16[1,2048,256]{2,1,0:T(8,128)(2,1)S(1)}, bf16[1,2048,256]{2,1,0:T(8,128)(2,1)}, u32[]{:S(2)}) copy-start(bf16[1,2048,256]{2,1,0:T(8,128)(2,1)} %param.38) | copy-start | bytes 3145732
  5.8 45.2 %copy-start.5 = (bf16[2048,64]{0,1:T(8,128)(2,1)S(1)}, bf16[2048,64]{0,1:T(8,128)(2,1)}, u32[]{:S(2)}) copy-start(bf16[2048,64]{0,1:T(8,128)(2,1)} %param.24) | copy-start | bytes 786436
  5.8 45.2 %copy-start.6 = (bf16[2048,64]{0,1:T(8,128)(2,1)S(1)}, bf16[2048,64]{0,1:T(8,128)(2,1)}, u32[]{:S(2)}) copy-start(bf16[2048,64]{0,1:T(8,128)(2,1)} %param.25) | copy-start | bytes 786436
  5.8 45.1 %copy-start.7 = (f32[2048]{0:T(1024)S(1)}, f32[2048]{0:T(1024)}, u32[]{:S(2)}) copy-start(f32[2048]{0:T(1024)} %param.22) | copy-start | bytes 24580
  5.8 1.3 %collective-permute-start = (bf16[16,2048]{1,0:T(8,128)(2,1)S(1)}, bf16[16,2048]{1,0:T(8,128)(2,1)S(1)}, u32[]{:S(2)}, u32[]{:S(2)}) collective-permute-start(bf16[16,2048]{1,0:T(8,128)(2,1)S(1)} %shard_map.211.own_ref), channel_id=1, source_target_pairs={{0,1},{1,0},{2,3},{3,2},{4,5},{5,4},{6,7},{7,6},{8,9},{9,8},{10,11... | collective-permute-start | bytes 196616 | tf_op jit(solution)/shard_map/ppermute | solution.py:464
  50.4 2.9 %copy-start.2 = (bf16[1,256,2048]{2,1,0:T(8,128)(2,1)S(1)}, bf16[1,256,2048]{2,1,0:T(8,128)(2,1)}, u32[]{:S(2)}) copy-start(bf16[1,256,2048]{2,1,0:T(8,128)(2,1)} %param.39) | copy-start | bytes 3145732
  50.4 2.9 %collective-permute-start.1 = (bf16[16,16,1792]{2,1,0:T(8,128)(2,1)S(1)}, bf16[16,16,1792]{2,1,0:T(8,128)(2,1)S(1)}, u32[]{:S(2)}, u32[]{:S(2)}) collective-permute-start(bf16[16,16,1792]{2,1,0:T(8,128)(2,1)S(1)} %all_to_all.21.slots_ref.own_ref), channel_id=1, source_target_pairs={{0,1},{1,0},{2,3},{3,2},{4,5},{5,4},{6,7},{7,6},{8,9},{9,8},{10,11... | collective-permute-start | bytes 2752520 | tf_op jit(solution)/shard_map/ppermute | solution.py:501
  50.4 2.9 %collective-permute-start.2 = (bf16[8,16,1152]{2,1,0:T(8,128)(2,1)S(1)}, bf16[8,16,1152]{2,1,0:T(8,128)(2,1)S(1)}, u32[]{:S(2)}, u32[]{:S(2)}) collective-permute-start(bf16[8,16,1152]{2,1,0:T(8,128)(2,1)S(1)} %all_to_all.20.got_ref.line_own_ref.line_ref), channel_id=1, source_target_pairs={{0,1},{1,0},{2,3},{3,2},{4,5},{5,4},{6,7},{7,6},{8,9},{9,8},{10,11... | collective-permute-start | bytes 884744 | tf_op jit(solution)/shard_map/ppermute | solution.py:489
  54.0 2.0 %collective-permute-start.3 = (bf16[256,1024]{1,0:T(8,128)(2,1)S(1)}, bf16[256,1024]{1,0:T(8,128)(2,1)S(1)}, u32[]{:S(2)}, u32[]{:S(2)}) collective-permute-start(bf16[256,1024]{1,0:T(8,128)(2,1)S(1)} %get-tuple-element.22), channel_id=1, source_target_pairs={{0,1},{1,0},{2,3},{3,2},{4,5},{5,4},{6,7},{7,6},{8,9},{9,8},{10,11... | collective-permute-start | bytes 1572872 | tf_op jit(solution)/shard_map/ppermute | solution.py:522

commit v6 on v5

--- a/solution.py
+++ b/solution.py
@@ -30,7 +30,9 @@
     key_hbm,
     value_hbm,
     out_hbm,
+    router_hbm,
     partial_ref,
+    router_ref,
     bias_ref,
     lengths_ref,
     tokens_ref,
@@ -66,34 +68,40 @@
             (lengths_hbm, lengths_ref),
         )
     ]
-    query_copies = fetch(query_hbm, query_buf, 2)
+    query_copies = fetch(query_hbm, query_buf, 4)
     key_copies = fetch(key_hbm, key_buf, 2)
     value_copies = fetch(value_hbm, value_buf, 2)
     out_copies = fetch(out_hbm, out_buf, 1)
+    router_copies = fetch(router_hbm, router_ref, 1)
     for copy in copies:
         copy.start()
 
     for copy in small_copies:
         copy.wait()
     normed = rms_scale(tokens_ref[...], gain_ref[...]).astype(BF16)
-    row = lax.broadcasted_iota(jnp.int32, (heads * seq_count, 1), 0)
-    bias = jnp.zeros((heads * seq_count, 1), F32)
+    parts = len(key_copies)
+    part = seq_count // parts
+    part_rows = row_total // parts
+    row = lax.broadcasted_iota(jnp.int32, (heads * part, 1), 0)
+    bias = jnp.zeros((heads * part, 1), F32)
     for h in range(heads):
-        bias = jnp.where(row // seq_count == h, bias_ref[:, h : h + 1], bias)
-    lengths = jnp.zeros((seq_count, 1), jnp.int32)
-    for n in range(seq_count):
-        lengths = jnp.where(row[:seq_count] == n, lengths_ref[:, n : n + 1], lengths)
-    lengths = jnp.concatenate([lengths] * heads, axis=0)
-    lane = lax.broadcasted_iota(jnp.int32, (seq_count, 128), 1)
-    low = lane < head_dim
+        bias = jnp.where(row // part == h, bias_ref[:, h : h + 1], bias)
+    low = lax.broadcasted_iota(jnp.int32, (part, 128), 1) < head_dim
     own = (
-        lax.broadcasted_iota(jnp.int32, (seq_count, row_total), 1) // head_dim
-        == lax.broadcasted_iota(jnp.int32, (seq_count, row_total), 0)
+        lax.broadcasted_iota(jnp.int32, (part, part_rows), 1) // head_dim
+        == lax.broadcasted_iota(jnp.int32, (part, part_rows), 0)
     )
     span = 256
     after_mask = (
         lax.broadcasted_iota(jnp.int32, (span, span), 0) > lax.broadcasted_iota(jnp.int32, (span, span), 1)
     ).astype(BF16)
+    lengths = []
+    for n in range(parts):
+        column = jnp.zeros((part, 1), jnp.int32)
+        for k in range(part):
+            at = n * part + k
+            column = jnp.where(row[:part] == k, lengths_ref[:, at : at + 1], column)
+        lengths.append(jnp.concatenate([column] * heads, axis=0))
 
     queries = jnp.zeros((seq_count, head_total), F32)
     piece = width // len(query_copies)
@@ -102,65 +110,61 @@
         at = slice(n * piece, (n + 1) * piece)
         queries += jnp.dot(normed[:, at], query_buf[at, :], preferred_element_type=F32)
     queries = queries.astype(BF16).astype(F32)
-    spread = []
-    for h in range(heads):
-        tile = queries[:, h // 2 * 128 : h // 2 * 128 + 128]
-        turned = pltpu.roll(tile, head_dim, 1)
-        both = jnp.where(low, tile, turned) if h % 2 == 0 else jnp.where(low, turned, tile)
-        wide = jnp.concatenate([both] * (row_total // 128), axis=1)
-        spread.append(jnp.where(own, wide, 0.0).astype(BF16))
-    spread = jnp.concatenate(spread, axis=0)
-
-    scores = None
-    piece = row_total // len(key_copies)
+
+    def spread(n):
+        out = []
+        for h in range(heads):
+            tile = queries[n * part : (n + 1) * part, h // 2 * 128 : h // 2 * 128 + 128]
+            turned = pltpu.roll(tile, head_dim, 1)
+            both = jnp.where(low, tile, turned) if h % 2 == 0 else jnp.where(low, turned, tile)
+            out.append(jnp.where(own, jnp.concatenate([both] * (part_rows // 128), axis=1), 0.0))
+        return jnp.concatenate(out, axis=0).astype(BF16)
+
+    def stick(scores, lengths):
+        later = jnp.zeros((heads * part, 1), F32)
+        out = []
+        for block in reversed(range(cache_len // span)):
+            score = scores[:, block * span : (block + 1) * span] * head_dim ** (-0.5) + bias
+            position = lax.broadcasted_iota(jnp.int32, score.shape, 1) + block * span
+            visible = position < lengths
+            soft = jnp.log1p(jnp.exp(-jnp.abs(score)))
+            log_keep = jnp.where(visible, -(jnp.maximum(score, 0.0) + soft), 0.0)
+            high = log_keep.astype(BF16)
+            rest = (log_keep - high.astype(F32)).astype(BF16)
+            log_after = jnp.dot(high, after_mask, preferred_element_type=F32)
+            log_after += jnp.dot(rest, after_mask, preferred_element_type=F32)
+            weight = jnp.exp(jnp.minimum(score, 0.0) - soft + (log_after + later))
+            out.append(jnp.where(visible, weight, 0.0).astype(BF16))
+            later += jnp.sum(log_keep, axis=-1, keepdims=True)
+        return jnp.concatenate(out[::-1], axis=1)
+
+    spreads = [spread(n) for n in range(parts)]
+    sticks = []
     for n, copy in enumerate(key_copies):
         copy.wait()
-        at = slice(n * piece, (n + 1) * piece)
-        part = jnp.dot(spread[:, at], key_buf[at, :], preferred_element_type=F32)
-        scores = part if scores is None else scores + part
-    later = jnp.zeros((heads * seq_count, 1), F32)
-    sticks = []
-    for block in reversed(range(cache_len // span)):
-        score = scores[:, block * span : (block + 1) * span] * head_dim ** (-0.5) + bias
-        position = lax.broadcasted_iota(jnp.int32, score.shape, 1) + block * span
-        visible = position < lengths
-        soft = jnp.log1p(jnp.exp(-jnp.abs(score)))
-        log_keep = jnp.where(visible, -(jnp.maximum(score, 0.0) + soft), 0.0)
-        high = log_keep.astype(BF16)
-        rest = (log_keep - high.astype(F32)).astype(BF16)
-        log_after = jnp.dot(high, after_mask, preferred_element_type=F32)
-        log_after += jnp.dot(rest, after_mask, preferred_element_type=F32)
-        weight = jnp.exp(jnp.minimum(score, 0.0) - soft + (log_after + later))
-        sticks.append(jnp.where(visible, weight, 0.0).astype(BF16))
-        later += jnp.sum(log_keep, axis=-1, keepdims=True)
-    sticks = jnp.concatenate(sticks[::-1], axis=1)
-
-    read = []
-    piece = row_total // len(value_copies)
+        keys = key_buf[n * part_rows : (n + 1) * part_rows, :]
+        sticks.append(stick(jnp.dot(spreads[n], keys, preferred_element_type=F32), lengths[n]))
+    heads_out = []
     for n, copy in enumerate(value_copies):
         copy.wait()
-        read.append(
-            lax.dot_general(
-                sticks,
-                value_buf[n * piece : (n + 1) * piece, :],
-                (((1,), (1,)), ((), ())),
-                preferred_element_type=F32,
-            )
+        values = value_buf[n * part_rows : (n + 1) * part_rows, :]
+        read = lax.dot_general(sticks[n], values, (((1,), (1,)), ((), ())), preferred_element_type=F32)
+        folded = []
+        for h in range(heads):
+            mine = jnp.where(own, read[h * part : (h + 1) * part], 0.0)
+            tile = mine[:, :128]
+            for k in range(1, part_rows // 128):
+                tile += mine[:, k * 128 : (k + 1) * 128]
+            folded.append(tile + pltpu.roll(tile, head_dim, 1))
+        heads_out.append(
+            jnp.concatenate([jnp.where(low, folded[h], folded[h + 1]) for h in range(0, heads, 2)], axis=1)
         )
-    read = jnp.concatenate(read, axis=1)
-    folded = []
-    for h in range(heads):
-        mine = jnp.where(own, read[h * seq_count : (h + 1) * seq_count], 0.0)
-        tile = mine[:, :128]
-        for n in range(1, row_total // 128):
-            tile += mine[:, n * 128 : (n + 1) * 128]
-        folded.append(tile + pltpu.roll(tile, head_dim, 1))
-    heads_out = jnp.concatenate(
-        [jnp.where(low, folded[h], folded[h + 1]) for h in range(0, heads, 2)], axis=1
-    ).astype(BF16)
+    heads_out = jnp.concatenate(heads_out, axis=0).astype(BF16)
     for copy in out_copies:
         copy.wait()
     partial_ref[...] = jnp.dot(heads_out, out_buf[...], preferred_element_type=F32).astype(BF16)
+    for copy in router_copies:
+        copy.wait()
 
 
 def call(kernel, out_shape, smem_count, inputs, limit, hbm_count=0, scratch=()):
@@ -433,9 +437,9 @@
     line = lax.axis_index(LINE).astype(jnp.int32).reshape(1)
     cache_rows = seq_count * key_cache.shape[2]
     cache_len = key_cache.shape[3]
-    attn_own = call(
+    attn_own, router = call(
         attend_kernel,
-        jax.ShapeDtypeStruct((seq_count, width), BF16),
+        (jax.ShapeDtypeStruct((seq_count, width), BF16), jax.ShapeDtypeStruct(w_router.shape, BF16)),
         0,
         (
             head_bias.reshape(1, -1),
@@ -446,9 +450,10 @@
             key_cache.reshape(cache_rows, cache_len),
             value_cache.reshape(cache_rows, cache_len),
             w_attn_out,
+            w_router,
         ),
         24,
-        hbm_count=8,
+        hbm_count=9,
         scratch=(
             pltpu.VMEM((1, head_bias.shape[0]), F32),
             pltpu.VMEM((1, seq_count), jnp.int32),
@@ -458,7 +463,7 @@
             pltpu.VMEM((cache_rows, cache_len), BF16),
             pltpu.VMEM((cache_rows, cache_len), BF16),
             pltpu.VMEM(w_attn_out.shape, BF16),
-            pltpu.SemaphoreType.DMA((11,)),
+            pltpu.SemaphoreType.DMA((14,)),
         ),
     )
     attn_other = lax.ppermute(attn_own, "tp", SWAP)
@@ -476,7 +481,7 @@
             attn_own,
             attn_other,
             ffn_gain.reshape(1, width),
-            w_router,
+            router,
             routes,
             w_dense_gate,
             w_dense_up,

time: 85.6 us -> 85.4 us (level)
  no operation moved by 1% of the time
where the time goes in v6:
time: 85.4 us; the launch traced here: 85.2 us
  blocking collectives  70.5 us (83%)
  Pallas kernels  9.88 us (12%)
  waiting for transfers between devices  2.8 us (3%)
  between operations  0.86 us (1%)
    all_to_all x1, blocking collectives, shards(): line_own = lax.all_to_all(line_send, LINE, 0, 0, tiled=True)  21.2 us
    all_to_all x1, blocking collectives, shards(): slot_own = lax.all_to_all(slot_send, PLANE, 0, 0, tiled=True)  21.1 us
    all_to_all x1, blocking collectives, shards(): lax.all_to_all(results.reshape(places, seq_count, half), PLANE, 0, 0, til...  14.7 us
    all_to_all x1, blocking collectives, shards(): parts = lax.all_to_all(partial, LINE, 0, 0, tiled=True)  13.6 us
    pallas_call x8, Pallas kernels, call(): pl.pallas_call(kernel, out_shape=out_shape, in_specs=in_specs, out_specs=...  9.88 us
  transfers between devices with their start and end apart: 4, of which 3 were waited for; matrix products, arithmetic and copies ran while one was open for 0% of the time, Pallas kernels for 3%

profile of v6, /device:TPU:2, one launch (start us, length us, event | category | flops | bytes accessed | tf_op | source)
XLA Modules:
  0.0 85.2 jit_solution(10074197938531112434)
XLA Ops:
  0.6 0.0 copy-start.12
  0.6 0.0 copy-start.3
  0.7 0.0 copy-start.7
  0.7 4.8 %shard_map.211 = (bf16[16,2048]{1,0:T(8,128)(2,1)S(1)}, bf16[2048,128]{1,0:T(8,128)(2,1)S(1)}) custom-call(f32[1,8]{1,0:T(1,128)} %bitcast.32, s32[1,16]{1,0:T(1,128)} %bitcast.33, bf16[16,2048]{1,0:T(8,128)(2,1)} %tokens_ref.3, f32[1,2048]{1,0:T(1,128)} %bitcast.24, bf16[2048,512]{1,0:T(8,128)(2,1)} %query_hbm.1, bf16[1024,1024]{1,0:T(8,128)(2,1)} %bitcast.30, ...), custom_call_target="tpu_custom_call" | custom-call | tf_op jit(solution)/shard_map/pallas_call | solution.py:175
  5.5 0.0 copy-start
  5.6 0.0 copy-start.1
  5.6 0.0 copy-start.4
  5.6 0.0 copy-start.5
  5.6 0.0 copy-start.6
  5.6 0.1 collective-permute-start
  5.7 0.1 copy.23.routes_ref
  5.8 1.1 %collective-permute-done.other_ref = bf16[16,2048]{1,0:T(8,128)(2,1)S(1)} collective-permute-done((bf16[16,2048]{1,0:T(8,128)(2,1)S(1)}, bf16[16,2048]{1,0:T(8,128)(2,1)S(1)}, u32[]{:S(2)}, u32[]{:S(2)}) %collective-permute-start) | collective-permute-done | bytes 65568 | tf_op jit(solution)/shard_map/ppermute | solution.py:469
  6.9 0.0 copy-done.7
  7.0 0.4 shard_map.212
  7.4 21.2 %all_to_all.20.got_ref.line_own_ref.line_ref = bf16[8,16,1152]{2,1,0:T(8,128)(2,1)S(1)} all-to-all(bf16[8,16,1152]{2,1,0:T(8,128)(2,1)S(1)} %get-tuple-element.20), channel_id=1, replica_groups=mesh['ep_0'=8,'ep_1'=4,'ep_2'=4,'tp'=2] {'ep_0'}, dimensions={0} | all-to-all | bytes 589824 | tf_op jit(solution)/shard_map/all_to_all | solution.py:493
  28.6 0.5 shard_map.213
  29.1 21.1 %all_to_all.21.slots_ref.own_ref = bf16[16,16,1792]{2,1,0:T(8,128)(2,1)S(1)} all-to-all(bf16[16,16,1792]{2,1,0:T(8,128)(2,1)S(1)} %get-tuple-element.21), channel_id=1, replica_groups=mesh['ep_0'=8,'ep_1'=4,'ep_2'=4,'tp'=2] {'ep_1','ep_2'}, dimensions={0} | all-to-all | bytes 1835008 | tf_op jit(solution)/shard_map/all_to_all | solution.py:505
  50.2 0.0 collective-permute-start.1
  50.2 0.5 collective-permute-start.2
  50.7 0.0 copy-done.4
  50.7 1.2 %shard_map.214 = (f32[256,256]{1,0:T(8,128)S(1)}, f32[256,256]{1,0:T(8,128)S(1)}, bf16[16,64]{1,0:T(8,128)(2,1)}, bf16[16,64]{1,0:T(8,128)(2,1)}) custom-call(s32[1]{0:T(128)} %bitcast.core_ref, bf16[16,16,1792]{2,1,0:T(8,128)(2,1)S(1)} %all_to_all.21.slots_ref.own_ref, bf16[2048,256]{1,0:T(8,128)(2,1)S(1)} %bitcast.16, bf16[2048,256]{1,0:T(8,128)(2,1)S(1)} %bitcast.18, ...), custom_call_target="tpu_custom_call" | custom-call | tf_op jit(solution)/shard_map/pallas_call | solution.py:175
  51.9 1.2 %collective-permute-done.2.line_other_ref = bf16[8,16,1152]{2,1,0:T(8,128)(2,1)S(1)} collective-permute-done((bf16[8,16,1152]{2,1,0:T(8,128)(2,1)S(1)}, bf16[8,16,1152]{2,1,0:T(8,128)(2,1)S(1)}, u32[]{:S(2)}, u32[]{:S(2)}) %collective-permute-start.2) | collective-permute-done | bytes 294944 | tf_op jit(solution)/shard_map/ppermute | solution.py:494
  53.1 0.0 collective-permute-done.1.other_ref
  53.1 0.7 shard_map.215
  53.8 0.2 collective-permute-start.3
  54.0 1.3 %shard_map.216 = (bf16[256,1024]{1,0:T(8,128)(2,1)S(1)}, f32[128,1024]{1,0:T(8,128)S(1)}) custom-call(s32[1]{0:T(128)} %bitcast.core_ref, bf16[256,256]{1,0:T(8,128)(2,1)S(1)} %get-tuple-element.24.hidden_ref, bf16[256,2048]{1,0:T(8,128)(2,1)S(1)} %bitcast.21, bf16[16,16,1792]{2,1,0:T(8,128)(2,1)S(1)} %all_to_all.21.slots_ref.own_ref, ...), custom_call_target="tpu_custom_call" | custom-call | tf_op jit(solution)/shard_map/pallas_call | solution.py:175
  55.3 0.5 collective-permute-done.3
  55.8 0.2 add_convert_fusion
  56.0 14.7 %all_to_all.22.back_ref = bf16[16,16,1024]{2,1,0:T(8,128)(2,1)S(1)} all-to-all(bf16[16,16,1024]{2,1,0:T(8,128)(2,1)S(1)} %bitcast.29), channel_id=1, replica_groups=mesh['ep_0'=8,'ep_1'=4,'ep_2'=4,'tp'=2] {'ep_1','ep_2'}, dimensions={0} | all-to-all | bytes 1048576 | tf_op jit(solution)/shard_map/all_to_all | solution.py:536
  70.7 0.3 shard_map.217
  71.0 13.6 %all_to_all.23.parts_ref = bf16[8,16,1024]{2,1,0:T(8,128)(2,1)S(1)} all-to-all(bf16[8,16,1024]{2,1,0:T(8,128)(2,1)S(1)} %shard_map.217), channel_id=1, replica_groups=mesh['ep_0'=8,'ep_1'=4,'ep_2'=4,'tp'=2] {'ep_0'}, dimensions={0} | all-to-all | bytes 524288 | tf_op jit(solution)/shard_map/all_to_all | solution.py:544
  84.5 0.7 shard_map.218
  (16 shorter events, 0.0 us)
Async XLA Ops:
  0.6 5.1 %copy-start.12 = (s32[16,6]{0,1:T(8,128)S(1)}, s32[16,6]{0,1:T(8,128)}, u32[]{:S(2)}) copy-start(s32[16,6]{0,1:T(8,128)} %param.32) | copy-start | bytes 1156
  0.6 6.3 %copy-start.3 = (bf16[16,2048]{1,0:T(8,128)(2,1)S(1)}, bf16[16,2048]{1,0:T(8,128)(2,1)}, u32[]{:S(2)}) copy-start(bf16[16,2048]{1,0:T(8,128)(2,1)} %tokens_ref.3) | copy-start | bytes 196612
  0.7 6.3 %copy-start.7 = (f32[2048]{0:T(1024)S(1)}, f32[2048]{0:T(1024)}, u32[]{:S(2)}) copy-start(f32[2048]{0:T(1024)} %param.30) | copy-start | bytes 24580
  0.7 6.3 %copy-start.8 = (bf16[16,256]{1,0:T(8,128)(2,1)S(1)}, bf16[16,256]{1,0:T(8,128)(2,1)}, u32[]{:S(2)}) copy-start(bf16[16,256]{1,0:T(8,128)(2,1)} %gate_ref.1) | copy-start | bytes 24580
  0.7 6.3 %copy-start.9 = (bf16[16,256]{1,0:T(8,128)(2,1)S(1)}, bf16[16,256]{1,0:T(8,128)(2,1)}, u32[]{:S(2)}) copy-start(bf16[16,256]{1,0:T(8,128)(2,1)} %up_ref.1) | copy-start | bytes 24580
  0.7 6.3 %copy-start.10 = (bf16[256,16]{0,1:T(8,128)(2,1)S(1)}, bf16[256,16]{0,1:T(8,128)(2,1)}, u32[]{:S(2)}) copy-start(bf16[256,16]{0,1:T(8,128)(2,1)} %param.35) | copy-start | bytes 24580
  0.7 6.3 %copy-start.11 = (f32[2048]{0:T(1024)S(1)}, f32[2048]{0:T(1024)}, u32[]{:S(2)}) copy-start(f32[2048]{0:T(1024)} %param.36) | copy-start | bytes 24580
  5.5 45.2 %copy-start = (bf16[1,2048,256]{2,1,0:T(8,128)(2,1)S(1)}, bf16[1,2048,256]{2,1,0:T(8,128)(2,1)}, u32[]{:S(2)}) copy-start(bf16[1,2048,256]{2,1,0:T(8,128)(2,1)} %param.37) | copy-start | bytes 3145732
  5.6 45.2 %copy-start.1 = (bf16[1,2048,256]{2,1,0:T(8,128)(2,1)S(1)}, bf16[1,2048,256]{2,1,0:T(8,128)(2,1)}, u32[]{:S(2)}) copy-start(bf16[1,2048,256]{2,1,0:T(8,128)(2,1)} %param.38) | copy-start | bytes 3145732
  5.6 45.2 %copy-start.4 = (bf16[2048,64]{0,1:T(8,128)(2,1)S(1)}, bf16[2048,64]{0,1:T(8,128)(2,1)}, u32[]{:S(2)}) copy-start(bf16[2048,64]{0,1:T(8,128)(2,1)} %param.24) | copy-start | bytes 786436
  5.6 45.1 %copy-start.5 = (bf16[2048,64]{0,1:T(8,128)(2,1)S(1)}, bf16[2048,64]{0,1:T(8,128)(2,1)}, u32[]{:S(2)}) copy-start(bf16[2048,64]{0,1:T(8,128)(2,1)} %param.25) | copy-start | bytes 786436
  5.6 45.1 %copy-start.6 = (f32[2048]{0:T(1024)S(1)}, f32[2048]{0:T(1024)}, u32[]{:S(2)}) copy-start(f32[2048]{0:T(1024)} %param.22) | copy-start | bytes 24580
  5.6 1.3 %collective-permute-start = (bf16[16,2048]{1,0:T(8,128)(2,1)S(1)}, bf16[16,2048]{1,0:T(8,128)(2,1)S(1)}, u32[]{:S(2)}, u32[]{:S(2)}) collective-permute-start(bf16[16,2048]{1,0:T(8,128)(2,1)S(1)} %get-tuple-element.17.own_ref), channel_id=1, source_target_pairs={{0,1},{1,0},{2,3},{3,2},{4,5},{5,4},{6,7},{7,6},{8,9},{9,8},{10,11... | collective-permute-start | bytes 196616 | tf_op jit(solution)/shard_map/ppermute | solution.py:469
  50.2 2.9 %copy-start.2 = (bf16[1,256,2048]{2,1,0:T(8,128)(2,1)S(1)}, bf16[1,256,2048]{2,1,0:T(8,128)(2,1)}, u32[]{:S(2)}) copy-start(bf16[1,256,2048]{2,1,0:T(8,128)(2,1)} %param.39) | copy-start | bytes 3145732
  50.2 2.9 %collective-permute-start.1 = (bf16[16,16,1792]{2,1,0:T(8,128)(2,1)S(1)}, bf16[16,16,1792]{2,1,0:T(8,128)(2,1)S(1)}, u32[]{:S(2)}, u32[]{:S(2)}) collective-permute-start(bf16[16,16,1792]{2,1,0:T(8,128)(2,1)S(1)} %all_to_all.21.slots_ref.own_ref), channel_id=1, source_target_pairs={{0,1},{1,0},{2,3},{3,2},{4,5},{5,4},{6,7},{7,6},{8,9},{9,8},{10,11... | collective-permute-start | bytes 2752520 | tf_op jit(solution)/shard_map/ppermute | solution.py:506
  50.2 2.9 %collective-permute-start.2 = (bf16[8,16,1152]{2,1,0:T(8,128)(2,1)S(1)}, bf16[8,16,1152]{2,1,0:T(8,128)(2,1)S(1)}, u32[]{:S(2)}, u32[]{:S(2)}) collective-permute-start(bf16[8,16,1152]{2,1,0:T(8,128)(2,1)S(1)} %all_to_all.20.got_ref.line_own_ref.line_ref), channel_id=1, source_target_pairs={{0,1},{1,0},{2,3},{3,2},{4,5},{5,4},{6,7},{7,6},{8,9},{9,8},{10,11... | collective-permute-start | bytes 884744 | tf_op jit(solution)/shard_map/ppermute | solution.py:494
  53.8 2.0 %collective-permute-start.3 = (bf16[256,1024]{1,0:T(8,128)(2,1)S(1)}, bf16[256,1024]{1,0:T(8,128)(2,1)S(1)}, u32[]{:S(2)}, u32[]{:S(2)}) collective-permute-start(bf16[256,1024]{1,0:T(8,128)(2,1)S(1)} %get-tuple-element.26), channel_id=1, source_target_pairs={{0,1},{1,0},{2,3},{3,2},{4,5},{5,4},{6,7},{7,6},{8,9},{9,8},{10,11... | collective-permute-start | bytes 1572872 | tf_op jit(solution)/shard_map/ppermute | solution.py:527

commit v7 on v6

--- a/solution.py
+++ b/solution.py
@@ -244,20 +244,16 @@
         send_ref[line, :, half:] = block.astype(BF16)
 
 
-def slots_kernel(line_ref, got_ref, send_ref, combine_ref):
-    lines, seq_count, width = got_ref.shape
-    places = send_ref.shape[0]
-    half = width - 128
+def slot_map(line, got, lines, seq_count, places, width):
     token_total = lines * seq_count
     capacity = seq_count
-    slot_total = places * capacity
-    got = got_ref[...].reshape(token_total, width)
-    meta = got[:, half:].astype(F32).T
-    slot = lax.broadcasted_iota(jnp.int32, (slot_total, token_total), 0)
-    token = lax.broadcasted_iota(jnp.int32, (slot_total, token_total), 1)
-    expert = (line_ref[0] * places + slot // capacity).astype(F32)
-    hit = jnp.zeros((slot_total, token_total), F32)
-    gate = jnp.zeros((slot_total, token_total), F32)
+    shape = (places * capacity, token_total)
+    meta = got[:, width - 128 :].astype(F32).T
+    slot = lax.broadcasted_iota(jnp.int32, shape, 0)
+    token = lax.broadcasted_iota(jnp.int32, shape, 1)
+    expert = (line * places + slot // capacity).astype(F32)
+    hit = jnp.zeros(shape, F32)
+    gate = jnp.zeros(shape, F32)
     for k in range(6):
         same = meta[k : k + 1] == expert
         hit = jnp.where(same, 1.0, hit)
@@ -271,7 +267,16 @@
         token // seq_count == slot % capacity // per_source,
         rank == (slot % per_source).astype(F32),
     )
-    chosen = jnp.where(here, hit, 0.0)
+    return jnp.where(here, hit, 0.0), jnp.where(here, gate * hit, 0.0)
+
+
+def slots_kernel(line_ref, got_ref, send_ref):
+    lines, seq_count, width = got_ref.shape
+    places = send_ref.shape[0]
+    half = width - 128
+    capacity = seq_count
+    got = got_ref[...].reshape(lines * seq_count, width)
+    chosen, _ = slot_map(line_ref[0], got, lines, seq_count, places, width)
     rows = jnp.dot(chosen.astype(BF16), got[:, :half], preferred_element_type=F32)
     send_ref[:, :, :half] = rows.astype(BF16).reshape(places, capacity, half)
     group = (lax.broadcasted_iota(jnp.int32, (seq_count, 128), 1)) // 32
@@ -284,10 +289,6 @@
                 tile = jnp.where(group == k, moved, tile)
             at = half + (n * lines + first) * 32
             send_ref[:, :, at : at + 128] = jnp.broadcast_to(tile.astype(BF16)[None], (places, seq_count, 128))
-    weights = jnp.where(here, gate * hit, 0.0).T
-    high = weights.astype(BF16)
-    combine_ref[:, :slot_total] = high
-    combine_ref[:, slot_total:] = (weights - high.astype(F32)).astype(BF16)
 
 
 def dense_weights(slots_ref, half, part, line):
@@ -337,7 +338,9 @@
 
 def own_kernel(
     core_ref,
+    line_ref,
     slots_ref,
+    got_ref,
     gate_ref,
     up_ref,
     tokens_ref,
@@ -348,6 +351,7 @@
     up_out,
     keys_ref,
     values_ref,
+    combine_ref,
 ):
     core = core_ref[0]
     gate_out[...], up_out[...] = half_products(core, slots_ref, gate_ref.shape[0], gate_ref, up_ref)
@@ -356,6 +360,13 @@
         target_ref[...] = lax.dot_general(
             normed, weight_ref[...], (((1,), (1,)), ((), ())), preferred_element_type=F32
         ).astype(BF16)
+    lines, seq_count, width = got_ref.shape
+    got = got_ref[...].reshape(lines * seq_count, width)
+    gates = slot_map(line_ref[0], got, lines, seq_count, slots_ref.shape[0], width)[1].T
+    high = gates.astype(BF16)
+    slot_total = gates.shape[1]
+    combine_ref[:, :slot_total] = high
+    combine_ref[:, slot_total:] = (gates - high.astype(F32)).astype(BF16)
 
 
 def down_product(side, hidden, down_ref):
@@ -492,12 +503,9 @@
     )
     line_own = lax.all_to_all(line_send, LINE, 0, 0, tiled=True)
     line_other = lax.ppermute(line_own, "tp", SWAP)
-    slot_send, combine = call(
+    slot_send = call(
         slots_kernel,
-        (
-            jax.ShapeDtypeStruct((places, seq_count, half + 96 * lines), BF16),
-            jax.ShapeDtypeStruct((token_total, 2 * slot_total), BF16),
-        ),
+        jax.ShapeDtypeStruct((places, seq_count, half + 96 * lines), BF16),
         1,
         (line, line_own),
         8,
@@ -509,11 +517,16 @@
     hidden_shape = (slot_total, w_expert_gate.shape[2])
     new_shape = jax.ShapeDtypeStruct((seq_count, w_key.shape[1]), BF16)
     dense_shape = jax.ShapeDtypeStruct((token_total, half), F32)
-    gate_sum, up_sum, new_keys, new_values = call(
+    gate_sum, up_sum, new_keys, new_values, combine = call(
         own_kernel,
-        (*(jax.ShapeDtypeStruct(hidden_shape, F32),) * 2, new_shape, new_shape),
-        1,
-        (core, slot_own, *weights, tokens, attn_gain.reshape(1, width), w_key.T, w_value.T),
+        (
+            *(jax.ShapeDtypeStruct(hidden_shape, F32),) * 2,
+            new_shape,
+            new_shape,
+            jax.ShapeDtypeStruct((token_total, 2 * slot_total), BF16),
+        ),
+        2,
+        (core, line, slot_own, line_own, *weights, tokens, attn_gain.reshape(1, width), w_key.T, w_value.T),
         8,
     )
     result_shape = jax.ShapeDtypeStruct((slot_total, half), BF16)

time: 85.4 us -> 85.5 us (level)
  no operation moved by 1% of the time
where the time goes in v7:
time: 85.5 us; the launch traced here: 85.3 us
  blocking collectives  70.6 us (83%)
  Pallas kernels  9.88 us (12%)
  waiting for transfers between devices  2.76 us (3%)
    all_to_all x1, blocking collectives, shards(): line_own = lax.all_to_all(line_send, LINE, 0, 0, tiled=True)  21.3 us
    all_to_all x1, blocking collectives, shards(): slot_own = lax.all_to_all(slot_send, PLANE, 0, 0, tiled=True)  21.1 us
    all_to_all x1, blocking collectives, shards(): lax.all_to_all(results.reshape(places, seq_count, half), PLANE, 0, 0, til...  14.7 us
    all_to_all x1, blocking collectives, shards(): parts = lax.all_to_all(partial, LINE, 0, 0, tiled=True)  13.6 us
    pallas_call x8, Pallas kernels, call(): pl.pallas_call(kernel, out_shape=out_shape, in_specs=in_specs, out_specs=...  9.88 us
  transfers between devices with their start and end apart: 4, of which 3 were waited for; matrix products, arithmetic and copies ran while one was open for 0% of the time, Pallas kernels for 3%

profile of v7, /device:TPU:2, one launch (start us, length us, event | category | flops | bytes accessed | tf_op | source)
XLA Modules:
  0.0 85.3 jit_solution(1814083848799275034)
XLA Ops:
  0.6 0.0 copy-start.12
  0.7 4.8 %shard_map.211 = (bf16[16,2048]{1,0:T(8,128)(2,1)S(1)}, bf16[2048,128]{1,0:T(8,128)(2,1)S(1)}) custom-call(f32[1,8]{1,0:T(1,128)} %bitcast.32, s32[1,16]{1,0:T(1,128)} %bitcast.33, bf16[16,2048]{1,0:T(8,128)(2,1)} %tokens_ref.3, f32[1,2048]{1,0:T(1,128)} %bitcast.24, bf16[2048,512]{1,0:T(8,128)(2,1)} %query_hbm.1, bf16[1024,1024]{1,0:T(8,128)(2,1)} %bitcast.30, ...), custom_call_target="tpu_custom_call" | custom-call | tf_op jit(solution)/shard_map/pallas_call | solution.py:175
  5.5 0.1 collective-permute-start
  5.6 0.0 copy-done.12
  5.7 0.1 copy.23.routes_ref
  5.7 1.1 %collective-permute-done.other_ref = bf16[16,2048]{1,0:T(8,128)(2,1)S(1)} collective-permute-done((bf16[16,2048]{1,0:T(8,128)(2,1)S(1)}, bf16[16,2048]{1,0:T(8,128)(2,1)S(1)}, u32[]{:S(2)}, u32[]{:S(2)}) %collective-permute-start) | collective-permute-done | bytes 65568 | tf_op jit(solution)/shard_map/ppermute | solution.py:480
  6.9 0.0 copy-done.7
  6.9 0.0 copy-start
  6.9 0.0 copy-start.1
  6.9 0.0 copy-start.4
  7.0 0.0 copy-start.5
  7.0 0.0 copy-start.6
  7.0 0.4 shard_map.212
  7.4 21.3 %all_to_all.20.got_ref.line_own_ref.line_ref = bf16[8,16,1152]{2,1,0:T(8,128)(2,1)S(1)} all-to-all(bf16[8,16,1152]{2,1,0:T(8,128)(2,1)S(1)} %get-tuple-element.19), channel_id=1, replica_groups=mesh['ep_0'=8,'ep_1'=4,'ep_2'=4,'tp'=2] {'ep_0'}, dimensions={0} | all-to-all | bytes 589824 | tf_op jit(solution)/shard_map/all_to_all | solution.py:504
  28.7 0.5 shard_map.213
  29.2 21.1 %all_to_all.21.slots_ref.own_ref = bf16[16,16,1792]{2,1,0:T(8,128)(2,1)S(1)} all-to-all(bf16[16,16,1792]{2,1,0:T(8,128)(2,1)S(1)} %shard_map.213), channel_id=1, replica_groups=mesh['ep_0'=8,'ep_1'=4,'ep_2'=4,'tp'=2] {'ep_1','ep_2'}, dimensions={0} | all-to-all | bytes 1835008 | tf_op jit(solution)/shard_map/all_to_all | solution.py:513
  50.3 0.0 collective-permute-start.1
  50.3 0.5 collective-permute-start.2
  50.8 0.0 copy-done
  50.8 0.0 copy-done.4
  50.8 1.2 %shard_map.214 = (f32[256,256]{1,0:T(8,128)S(1)}, f32[256,256]{1,0:T(8,128)S(1)}, bf16[16,64]{1,0:T(8,128)(2,1)}, bf16[16,64]{1,0:T(8,128)(2,1)}, bf16[128,512]{1,0:T(8,128)(2,1)S(1)}) custom-call(s32[1]{0:T(128)} %bitcast.core_ref, s32[1]{0:T(128)} %bitcast.1.line_ref, bf16[16,16,1792]{2,1,0:T(8,128)(2,1)S(1)} %all_to_all.21.slots_ref.own_ref, ...), custom_call_target="tpu_custom_call" | custom-call | tf_op jit(solution)/shard_map/pallas_call | solution.py:175
  52.0 1.2 %collective-permute-done.2.line_other_ref = bf16[8,16,1152]{2,1,0:T(8,128)(2,1)S(1)} collective-permute-done((bf16[8,16,1152]{2,1,0:T(8,128)(2,1)S(1)}, bf16[8,16,1152]{2,1,0:T(8,128)(2,1)S(1)}, u32[]{:S(2)}, u32[]{:S(2)}) %collective-permute-start.2) | collective-permute-done | bytes 294944 | tf_op jit(solution)/shard_map/ppermute | solution.py:505
  53.2 0.0 collective-permute-done.1.other_ref
  53.2 0.7 shard_map.215
  53.9 0.2 collective-permute-start.3
  54.1 1.3 %shard_map.216 = (bf16[256,1024]{1,0:T(8,128)(2,1)S(1)}, f32[128,1024]{1,0:T(8,128)S(1)}) custom-call(s32[1]{0:T(128)} %bitcast.core_ref, bf16[256,256]{1,0:T(8,128)(2,1)S(1)} %get-tuple-element.22.hidden_ref, bf16[256,2048]{1,0:T(8,128)(2,1)S(1)} %bitcast.21, bf16[16,16,1792]{2,1,0:T(8,128)(2,1)S(1)} %all_to_all.21.slots_ref.own_ref, ...), custom_call_target="tpu_custom_call" | custom-call | tf_op jit(solution)/shard_map/pallas_call | solution.py:175
  55.4 0.5 collective-permute-done.3
  55.9 0.2 add_convert_fusion
  56.1 14.7 %all_to_all.22.back_ref = bf16[16,16,1024]{2,1,0:T(8,128)(2,1)S(1)} all-to-all(bf16[16,16,1024]{2,1,0:T(8,128)(2,1)S(1)} %bitcast.29), channel_id=1, replica_groups=mesh['ep_0'=8,'ep_1'=4,'ep_2'=4,'tp'=2] {'ep_1','ep_2'}, dimensions={0} | all-to-all | bytes 1048576 | tf_op jit(solution)/shard_map/all_to_all | solution.py:549
  70.8 0.3 shard_map.217
  71.1 13.6 %all_to_all.23.parts_ref = bf16[8,16,1024]{2,1,0:T(8,128)(2,1)S(1)} all-to-all(bf16[8,16,1024]{2,1,0:T(8,128)(2,1)S(1)} %shard_map.217), channel_id=1, replica_groups=mesh['ep_0'=8,'ep_1'=4,'ep_2'=4,'tp'=2] {'ep_0'}, dimensions={0} | all-to-all | bytes 524288 | tf_op jit(solution)/shard_map/all_to_all | solution.py:557
  84.6 0.7 shard_map.218
  (16 shorter events, 0.0 us)
Async XLA Ops:
  0.6 5.0 %copy-start.12 = (s32[16,6]{0,1:T(8,128)S(1)}, s32[16,6]{0,1:T(8,128)}, u32[]{:S(2)}) copy-start(s32[16,6]{0,1:T(8,128)} %param.32) | copy-start | bytes 1156
  0.6 6.2 %copy-start.3 = (bf16[16,2048]{1,0:T(8,128)(2,1)S(1)}, bf16[16,2048]{1,0:T(8,128)(2,1)}, u32[]{:S(2)}) copy-start(bf16[16,2048]{1,0:T(8,128)(2,1)} %tokens_ref.3) | copy-start | bytes 196612
  0.7 6.2 %copy-start.7 = (f32[2048]{0:T(1024)S(1)}, f32[2048]{0:T(1024)}, u32[]{:S(2)}) copy-start(f32[2048]{0:T(1024)} %param.30) | copy-start | bytes 24580
  0.7 6.2 %copy-start.8 = (bf16[16,256]{1,0:T(8,128)(2,1)S(1)}, bf16[16,256]{1,0:T(8,128)(2,1)}, u32[]{:S(2)}) copy-start(bf16[16,256]{1,0:T(8,128)(2,1)} %gate_ref.1) | copy-start | bytes 24580
  0.7 6.2 %copy-start.9 = (bf16[16,256]{1,0:T(8,128)(2,1)S(1)}, bf16[16,256]{1,0:T(8,128)(2,1)}, u32[]{:S(2)}) copy-start(bf16[16,256]{1,0:T(8,128)(2,1)} %up_ref.1) | copy-start | bytes 24580
  0.7 6.2 %copy-start.10 = (bf16[256,16]{0,1:T(8,128)(2,1)S(1)}, bf16[256,16]{0,1:T(8,128)(2,1)}, u32[]{:S(2)}) copy-start(bf16[256,16]{0,1:T(8,128)(2,1)} %param.35) | copy-start | bytes 24580
  0.7 6.2 %copy-start.11 = (f32[2048]{0:T(1024)S(1)}, f32[2048]{0:T(1024)}, u32[]{:S(2)}) copy-start(f32[2048]{0:T(1024)} %param.36) | copy-start | bytes 24580
  5.5 1.3 %collective-permute-start = (bf16[16,2048]{1,0:T(8,128)(2,1)S(1)}, bf16[16,2048]{1,0:T(8,128)(2,1)S(1)}, u32[]{:S(2)}, u32[]{:S(2)}) collective-permute-start(bf16[16,2048]{1,0:T(8,128)(2,1)S(1)} %get-tuple-element.16.own_ref), channel_id=1, source_target_pairs={{0,1},{1,0},{2,3},{3,2},{4,5},{5,4},{6,7},{7,6},{8,9},{9,8},{10,11... | collective-permute-start | bytes 196616 | tf_op jit(solution)/shard_map/ppermute | solution.py:480
  6.9 43.9 %copy-start = (bf16[1,2048,256]{2,1,0:T(8,128)(2,1)S(1)}, bf16[1,2048,256]{2,1,0:T(8,128)(2,1)}, u32[]{:S(2)}) copy-start(bf16[1,2048,256]{2,1,0:T(8,128)(2,1)} %param.37) | copy-start | bytes 3145732
  6.9 43.9 %copy-start.1 = (bf16[1,2048,256]{2,1,0:T(8,128)(2,1)S(1)}, bf16[1,2048,256]{2,1,0:T(8,128)(2,1)}, u32[]{:S(2)}) copy-start(bf16[1,2048,256]{2,1,0:T(8,128)(2,1)} %param.38) | copy-start | bytes 3145732
  6.9 43.9 %copy-start.4 = (bf16[2048,64]{0,1:T(8,128)(2,1)S(1)}, bf16[2048,64]{0,1:T(8,128)(2,1)}, u32[]{:S(2)}) copy-start(bf16[2048,64]{0,1:T(8,128)(2,1)} %param.24) | copy-start | bytes 786436
  7.0 43.8 %copy-start.5 = (bf16[2048,64]{0,1:T(8,128)(2,1)S(1)}, bf16[2048,64]{0,1:T(8,128)(2,1)}, u32[]{:S(2)}) copy-start(bf16[2048,64]{0,1:T(8,128)(2,1)} %param.25) | copy-start | bytes 786436
  7.0 43.8 %copy-start.6 = (f32[2048]{0:T(1024)S(1)}, f32[2048]{0:T(1024)}, u32[]{:S(2)}) copy-start(f32[2048]{0:T(1024)} %param.22) | copy-start | bytes 24580
  50.3 2.9 %copy-start.2 = (bf16[1,256,2048]{2,1,0:T(8,128)(2,1)S(1)}, bf16[1,256,2048]{2,1,0:T(8,128)(2,1)}, u32[]{:S(2)}) copy-start(bf16[1,256,2048]{2,1,0:T(8,128)(2,1)} %param.39) | copy-start | bytes 3145732
  50.3 2.9 %collective-permute-start.1 = (bf16[16,16,1792]{2,1,0:T(8,128)(2,1)S(1)}, bf16[16,16,1792]{2,1,0:T(8,128)(2,1)S(1)}, u32[]{:S(2)}, u32[]{:S(2)}) collective-permute-start(bf16[16,16,1792]{2,1,0:T(8,128)(2,1)S(1)} %all_to_all.21.slots_ref.own_ref), channel_id=1, source_target_pairs={{0,1},{1,0},{2,3},{3,2},{4,5},{5,4},{6,7},{7,6},{8,9},{9,8},{10,11... | collective-permute-start | bytes 2752520 | tf_op jit(solution)/shard_map/ppermute | solution.py:514
  50.3 2.9 %collective-permute-start.2 = (bf16[8,16,1152]{2,1,0:T(8,128)(2,1)S(1)}, bf16[8,16,1152]{2,1,0:T(8,128)(2,1)S(1)}, u32[]{:S(2)}, u32[]{:S(2)}) collective-permute-start(bf16[8,16,1152]{2,1,0:T(8,128)(2,1)S(1)} %all_to_all.20.got_ref.line_own_ref.line_ref), channel_id=1, source_target_pairs={{0,1},{1,0},{2,3},{3,2},{4,5},{5,4},{6,7},{7,6},{8,9},{9,8},{10,11... | collective-permute-start | bytes 884744 | tf_op jit(solution)/shard_map/ppermute | solution.py:505
  53.9 2.0 %collective-permute-start.3 = (bf16[256,1024]{1,0:T(8,128)(2,1)S(1)}, bf16[256,1024]{1,0:T(8,128)(2,1)S(1)}, u32[]{:S(2)}, u32[]{:S(2)}) collective-permute-start(bf16[256,1024]{1,0:T(8,128)(2,1)S(1)} %get-tuple-element.24), channel_id=1, source_target_pairs={{0,1},{1,0},{2,3},{3,2},{4,5},{5,4},{6,7},{7,6},{8,9},{9,8},{10,11... | collective-permute-start | bytes 1572872 | tf_op jit(solution)/shard_map/ppermute | solution.py:540
